TPU v7x, 32 devices: a whole 2x2x4 slice. The times are simulated.
32 devices in a mesh: sp: 8 (over z, y), tp: 4 (over x, core).
Axes of the slice: x: 2, y: 2, z: 4, core: 2. Of those that a mesh axis runs over, the one named last changes fastest.
Arguments:
- latent: bfloat16 [3072, 2048], P(('sp', 'tp')), may hold values from -6 to 6
- context: bfloat16 [512, 2048], P('sp'), may hold values from -6 to 6
- cond_latent: float32 [2048], replicated, may hold values from -6 to 6
- cond_context: float32 [2048], replicated, may hold values from -12 to 12
- shift_weight: bfloat16 [2048, 2048], P('sp', 'tp'), may hold values from -0.125 to 0.125
- scale_weight: bfloat16 [2048, 2048], P('sp', 'tp'), may hold values from -0.125 to 0.125
- gate_weight: bfloat16 [2048, 2048], P('sp', 'tp'), may hold values from -0.125 to 0.125
- query_weight: bfloat16 [2, 2048, 1024], P(None, None, 'tp'), may hold values from -1.3258252 to 1.3258252
- key_weight: bfloat16 [2, 2048, 1024], P(None, None, 'tp'), may hold values from -1.3258252 to 1.3258252
- value_weight: bfloat16 [2048, 2048], P(None, 'tp'), may hold values from -0.125 to 0.125
- out_weight: bfloat16 [2048, 2048], P('tp'), may hold values from -0.125 to 0.125
- lambda_heads: float32 [16], P('tp'), may hold values from 0.3 to 0.8
- out_gain: float32 [2048], P('tp'), may hold values from 0.1 to 1.9
Outputs:
- result: bfloat16 [3072, 2048], P(('sp', 'tp'))
All inputs are finite; a program needn't handle non-finite values.
Results may differ from a plain program's by a relative error of at most 0.02.
The roundings to bfloat16 on the way count: a program that leaves them out, or rounds other values in their place, can miss the bound.
Values may be sent and summed in bfloat16 or wider, within the bound.
No kernel may reach another device: no remote copies, remote signals or barrier semaphores. Data moves between devices by JAX's collectives and lax.ppermute only.
A program may use at most 128 MiB of HBM per device.

v0:
```python
import jax
import jax.numpy as jnp
from jax import lax
from jax.sharding import PartitionSpec as P

HEAD_DIM = 64
GRID_W = 64
VALUE_DIM = 128


norm_eps = 1e-06
rope_theta = 10000.0
block_limit = 1024


def rms_scale(matrix):
    return matrix * lax.rsqrt(jnp.mean(matrix * matrix, axis=-1, keepdims=True) + norm_eps)


def modulated(activations, shift, scale):
    return (rms_scale(activations.astype(jnp.float32)) * (1.0 + scale) + shift).astype(jnp.bfloat16)


def rotate(vectors, positions, grid_width):
    quarter = vectors.shape[-1] // 4
    inverse = rope_theta ** (-jnp.arange(quarter, dtype=jnp.float32) / quarter)
    grid_row = (positions // grid_width).astype(jnp.float32)
    grid_col = (positions % grid_width).astype(jnp.float32)
    angles = jnp.concatenate([grid_row[:, None] * inverse, grid_col[:, None] * inverse], axis=-1)
    cos_table = jnp.cos(angles)[:, None, :]
    sin_table = jnp.sin(angles)[:, None, :]
    former = vectors[..., : 2 * quarter]
    latter = vectors[..., 2 * quarter :]
    return jnp.concatenate(
        [former * cos_table - latter * sin_table, latter * cos_table + former * sin_table], axis=-1
    )


def absorb(carry_state, key_block, value_block, queries, head_count):
    maxima, totals, numerator = carry_state
    row_count = key_block.shape[0]
    scores = jnp.einsum(
        "mhqd,kmhd->mhqk",
        queries,
        key_block.reshape(row_count, 2, head_count, HEAD_DIM),
        preferred_element_type=jnp.float32,
    ) * HEAD_DIM ** (-0.5)
    new_maxima = jnp.maximum(maxima, jnp.max(scores, axis=-1))
    rescale = jnp.exp(maxima - new_maxima)
    weights = jnp.exp(scores - new_maxima[..., None])
    totals = totals * rescale + jnp.sum(weights, axis=-1)
    numerator = numerator * rescale[..., None] + jnp.einsum(
        "mhqk,khe->mhqe",
        weights.astype(jnp.bfloat16),
        value_block.reshape(row_count, head_count, VALUE_DIM),
        preferred_element_type=jnp.float32,
    )
    return (new_maxima, totals, numerator)


def absorb_all(carry_state, key_rows, value_rows, queries, head_count, shard_len):
    total_rows = key_rows.shape[0]
    shards = total_rows // shard_len
    shard_group = max(
        [
            candidate
            for candidate in range(1, shards + 1)
            if shards % candidate == 0 and candidate * shard_len <= block_limit
        ]
        + [1]
    )
    block_rows = shard_group * shard_len

    def absorb_block(block_index, inner_state):
        key_block = lax.dynamic_slice_in_dim(key_rows, block_index * block_rows, block_rows, 0)
        value_block = lax.dynamic_slice_in_dim(value_rows, block_index * block_rows, block_rows, 0)
        return absorb(inner_state, key_block, value_block, queries, head_count)

    return lax.fori_loop(0, total_rows // block_rows, absorb_block, carry_state)


def local(
    latent,
    context,
    cond_latent,
    cond_context,
    shift_weight,
    scale_weight,
    gate_weight,
    query_weight,
    key_weight,
    value_weight,
    out_weight,
    lambda_heads,
    out_gain,
):
    mod_rows = shift_weight.shape[0]
    conditions = jnp.stack([cond_latent, cond_context])
    conditions = jax.nn.silu(
        lax.dynamic_slice_in_dim(conditions, lax.axis_index("sp") * mod_rows, mod_rows, 1)
    )
    conditions = conditions.astype(jnp.bfloat16)
    partial_value = jnp.concatenate(
        [
            jnp.dot(conditions, shift_weight, preferred_element_type=jnp.float32),
            jnp.dot(conditions, scale_weight, preferred_element_type=jnp.float32),
            jnp.dot(conditions[:1], gate_weight, preferred_element_type=jnp.float32),
        ],
        axis=0,
    )
    summed_mod = lax.psum(partial_value, "sp")
    whole_mod = lax.all_gather(summed_mod, "tp", axis=1, tiled=True)
    hidden = modulated(latent, whole_mod[0], whole_mod[2])
    context_hidden = modulated(context, whole_mod[1], whole_mod[3])
    head_count = lambda_heads.shape[0]
    own_rows = latent.shape[0]
    tok_rows = own_rows * lax.axis_size("tp")
    row_offset = lax.axis_index("sp") * tok_rows
    piece_rows = lax.all_gather(hidden, "tp", axis=0, tiled=True)
    row_count = piece_rows.shape[0]
    positions = row_offset + jnp.arange(row_count, dtype=jnp.int32)

    def rotated(weight):
        product = jnp.concatenate(
            [
                jnp.dot(piece_rows, weight[0], preferred_element_type=jnp.float32),
                jnp.dot(piece_rows, weight[1], preferred_element_type=jnp.float32),
            ],
            axis=-1,
        )
        turned = rotate(product.reshape(row_count, 2 * head_count, HEAD_DIM), positions, GRID_W)
        return turned.reshape(row_count, 2 * head_count * HEAD_DIM).astype(jnp.bfloat16)

    values = jnp.dot(piece_rows, value_weight, preferred_element_type=jnp.float32).astype(
        jnp.bfloat16
    )
    projected = jnp.concatenate([rotated(query_weight), rotated(key_weight), values], axis=-1)
    key_width = 2 * head_count * HEAD_DIM
    queries = (
        projected[:, :key_width].reshape(tok_rows, 2, head_count, HEAD_DIM).transpose(1, 2, 0, 3)
    )
    latent_keys = projected[:, key_width : 2 * key_width]
    latent_values = projected[:, 2 * key_width :]
    context_keys = jnp.concatenate(
        [
            jnp.dot(context_hidden, key_weight[0], preferred_element_type=jnp.float32),
            jnp.dot(context_hidden, key_weight[1], preferred_element_type=jnp.float32),
        ],
        axis=-1,
    ).astype(jnp.bfloat16)
    context_values = jnp.dot(
        context_hidden, value_weight, preferred_element_type=jnp.float32
    ).astype(jnp.bfloat16)
    initial = (
        jnp.full((2, head_count, tok_rows), -jnp.inf, jnp.float32),
        jnp.zeros((2, head_count, tok_rows), jnp.float32),
        jnp.zeros((2, head_count, tok_rows, VALUE_DIM), jnp.float32),
    )
    context_dev = context_keys.shape[0]
    shard_len = tok_rows + context_dev
    value_width = context_values.shape[1]
    joined_keys = jnp.concatenate([latent_keys, context_keys], axis=0)
    joined_values = jnp.concatenate([latent_values, context_values], axis=0)
    context_total = context_dev * lax.axis_size("sp")
    pieces = (
        lax.all_gather(joined_keys, "sp", axis=0, tiled=True),
        lax.all_gather(joined_values, "sp", axis=0, tiled=True),
    )
    attention_state = initial
    shard_count = pieces[0].shape[0] // shard_len
    key_parts = pieces[0].reshape(shard_count, shard_len, key_width)
    value_parts = pieces[1].reshape(shard_count, shard_len, value_width)
    attention_state = absorb_all(
        attention_state,
        key_parts[:, :tok_rows].reshape(shard_count * tok_rows, key_width),
        value_parts[:, :tok_rows].reshape(shard_count * tok_rows, value_width),
        queries,
        head_count,
        tok_rows,
    )
    held_keys = key_parts[:, tok_rows:].reshape(shard_count * context_dev, key_width)
    held_values = value_parts[:, tok_rows:].reshape(shard_count * context_dev, value_width)
    folded, held_keys, held_values = (attention_state, held_keys, held_values)
    final = absorb_all(folded, held_keys, held_values, queries, head_count, context_total)
    totals = final[1]
    numerator = final[2]
    mixed = numerator[0] / totals[0][..., None] - lambda_heads[:, None, None] * (
        numerator[1] / totals[1][..., None]
    )
    normed = rms_scale(mixed) * out_gain.reshape(head_count, 1, VALUE_DIM)
    heads_out = (
        normed.transpose(1, 0, 2).reshape(tok_rows, head_count * VALUE_DIM).astype(jnp.bfloat16)
    )
    summed = lax.psum_scatter(
        jnp.dot(heads_out, out_weight, preferred_element_type=jnp.float32).astype(jnp.bfloat16),
        "tp",
        scatter_dimension=0,
        tiled=True,
    ).astype(jnp.float32)
    return (latent.astype(jnp.float32) + whole_mod[4] * summed).astype(jnp.bfloat16)


def solution(mesh):
    placed = (
        P(("sp", "tp"), None),
        P("sp", None),
        P(),
        P(),
        P("sp", "tp"),
        P("sp", "tp"),
        P("sp", "tp"),
        P(None, None, "tp"),
        P(None, None, "tp"),
        P(None, "tp"),
        P("tp", None),
        P("tp"),
        P("tp"),
    )
    return jax.shard_map(
        local, mesh=mesh, in_specs=placed, out_specs=P(("sp", "tp"), None), check_vma=False
    )
```

profile of v0, /device:TPU:0, one launch (start us, length us, event | category | flops | bytes accessed | tf_op | source)
XLA Modules:
  0.0 315.6 jit_solution(14840474781034838104)
XLA Ops:
  6.5 1.3 fusion.32
  12.0 38.9 %psum.7 = f32[5,512]{1,0:T(8,128)S(1)} all-reduce(f32[5,512]{1,0:T(8,128)S(1)} %pad_maximum_fusion.8), channel_id=1, replica_groups=mesh['sp'=8,'tp'=4] {'sp'}, use_global_device_ids=true, to_apply=%region_0.1 | all-reduce | flops 2560 | bytes 20480 | tf_op jit(solution)/shard_map/psum | solution.py:111
  50.9 5.2 %all_gather.12 = f32[5,2048]{1,0:T(8,128)S(1)} all-gather(f32[5,512]{1,0:T(8,128)S(1)} %psum.7), channel_id=1, replica_groups=mesh['sp'=8,'tp'=4] {'tp'}, dimensions={1}, use_global_device_ids=true | all-gather | bytes 51200 | tf_op jit(solution)/shard_map/all_gather | solution.py:112
  56.7 1.9 fusion.35
  58.9 1.6 convolution_convert_fusion.3
  60.5 1.6 convolution_convert_fusion.4
  62.5 13.2 %all-gather.4.cloned.1.call-done = bf16[384,2048]{1,0:T(8,128)(2,1)} async-done(((bf16[96,2048]{1,0:T(8,128)(2,1)}), bf16[384,2048]{1,0:T(8,128)(2,1)}) %all-gather.4.cloned.1.call-update) | async-done | bytes 1572880 | tf_op jit(solution)/shard_map/all_gather | solution.py:119
  75.7 2.6 fusion.16
  78.3 2.3 fusion.18
  83.8 2.3 convolution_convert_fusion.2
  86.1 2.4 convolution_convert_fusion.1
  89.6 60.5 %all-gather.6.cloned.1.call-done = bf16[3584,512]{1,0:T(8,128)(2,1)} async-done(((bf16[448,512]{1,0:T(8,128)(2,1)}), bf16[3584,512]{1,0:T(8,128)(2,1)}) %all-gather.6.cloned.1.call-update) | async-done | bytes 3670032 | tf_op jit(solution)/shard_map/all_gather | solution.py:166
  151.2 3.8 %slice.98 = bf16[8,384,512]{2,1,0:T(8,128)(2,1)} slice(bf16[8,448,512]{2,1,0:T(8,128)(2,1)} %bitcast.129), slice={[0:8], [0:384], [0:512]} | slice | bytes 6291456 | tf_op jit(solution)/shard_map/slice | solution.py:175
  155.0 62.2 %all-gather.8.cloned.1.call-done = bf16[3584,512]{1,0:T(8,128)(2,1)} async-done(((bf16[448,512]{1,0:T(8,128)(2,1)}), bf16[3584,512]{1,0:T(8,128)(2,1)}) %all-gather.8.cloned.1.call-update) | async-done | bytes 3670032 | tf_op jit(solution)/shard_map/all_gather | solution.py:167
  218.4 3.7 %slice.101 = bf16[8,384,512]{2,1,0:T(8,128)(2,1)} slice(bf16[8,448,512]{2,1,0:T(8,128)(2,1)} %bitcast.131), slice={[0:8], [0:384], [0:512]} | slice | bytes 6291456 | tf_op jit(solution)/shard_map/slice | solution.py:176
  222.1 1.6 reshape.199
  224.6 47.3 %while.5 = (s32[]{:T(128)}, f32[2,4,384]{2,1,0:T(4,128)S(1)}, f32[2,4,384]{2,1,0:T(4,128)}, f32[2,4,384,128]{2,3,0,1:T(8,128)}, bf16[3072,512]{1,0:T(8,128)(2,1)...) while((s32[]{:T(128)}, f32[2,4,384]{2,1,0:T(4,128)S(1)}, ...), condition=%wide.region_6.7_spmd.clone, body=%wide.region_3.6_spmd.clone.sunk | while | flops 921320448 | bytes 52605216 | solution.py:79
  224.6 2.4 constant_dynamic-slice_fusion.3
  227.0 1.2 copy.84
  228.2 1.4 copy.85
  229.6 2.6 bitcast_reduce_fusion.2
  232.2 1.9 fusion.91
  235.3 1.1 copy-done.2
  236.4 2.4 constant_dynamic-slice_fusion.3
  238.8 1.2 copy.84
  240.0 1.4 copy.85
  241.4 2.6 bitcast_reduce_fusion.2
  244.0 1.9 fusion.91
  245.9 1.1 bitcast_add_fusion.3
  247.1 1.1 copy-done.2
  248.2 2.4 constant_dynamic-slice_fusion.3
  250.6 1.2 copy.84
  251.8 1.4 copy.85
  253.2 2.6 bitcast_reduce_fusion.2
  255.8 1.9 fusion.91
  260.0 2.4 constant_dynamic-slice_fusion.3
  262.4 1.2 copy.84
  263.6 1.4 copy.85
  265.0 2.6 bitcast_reduce_fusion.2
  267.6 1.9 fusion.91
  269.6 1.1 bitcast_add_fusion.3
  270.7 1.1 copy-done.2
  271.9 2.4 multiply_reduce_fusion
  274.3 1.6 fusion.9
  276.1 1.2 bitcast_add_fusion.1
  278.1 2.2 convolution_convert_fusion
  280.3 26.9 %reduce-scatter.2.cloned.1.call-done = bf16[96,2048]{1,0:T(8,128)(2,1)} async-done(((bf16[384,2048]{1,0:T(8,128)(2,1)}), bf16[96,2048]{1,0:T(8,128)(2,1)}) %reduce-scatter.2.cloned.1.call-update) | async-done | bytes 393232 | tf_op jit(solution)/shard_map/reduce_scatter | solution.py:194
  307.2 1.9 fusion.36
  (119 shorter events, 17.1 us)
Async XLA Ops:
  6.5 271.6 %copy-start = (bf16[512,2048]{1,0:T(8,128)(2,1)S(1)}, bf16[512,2048]{1,0:T(8,128)(2,1)}, u32[]{:S(2)}) copy-start(bf16[512,2048]{1,0:T(8,128)(2,1)} %param.25) | copy-start | bytes 6291460
  6.5 52.2 %copy-start.7 = (bf16[64,2048]{1,0:T(8,128)(2,1)S(1)}, bf16[64,2048]{1,0:T(8,128)(2,1)}, u32[]{:S(2)}) copy-start(bf16[64,2048]{1,0:T(8,128)(2,1)} %param.16) | copy-start | bytes 786436
  6.5 69.2 %all-gather.4.cloned.1.call-start = ((), (), s32[]{:S(2)}) async-start(), calls=%async_computation.1 | async-start | bytes 1966080 | tf_op jit(solution)/shard_map/all_gather | solution.py:119
  58.7 91.5 %all-gather.6.cloned.1.call-start = ((), (), s32[]{:S(2)}) async-start(), calls=%async_computation.2 | async-start | bytes 4128768 | tf_op jit(solution)/shard_map/all_gather | solution.py:166
  75.7 2.6 copy-start.14
  78.3 2.4 copy-start.15
  78.3 2.5 copy-start.16
  83.8 133.5 %all-gather.8.cloned.1.call-start = ((), (), s32[]{:S(2)}) async-start(), calls=%async_computation.3 | async-start | bytes 4128768 | tf_op jit(solution)/shard_map/all_gather | solution.py:167
  83.8 2.3 copy-start.6
  89.3 217.9 %reduce-scatter.2.cloned.1.call-start = ((), (), s32[]{:S(2)}) async-start(), calls=%async_computation.4 | async-start | bytes 1966080 | tf_op jit(solution)/shard_map/reduce_scatter | solution.py:194
  232.2 1.9 copy-start.8
  232.2 1.9 copy-start.1
  234.1 1.2 copy-start.9
  235.3 1.1 copy-start.2
  244.0 1.9 copy-start.8
  244.0 1.9 copy-start.1
  245.9 1.2 copy-start.9
  247.1 1.1 copy-start.2
  255.8 1.9 copy-start.8
  255.8 1.9 copy-start.1
  257.7 1.2 copy-start.9
  258.9 1.1 copy-start.2
  267.6 1.9 copy-start.8
  267.6 1.9 copy-start.1
  269.5 1.2 copy-start.9
  270.7 1.1 copy-start.2
  274.3 1.7 copy-start.10
  274.3 1.7 copy-start.3
  274.3 1.7 copy-start.5
  276.0 1.2 copy-start.13
  277.3 0.7 copy-start.12
  278.1 29.1 %copy-start.4 = (bf16[96,2048]{1,0:T(8,128)(2,1)S(1)}, bf16[96,2048]{1,0:T(8,128)(2,1)}, u32[]{:S(2)}) copy-start(bf16[96,2048]{1,0:T(8,128)(2,1)} %param.15) | copy-start | bytes 1179652
  278.1 29.1 %copy-start.11 = (f32[1,2048]{1,0:T(1,128)S(1)}, f32[1,2048]{1,0:T(1,128)}, u32[]{:S(2)}) copy-start(f32[1,2048]{1,0:T(1,128)} %get-tuple-element.237) | copy-start | bytes 24580
Sparse Core Ops, SparseCore 0:
  58.8 16.8 all-gather.3
  83.9 66.2 all-gather.5
  152.3 64.9 all-gather.7
  280.5 26.7 reduce-scatter.1
where the time goes:
time: 317 us; the launch traced here: 316 us
  waiting for transfers between devices  163 us (51%)
  blocking collectives  44.1 us (14%)
  local copies, waits for them, and re-layouts  38.4 us (12%)
  matrix products  38.1 us (12%)
  other arithmetic  17.9 us (6%)
  between operations  13.5 us (4%)
    all_gather x1, waiting for transfers between devices, local(): lax.all_gather(joined_values, 'sp', axis=0, tiled=True)  62.2 us
    all_gather x1, waiting for transfers between devices, local(): lax.all_gather(joined_keys, 'sp', axis=0, tiled=True)  60.5 us
    psum x1, blocking collectives, local(): summed_mod = lax.psum(partial_value, 'sp')  38.9 us
    reduce_scatter x1, waiting for transfers between devices, local(): lax.psum_scatter(jnp.dot(heads_out, out_weight, preferred_element_type=jn...  26.9 us
    dynamic_slice x8, local copies, waits for them, and re-layouts, absorb_block(): lax.dynamic_slice_in_dim(value_rows, block_index * block_rows, block_rows...  15 us
    all_gather x1, waiting for transfers between devices, local(): piece_rows = lax.all_gather(hidden, 'tp', axis=0, tiled=True)  13.2 us
    dot_general x5, matrix products, absorb(): jnp.einsum('mhqd,kmhd->mhqk', queries, key_block.reshape(row_count, 2, he...  12.7 us
    convert_element_type x5, other arithmetic, absorb(): weights.astype(jnp.bfloat16)  9.04 us
  transfers between devices with their start and end apart: 4, of which 4 were waited for; matrix products, arithmetic and copies ran while one was open for 4% of the time, Pallas kernels for 0%

commit v1 on v0

--- a/solution.py
+++ b/solution.py
@@ -1,16 +1,23 @@
+import functools
+import math
+
 import jax
 import jax.numpy as jnp
 from jax import lax
+from jax.experimental import pallas as pl
+from jax.experimental.pallas import tpu as pltpu
 from jax.sharding import PartitionSpec as P
+
 
 HEAD_DIM = 64
 GRID_W = 64
 VALUE_DIM = 128
-
+LANES = 128
 
 norm_eps = 1e-06
 rope_theta = 10000.0
 block_limit = 1024
+query_block = 256
 
 
 def rms_scale(matrix):
@@ -21,14 +28,20 @@
     return (rms_scale(activations.astype(jnp.float32)) * (1.0 + scale) + shift).astype(jnp.bfloat16)
 
 
-def rotate(vectors, positions, grid_width):
-    quarter = vectors.shape[-1] // 4
+def rope_tables(positions, grid_width, head_dim):
+    quarter = head_dim // 4
     inverse = rope_theta ** (-jnp.arange(quarter, dtype=jnp.float32) / quarter)
     grid_row = (positions // grid_width).astype(jnp.float32)
     grid_col = (positions % grid_width).astype(jnp.float32)
     angles = jnp.concatenate([grid_row[:, None] * inverse, grid_col[:, None] * inverse], axis=-1)
-    cos_table = jnp.cos(angles)[:, None, :]
-    sin_table = jnp.sin(angles)[:, None, :]
+    return jnp.cos(angles), jnp.sin(angles)
+
+
+def rotate(vectors, positions, grid_width):
+    quarter = vectors.shape[-1] // 4
+    cos_table, sin_table = rope_tables(positions, grid_width, vectors.shape[-1])
+    cos_table = cos_table[:, None, :]
+    sin_table = sin_table[:, None, :]
     former = vectors[..., : 2 * quarter]
     latter = vectors[..., 2 * quarter :]
     return jnp.concatenate(
@@ -79,7 +92,7 @@
     return lax.fori_loop(0, total_rows // block_rows, absorb_block, carry_state)
 
 
-def local(
+def local_general(
     latent,
     context,
     cond_latent,
@@ -134,13 +147,9 @@
     values = jnp.dot(piece_rows, value_weight, preferred_element_type=jnp.float32).astype(
         jnp.bfloat16
     )
-    projected = jnp.concatenate([rotated(query_weight), rotated(key_weight), values], axis=-1)
     key_width = 2 * head_count * HEAD_DIM
-    queries = (
-        projected[:, :key_width].reshape(tok_rows, 2, head_count, HEAD_DIM).transpose(1, 2, 0, 3)
-    )
-    latent_keys = projected[:, key_width : 2 * key_width]
-    latent_values = projected[:, 2 * key_width :]
+    queries = rotated(query_weight).reshape(tok_rows, 2, head_count, HEAD_DIM).transpose(1, 2, 0, 3)
+    latent_keys = rotated(key_weight)
     context_keys = jnp.concatenate(
         [
             jnp.dot(context_hidden, key_weight[0], preferred_element_type=jnp.float32),
@@ -151,7 +160,7 @@
     context_values = jnp.dot(
         context_hidden, value_weight, preferred_element_type=jnp.float32
     ).astype(jnp.bfloat16)
-    initial = (
+    state = (
         jnp.full((2, head_count, tok_rows), -jnp.inf, jnp.float32),
         jnp.zeros((2, head_count, tok_rows), jnp.float32),
         jnp.zeros((2, head_count, tok_rows, VALUE_DIM), jnp.float32),
@@ -159,19 +168,14 @@
     context_dev = context_keys.shape[0]
     shard_len = tok_rows + context_dev
     value_width = context_values.shape[1]
-    joined_keys = jnp.concatenate([latent_keys, context_keys], axis=0)
-    joined_values = jnp.concatenate([latent_values, context_values], axis=0)
     context_total = context_dev * lax.axis_size("sp")
-    pieces = (
-        lax.all_gather(joined_keys, "sp", axis=0, tiled=True),
-        lax.all_gather(joined_values, "sp", axis=0, tiled=True),
-    )
-    attention_state = initial
-    shard_count = pieces[0].shape[0] // shard_len
-    key_parts = pieces[0].reshape(shard_count, shard_len, key_width)
-    value_parts = pieces[1].reshape(shard_count, shard_len, value_width)
-    attention_state = absorb_all(
-        attention_state,
+    whole_keys = lax.all_gather(jnp.concatenate([latent_keys, context_keys], axis=0), "sp", axis=0, tiled=True)
+    whole_values = lax.all_gather(jnp.concatenate([values, context_values], axis=0), "sp", axis=0, tiled=True)
+    shard_count = whole_keys.shape[0] // shard_len
+    key_parts = whole_keys.reshape(shard_count, shard_len, key_width)
+    value_parts = whole_values.reshape(shard_count, shard_len, value_width)
+    state = absorb_all(
+        state,
         key_parts[:, :tok_rows].reshape(shard_count * tok_rows, key_width),
         value_parts[:, :tok_rows].reshape(shard_count * tok_rows, value_width),
         queries,
@@ -180,8 +184,7 @@
     )
     held_keys = key_parts[:, tok_rows:].reshape(shard_count * context_dev, key_width)
     held_values = value_parts[:, tok_rows:].reshape(shard_count * context_dev, value_width)
-    folded, held_keys, held_values = (attention_state, held_keys, held_values)
-    final = absorb_all(folded, held_keys, held_values, queries, head_count, context_total)
+    final = absorb_all(state, held_keys, held_values, queries, head_count, context_total)
     totals = final[1]
     numerator = final[2]
     mixed = numerator[0] / totals[0][..., None] - lambda_heads[:, None, None] * (
@@ -198,6 +201,328 @@
         tiled=True,
     ).astype(jnp.float32)
     return (latent.astype(jnp.float32) + whole_mod[4] * summed).astype(jnp.bfloat16)
+
+
+def query_slots_of(heads):
+    return (tuple(range(heads)),)
+
+
+def vmem(count):
+    return [pl.BlockSpec(memory_space=pltpu.VMEM)] * count
+
+
+SMEM = pl.BlockSpec(memory_space=pltpu.SMEM)
+
+
+def cost(flops, moved):
+    return pl.CostEstimate(flops=flops, bytes_accessed=moved, transcendentals=0)
+
+
+def params():
+    return pltpu.CompilerParams(vmem_limit_bytes=56 * 1024 * 1024)
+
+
+def modulation_kernel(lam, cond_latent, cond_context, shift_w, scale_w, gate_w, gain, out):
+    mod_rows = shift_w.shape[0]
+    sp = lax.axis_index("sp")
+    own = pl.ds(pl.multiple_of(sp * mod_rows, LANES), mod_rows)
+    rows = lax.broadcasted_iota(jnp.int32, (8, mod_rows), 0)
+    cond = jnp.where(rows == 0, cond_latent[:, own], cond_context[:, own])
+    cond = (cond / (1.0 + jnp.exp(-cond))).astype(jnp.bfloat16)
+    dot = functools.partial(jnp.dot, preferred_element_type=jnp.float32)
+    out[0:2, :] = dot(cond, shift_w[...])[0:2]
+    out[2:4, :] = dot(cond, scale_w[...])[0:2]
+    out[4:5, :] = dot(cond, gate_w[...])[0:1]
+    first = sp == 0
+    out[5:6, :] = jnp.where(first, gain[...], 0.0)
+    lane = lax.broadcasted_iota(jnp.int32, gain.shape, 1)
+    lam_row = jnp.zeros(gain.shape, jnp.float32)
+    for head in range(lam.shape[0]):
+        lam_row = jnp.where(lane == head, lam[head], lam_row)
+    out[6:7, :] = jnp.where(first, lam_row, 0.0)
+    out[7:8, :] = jnp.zeros_like(gain)
+
+
+def project_kernel(head_count, *refs):
+    slots = refs[0:4]
+    context, mods, cos_t, sin_t, query_w, key_w, value_w = refs[4:11]
+    outs = refs[11 : 11 + head_count]
+    hidden, ready = refs[11 + head_count :]
+    own_rows = slots[0].shape[0]
+    tok = 4 * own_rows
+    ctx = context.shape[0]
+    shift_l, shift_c = mods[0:1, :], mods[1:2, :]
+    scale_l, scale_c = 1.0 + mods[2:3, :], 1.0 + mods[3:4, :]
+
+    def modulate(block, scale, shift):
+        v = block.astype(jnp.float32)
+        r = lax.rsqrt(jnp.mean(v * v, axis=-1, keepdims=True) + norm_eps)
+        return (v * r * scale + shift).astype(jnp.bfloat16)
+
+    for index, slot in enumerate(slots):
+        hidden[index * own_rows : (index + 1) * own_rows, :] = modulate(slot[...], scale_l, shift_l)
+    hidden[tok:, :] = modulate(context[...], scale_c, shift_c)
+    dot = functools.partial(jnp.dot, preferred_element_type=jnp.float32)
+
+    def turned(tile):
+        lane = lax.broadcasted_iota(jnp.int32, tile.shape, 1)
+        swapped = jnp.where(
+            lane % HEAD_DIM < HEAD_DIM // 2,
+            pltpu.roll(tile, LANES - HEAD_DIM // 2, 1),
+            pltpu.roll(tile, HEAD_DIM // 2, 1),
+        )
+        return tile * cos_t[...] + swapped * sin_t[...]
+
+    def joined(first, second, odd):
+        lane = lax.broadcasted_iota(jnp.int32, first.shape, 1)
+        if odd:
+            return jnp.where(lane < HEAD_DIM, pltpu.roll(first, HEAD_DIM, 1), second)
+        return jnp.where(lane < HEAD_DIM, first, pltpu.roll(second, HEAD_DIM, 1))
+
+    per_tile = LANES // HEAD_DIM
+    for weight, base, count in ((query_w, 0, tok), (key_w, tok, tok + ctx)):
+        first = dot(hidden[:count, :], weight[0])
+        second = dot(hidden[:count, :], weight[1])
+        for head in range(head_count):
+            cols = slice(head // per_tile * LANES, (head // per_tile + 1) * LANES)
+            whole = joined(first[:, cols], second[:, cols], head % per_tile)
+            ready[head, base : base + tok, :] = turned(whole[:tok]).astype(jnp.bfloat16)
+            if count > tok:
+                ready[head, base + tok : base + count, :] = whole[tok:].astype(jnp.bfloat16)
+    base = 2 * tok + ctx
+    wide = 2 * VALUE_DIM
+    for pair in range(head_count // 2):
+        both = dot(hidden[...], value_w[:, pair * wide : (pair + 1) * wide]).astype(jnp.bfloat16)
+        ready[2 * pair, base:, :] = both[:, :VALUE_DIM]
+        ready[2 * pair + 1, base:, :] = both[:, VALUE_DIM:]
+    low = lax.axis_index("sp") % head_count
+    for k in range(head_count):
+        outs[k][...] = ready[low ^ k]
+
+
+def attention_kernel(head_count, tok, ctx, query_slots, *refs):
+    whole = refs[0:head_count]
+    swapped = refs[head_count : 2 * head_count]
+    mods = refs[2 * head_count]
+    outs = refs[2 * head_count + 1 : 2 * head_count + 1 + len(query_slots)]
+    queries, keys, values, results, scores_a, scores_b, top_a, top_b, weights = refs[
+        2 * head_count + 1 + len(query_slots) :
+    ]
+    part = tok + ctx
+    for index, k in enumerate(query_slots):
+        queries[index * tok : (index + 1) * tok, :] = whole[k][:tok, :]
+    for k in range(head_count):
+        for place_of, ref, base in ((k, whole[k], tok), (head_count + k, swapped[k], 0)):
+            rows = slice(place_of * part, (place_of + 1) * part)
+            keys[rows, :] = ref[base : base + part, :]
+            values[rows, :LANES] = ref[base + part : base + 2 * part, :]
+    ones = lax.broadcasted_iota(jnp.int32, (keys.shape[0], LANES), 1) == 0
+    values[:, LANES:] = ones.astype(jnp.float32).astype(jnp.bfloat16)
+    sp, tp = lax.axis_index("sp"), lax.axis_index("tp")
+    head = sp % head_count
+    owner = tp - tp % 2 + sp // head_count
+    width = head_count * VALUE_DIM
+    gain = mods[5:6, pl.ds(pl.multiple_of((owner * head_count + head) * VALUE_DIM, LANES), VALUE_DIM)]
+    lam_row = mods[6:7, pl.ds(pl.multiple_of(owner * width, LANES), LANES)]
+    lane_row = lax.broadcasted_iota(jnp.int32, lam_row.shape, 1)
+    lam = jnp.sum(jnp.where(lane_row == head, lam_row, 0.0), axis=-1, keepdims=True)
+    factor = HEAD_DIM ** (-0.5) * math.log2(math.e)
+    block = scores_a.shape[0] // 2
+    blocks = queries.shape[0] // block
+    lane = lax.broadcasted_iota(jnp.int32, (block, LANES), 1)
+    span = keys.shape[0]
+
+    def score(index, scores, top):
+        q = queries[pl.ds(pl.multiple_of(index * block, block), block), :]
+        zero = jnp.zeros_like(q)
+        both = jnp.concatenate(
+            [jnp.where(lane < HEAD_DIM, q, zero), jnp.where(lane < HEAD_DIM, zero, q)], axis=0
+        )
+        result = lax.dot_general(
+            both, keys[...], (((1,), (1,)), ((), ())), preferred_element_type=jnp.float32
+        )
+        scores[...] = result
+        running = result[:, :LANES]
+        for start in range(LANES, span, LANES):
+            running = jnp.maximum(running, result[:, start : start + LANES])
+        top[...] = jnp.broadcast_to(jnp.max(running, axis=-1, keepdims=True), top.shape)
+
+    def absorb_block(index, scores, top):
+        weights[...] = jnp.exp2((scores[...] - top[:, 0:1]) * factor).astype(jnp.bfloat16)
+        sums = jnp.dot(weights[...], values[...], preferred_element_type=jnp.float32)
+        share = sums[:, :LANES] / sums[:, LANES : LANES + 1]
+        mixed = share[:block] - lam * share[block:]
+        norm = lax.rsqrt(jnp.mean(mixed * mixed, axis=-1, keepdims=True) + norm_eps)
+        rows = pl.ds(pl.multiple_of(index * block, block), block)
+        results[rows, :] = (mixed * norm * gain).astype(jnp.bfloat16)
+
+    score(0, scores_a, top_a)
+
+    def step(pair, carry):
+        index = 2 * pair
+        score(jnp.minimum(index + 1, blocks - 1), scores_b, top_b)
+        absorb_block(index, scores_a, top_a)
+        score(jnp.minimum(index + 2, blocks - 1), scores_a, top_a)
+        absorb_block(jnp.minimum(index + 1, blocks - 1), scores_b, top_b)
+        return carry
+
+    lax.fori_loop(0, pl.cdiv(blocks, 2), step, 0)
+    for index in range(len(query_slots)):
+        outs[index][...] = results[index * tok : (index + 1) * tok, :]
+
+
+def output_kernel(*refs):
+    terms = refs[0:4]
+    weights = refs[4:8]
+    latent, mods, out = refs[8:11]
+    total = None
+    for term, weight in zip(terms, weights):
+        group = jnp.dot(term[...], weight[...], preferred_element_type=jnp.float32)
+        group = group.astype(jnp.bfloat16).astype(jnp.float32)
+        total = group if total is None else total + group
+    out[...] = (latent[...].astype(jnp.float32) + mods[4:5, :] * total).astype(jnp.bfloat16)
+
+
+def local_owner(
+    sp_size,
+    latent,
+    context,
+    cond_latent,
+    cond_context,
+    shift_weight,
+    scale_weight,
+    gate_weight,
+    query_weight,
+    key_weight,
+    value_weight,
+    out_weight,
+    lambda_heads,
+    out_gain,
+):
+    axes = ("sp", "tp")
+    tp_size = 4
+    heads = lambda_heads.shape[0]
+    own_rows, width = latent.shape
+    tok = tp_size * own_rows
+    ctx = context.shape[0]
+    f32, bf16 = jnp.float32, jnp.bfloat16
+    sp = lax.axis_index("sp")
+    tp = lax.axis_index("tp")
+    low = sp % heads
+
+    def hop(array, target):
+        pairs = []
+        for s in range(sp_size):
+            for t in range(tp_size):
+                s2, t2 = target(s, t)
+                pairs.append((s * tp_size + t, s2 * tp_size + t2))
+        return lax.ppermute(array, axes, pairs)
+
+    def across(array, bit):
+        return hop(array, lambda s, t: (s, t ^ bit))
+
+    def to_owner(k):
+        return lambda s, t: ((t % 2) * heads + ((s % heads) ^ k), t - t % 2 + s // heads)
+
+    mod_part = pl.pallas_call(
+        modulation_kernel,
+        out_shape=jax.ShapeDtypeStruct((8, shift_weight.shape[1]), f32),
+        in_specs=[SMEM] + vmem(6),
+        out_specs=vmem(1)[0],
+        compiler_params=params(),
+        cost_estimate=cost(10**9, 10**6),
+        name="modulation",
+    )(
+        lambda_heads,
+        cond_latent[None, :],
+        cond_context[None, :],
+        shift_weight,
+        scale_weight,
+        gate_weight,
+        out_gain[None, :],
+    )
+
+    lat_x = across(latent, 2)
+    lat_c = across(latent, 1)
+    step = 1
+    while step < sp_size:
+        mod_part = mod_part + hop(mod_part, lambda s, t, step=step: (s ^ step, t))
+        step *= 2
+    mods = lax.all_gather(mod_part, "tp", axis=1, tiled=True)
+    lat_xc = across(lat_x, 1)
+    slots = (latent, lat_x, lat_c, lat_xc)
+    slot_bits = (0, 2, 1, 3)
+
+    positions = jnp.concatenate(
+        [sp * tok + (tp ^ bit) * own_rows + jnp.arange(own_rows, dtype=jnp.int32) for bit in slot_bits]
+    )
+    cos_half, sin_half = rope_tables(positions, GRID_W, HEAD_DIM)
+    cos_t = jnp.concatenate([cos_half] * (2 * LANES // HEAD_DIM), axis=-1)
+    sin_t = jnp.concatenate([-sin_half, sin_half] * (LANES // HEAD_DIM), axis=-1)
+
+    part = tok + ctx
+    message = jax.ShapeDtypeStruct((tok + 2 * part, LANES), bf16)
+    messages = pl.pallas_call(
+        functools.partial(project_kernel, heads),
+        out_shape=[message] * heads,
+        in_specs=vmem(11),
+        out_specs=vmem(heads),
+        scratch_shapes=[
+            pltpu.VMEM((part, width), bf16),
+            pltpu.VMEM((heads,) + message.shape, bf16),
+        ],
+        compiler_params=params(),
+        cost_estimate=cost(2 * part * width * 6 * heads * HEAD_DIM, 8 * 10**6),
+        name="project",
+    )(*slots, context, mods, cos_t, sin_t, query_weight, key_weight, value_weight)
+
+    arrived = [hop(messages[k], to_owner(k)) for k in range(heads)]
+    swapped = [across(arrived[k][tok:], 1) for k in range(heads)]
+
+    results = []
+    for slots_of in query_slots_of(heads):
+        results += pl.pallas_call(
+            functools.partial(attention_kernel, heads, tok, ctx, slots_of),
+            out_shape=[jax.ShapeDtypeStruct((tok, LANES), bf16)] * len(slots_of),
+            in_specs=vmem(2 * heads + 1),
+            out_specs=vmem(len(slots_of)),
+            scratch_shapes=[
+                pltpu.VMEM((len(slots_of) * tok, LANES), bf16),
+                pltpu.VMEM((2 * heads * part, LANES), bf16),
+                pltpu.VMEM((2 * heads * part, 2 * LANES), bf16),
+                pltpu.VMEM((len(slots_of) * tok, LANES), bf16),
+                pltpu.VMEM((2 * query_block, 2 * heads * part), f32),
+                pltpu.VMEM((2 * query_block, 2 * heads * part), f32),
+                pltpu.VMEM((2 * query_block, LANES), f32),
+                pltpu.VMEM((2 * query_block, LANES), f32),
+                pltpu.VMEM((2 * query_block, 2 * heads * part), bf16),
+            ],
+            compiler_params=params(),
+            cost_estimate=cost(2 * 2 * len(slots_of) * tok * 2 * heads * part * 4 * LANES, 4 * 10**6),
+            name="attention",
+        )(*arrived, *swapped, mods)
+
+    back = [hop(results[k], to_owner(k)) for k in range(heads)]
+    stacked = jnp.stack(back)
+    ordered = jnp.concatenate(
+        [lax.dynamic_index_in_dim(stacked, low ^ m, 0, keepdims=False) for m in range(heads)], axis=1
+    )
+    pieces = [ordered[i * own_rows : (i + 1) * own_rows] for i in range(tp_size)]
+    terms = [pieces[0]] + [across(pieces[i], slot_bits[i]) for i in range(1, tp_size)]
+
+    late_weight, _ = lax.optimization_barrier((out_weight, mods))
+    weight_x = across(late_weight, 2)
+    weight_c = across(late_weight, 1)
+    weight_xc = across(weight_x, 1)
+    return pl.pallas_call(
+        output_kernel,
+        out_shape=jax.ShapeDtypeStruct(latent.shape, bf16),
+        in_specs=vmem(10),
+        out_specs=vmem(1)[0],
+        compiler_params=params(),
+        cost_estimate=cost(2 * own_rows * width * width, 8 * 10**6),
+        name="output",
+    )(*terms, out_weight, weight_x, weight_c, weight_xc, latent, mods)
 
 
 def solution(mesh):
@@ -216,6 +541,26 @@
         P("tp"),
         P("tp"),
     )
+    sp_size, tp_size = mesh.shape["sp"], mesh.shape["tp"]
+
+    def local(*args):
+        heads = args[11].shape[0]
+        own_rows = args[0].shape[0]
+        owner_plan = (
+            tp_size == 4
+            and sp_size == 2 * heads
+            and heads % 2 == 0
+            and heads & (heads - 1) == 0
+            and 2 * HEAD_DIM == LANES
+            and VALUE_DIM == LANES
+            and own_rows % 32 == 0
+            and (heads * tp_size * own_rows) % query_block == 0
+            and args[1].shape[0] % 16 == 0
+        )
+        if owner_plan:
+            return local_owner(sp_size, *args)
+        return local_general(*args)
+
     return jax.shard_map(
         local, mesh=mesh, in_specs=placed, out_specs=P(("sp", "tp"), None), check_vma=False
     )

time: 317 us -> 175 us (0.55)
  waiting for transfers between devices: 163 us -> 70.3 us
  starting transfers between devices: 0.31 us -> 58 us
  blocking collectives: 44.1 us -> 5.65 us
  matrix products: 38.1 us -> 0 us
  local copies, waits for them, and re-layouts: 38.4 us -> 3.29 us
  Pallas kernels: 0 us -> 34.1 us
  other arithmetic: 17.9 us -> 3.04 us
  between operations: 13.5 us -> 0.16 us
    all_gather x3 -> x0, waiting for transfers between devices: 136 us -> none  [the longest x1 62.2 us: local(): lax.all_gather(joined_values, 'sp', axis=0, tiled=True)]
    ppermute x0 -> x24, waiting for transfers between devices: none -> 70.3 us  [hop(): return lax.ppermute(array, axes, pairs)]
    ppermute x0 -> x24, starting transfers between devices: none -> 58 us  [hop(): return lax.ppermute(array, axes, pairs)]
    psum x1 -> x0, blocking collectives: 38.9 us -> none  [local(): summed_mod = lax.psum(partial_value, 'sp')]
    dot_general x22 -> x0, matrix products: 38.1 us -> none  [the longest x5 12.7 us: absorb(): jnp.einsum('mhqd,kmhd->mhqk', queries, key_block.reshape(row_count, 2, he...]
    pallas_call x0 -> x4, Pallas kernels: none -> 34.1 us  [the longest x1 18.2 us: local_owner(): pl.pallas_call(functools.partial(attention_kernel, heads, tok, ctx, slots...]
    reduce_scatter x1 -> x0, waiting for transfers between devices: 26.9 us -> none  [local(): lax.psum_scatter(jnp.dot(heads_out, out_weight, preferred_element_type=jn...]
    dynamic_slice x12 -> x0, local copies, waits for them, and re-layouts: 19.8 us -> none  [the longest x8 15 us: absorb_block(): lax.dynamic_slice_in_dim(value_rows, block_index * block_rows, block_rows...]
  transfers between devices with their start and end apart: 4 -> 24, of which waited for: 4 -> 9; matrix products, arithmetic and copies ran while one was open for 4% -> 2% of each run, Pallas kernels for 0% -> 15%
where the time goes in v1:
time: 175 us
  waiting for transfers between devices  70.3 us (40%)
  starting transfers between devices  58 us (33%)
  Pallas kernels  34.1 us (19%)
  blocking collectives  5.65 us (3%)
  local copies, waits for them, and re-layouts  3.29 us (2%)
  other arithmetic  3.04 us (2%)
    ppermute x24, waiting for transfers between devices, hop(): return lax.ppermute(array, axes, pairs)  70.3 us
    ppermute x24, starting transfers between devices, hop(): return lax.ppermute(array, axes, pairs)  58 us
    pallas_call x1, Pallas kernels, local_owner(): pl.pallas_call(functools.partial(attention_kernel, heads, tok, ctx, slots...  18.2 us
    pallas_call x1, Pallas kernels, local_owner(): pl.pallas_call(functools.partial(project_kernel, heads), out_shape=[messa...  7.84 us
    pallas_call x1, Pallas kernels, local_owner(): pl.pallas_call(output_kernel, out_shape=jax.ShapeDtypeStruct(latent.shape...  5.89 us
    all_gather x1, blocking collectives, local_owner(): mods = lax.all_gather(mod_part, 'tp', axis=1, tiled=True)  5.65 us
  transfers between devices with their start and end apart: 24, of which 9 were waited for; matrix products, arithmetic and copies ran while one was open for 2% of the time, Pallas kernels for 15%

profile of v1, /device:TPU:0, one launch (start us, length us, event | category | flops | bytes accessed | tf_op | source)
XLA Modules:
  0.0 174.6 jit_solution(9458917101450545359)
XLA Ops:
  0.0 2.1 %modulation.1 = f32[8,512]{1,0:T(8,128)} custom-call(f32[4]{0:T(128)} %lam.1, f32[1,2048]{1,0:T(1,128)} %bitcast.19, f32[1,2048]{1,0:T(1,128)} %bitcast.20, bf16[256,512]{1,0:T(8,128)(2,1)} %shift_w.1, bf16[256,512]{1,0:T(8,128)(2,1)} %scale_w.1, bf16[256,512]{1,0:T(8,128)(2,1)} %gate_w.1, f32[1,512]{1,0:T(1,128)} %bitcast.21), custom_call_target="tpu_custom_call" | custom-call | flops 1000000000 | bytes 1000000 | tf_op jit(solution)/shard_map/modulation/pallas_call | solution.py:427
  2.1 3.0 %collective-permute-start.3 = (f32[8,512]{1,0:T(8,128)}, f32[8,512]{1,0:T(8,128)S(1)}, u32[]{:S(2)}, u32[]{:S(2)}) collective-permute-start(f32[8,512]{1,0:T(8,128)} %modulation.1), channel_id=1, source_target_pairs={{0,4},{1,5},{2,6},{3,7},{4,0},{5,1},{6,2},{7,3},{8,12},{9,13},{10,... | collective-permute-start | bytes 49160 | tf_op jit(solution)/shard_map/ppermute | solution.py:419
  5.1 1.9 %collective-permute-done.3 = f32[8,512]{1,0:T(8,128)S(1)} collective-permute-done((f32[8,512]{1,0:T(8,128)}, f32[8,512]{1,0:T(8,128)S(1)}, u32[]{:S(2)}, u32[]{:S(2)}) %collective-permute-start.3) | collective-permute-done | bytes 16416 | tf_op jit(solution)/shard_map/ppermute | solution.py:419
  7.1 0.7 add.109
  7.8 2.1 %collective-permute-start.4 = (f32[8,512]{1,0:T(8,128)S(1)}, f32[8,512]{1,0:T(8,128)S(1)}, u32[]{:S(2)}, u32[]{:S(2)}) collective-permute-start(f32[8,512]{1,0:T(8,128)S(1)} %add.109), channel_id=1, source_target_pairs={{0,8},{1,9},{2,10},{3,11},{4,12},{5,13},{6,14},{7,15},{8,0},{9,1},... | collective-permute-start | bytes 49160 | tf_op jit(solution)/shard_map/ppermute | solution.py:419
  9.9 1.7 collective-permute-done.4
  11.6 3.0 %collective-permute-start.5 = (f32[8,512]{1,0:T(8,128)S(1)}, f32[8,512]{1,0:T(8,128)S(1)}, u32[]{:S(2)}, u32[]{:S(2)}) collective-permute-start(f32[8,512]{1,0:T(8,128)S(1)} %add.110), channel_id=1, source_target_pairs={{0,16},{1,17},{2,18},{3,19},{4,20},{5,21},{6,22},{7,23},{8,24},{9,... | collective-permute-start | bytes 49160 | tf_op jit(solution)/shard_map/ppermute | solution.py:419
  14.6 1.7 collective-permute-done.5
  16.3 5.6 %all_gather.3.refs_5_.refs_8_.refs_9_ = f32[8,2048]{1,0:T(8,128)} all-gather(f32[8,512]{1,0:T(8,128)S(1)} %add.111), channel_id=1, replica_groups=mesh['sp'=8,'tp'=4] {'tp'}, dimensions={1}, use_global_device_ids=true | all-gather | bytes 81920 | tf_op jit(solution)/shard_map/all_gather | solution.py:451
  22.0 1.8 %collective-permute-start.21 = (bf16[512,2048]{1,0:T(8,128)(2,1)S(1)}, bf16[512,2048]{1,0:T(8,128)(2,1)}, u32[]{:S(2)}, u32[]{:S(2)}) collective-permute-start(bf16[512,2048]{1,0:T(8,128)(2,1)S(1)} %copy-done), channel_id=1, source_target_pairs={{0,2},{1,3},{2,0},{3,1},{4,6},{5,7},{6,4},{7,5},{8,10},{9,11},{10,... | collective-permute-start | bytes 6291464 | tf_op jit(solution)/shard_map/ppermute | solution.py:419
  23.9 0.4 collective-permute-start
  24.3 0.1 fusion.2
  24.4 54.1 %collective-permute-done.refs_1_ = bf16[96,2048]{1,0:T(8,128)(2,1)} collective-permute-done((bf16[96,2048]{1,0:T(8,128)(2,1)S(1)}, bf16[96,2048]{1,0:T(8,128)(2,1)}, u32[]{:S(2)}, u32[]{:S(2)}) %collective-permute-start) | collective-permute-done | bytes 393248 | tf_op jit(solution)/shard_map/ppermute | solution.py:419
  78.5 0.1 broadcast_multiply_fusion.1
  78.6 0.2 fusion
  78.8 0.1 copy.20
  78.9 0.1 copy.16
  79.1 0.9 pad_maximum_fusion.3.refs_7_
  80.0 0.9 pad_maximum_fusion.2.refs_6_
  80.9 0.7 copy-done.9
  81.6 7.8 %project.1 = (bf16[1280,128]{1,0:T(8,128)(2,1)}, bf16[1280,128]{1,0:T(8,128)(2,1)}, bf16[1280,128]{1,0:T(8,128)(2,1)}, bf16[1280,128]{1,0:T(8,128)(2,1)}) custom-call(bf16[96,2048]{1,0:T(8,128)(2,1)} %refs_8_.3, bf16[96,2048]{1,0:T(8,128)(2,1)} %collective-permute-done.refs_1_, bf16[96,2048]{1,0:T(8,128)(2,1)} %copy-done.9, ...), custom_call_target="tpu_custom_call" | custom-call | flops 2818572288 | bytes 8000000 | tf_op jit(solution)/shard_map/project/pallas_call | solution.py:465
  89.5 1.6 collective-permute-start.6
  91.1 1.8 %collective-permute-start.7 = (bf16[1280,128]{1,0:T(8,128)(2,1)}, bf16[1280,128]{1,0:T(8,128)(2,1)S(1)}, u32[]{:S(2)}, u32[]{:S(2)}) collective-permute-start(bf16[1280,128]{1,0:T(8,128)(2,1)} %get-tuple-element.15), channel_id=1, source_target_pairs={{0,4},{1,20},{2,6},{3,22},{4,0},{5,16},{6,2},{7,18},{8,12},{9,28},... | collective-permute-start | bytes 983048 | tf_op jit(solution)/shard_map/ppermute | solution.py:419
  92.9 1.6 collective-permute-start.8
  94.4 0.1 collective-permute-start.9
  94.6 7.7 %collective-permute-start.10 = (bf16[896,128]{1,0:T(8,128)(2,1)S(1)}, bf16[896,128]{1,0:T(8,128)(2,1)S(1)}, u32[]{:S(2)}, u32[]{:S(2)}) collective-permute-start(bf16[896,128]{1,0:T(8,128)(2,1)S(1)} %slice.32), channel_id=1, source_target_pairs={{0,1},{1,0},{2,3},{3,2},{4,5},{5,4},{6,7},{7,6},{8,9},{9,8},{10,11... | collective-permute-start | bytes 688136 | tf_op jit(solution)/shard_map/ppermute | solution.py:419
  102.4 8.0 %collective-permute-start.11 = (bf16[896,128]{1,0:T(8,128)(2,1)S(1)}, bf16[896,128]{1,0:T(8,128)(2,1)S(1)}, u32[]{:S(2)}, u32[]{:S(2)}) collective-permute-start(bf16[896,128]{1,0:T(8,128)(2,1)S(1)} %slice.33), channel_id=1, source_target_pairs={{0,1},{1,0},{2,3},{3,2},{4,5},{5,4},{6,7},{7,6},{8,9},{9,8},{10,11... | collective-permute-start | bytes 688136 | tf_op jit(solution)/shard_map/ppermute | solution.py:419
  110.4 4.5 %collective-permute-start.12 = (bf16[896,128]{1,0:T(8,128)(2,1)S(1)}, bf16[896,128]{1,0:T(8,128)(2,1)S(1)}, u32[]{:S(2)}, u32[]{:S(2)}) collective-permute-start(bf16[896,128]{1,0:T(8,128)(2,1)S(1)} %slice.34), channel_id=1, source_target_pairs={{0,1},{1,0},{2,3},{3,2},{4,5},{5,4},{6,7},{7,6},{8,9},{9,8},{10,11... | collective-permute-start | bytes 688136 | tf_op jit(solution)/shard_map/ppermute | solution.py:419
  114.9 4.1 %collective-permute-start.13 = (bf16[896,128]{1,0:T(8,128)(2,1)S(1)}, bf16[896,128]{1,0:T(8,128)(2,1)S(1)}, u32[]{:S(2)}, u32[]{:S(2)}) collective-permute-start(bf16[896,128]{1,0:T(8,128)(2,1)S(1)} %slice.35), channel_id=1, source_target_pairs={{0,1},{1,0},{2,3},{3,2},{4,5},{5,4},{6,7},{7,6},{8,9},{9,8},{10,11... | collective-permute-start | bytes 688136 | tf_op jit(solution)/shard_map/ppermute | solution.py:419
  118.9 0.1 collective-permute-start.22
  119.0 0.4 collective-permute-start.23
  119.5 0.6 collective-permute-done.13.refs_7_
  120.1 0.1 copy-done.11
  120.3 0.7 copy-done.13
  121.0 18.2 %attention.1 = (bf16[384,128]{1,0:T(8,128)(2,1)}, bf16[384,128]{1,0:T(8,128)(2,1)}, bf16[384,128]{1,0:T(8,128)(2,1)}, bf16[384,128]{1,0:T(8,128)(2,1)}) custom-call(bf16[1280,128]{1,0:T(8,128)(2,1)} %copy-done.2, bf16[1280,128]{1,0:T(8,128)(2,1)} %copy-done.3, bf16[1280,128]{1,0:T(8,128)(2,1)} %copy-done.4, bf16[1280,128]{1,0:T(8,128)(2,1)} %copy-done.5, ...), custom_call_target="tpu_custom_call" | custom-call | flops 11274289152 | bytes 4000000 | tf_op jit(solution)/shard_map/attention/pallas_call | solution.py:484
  139.2 1.5 collective-permute-start.14
  140.8 0.9 collective-permute-start.15
  141.6 6.5 %collective-permute-start.16 = (bf16[384,128]{1,0:T(8,128)(2,1)}, bf16[384,128]{1,0:T(8,128)(2,1)S(1)}, u32[]{:S(2)}, u32[]{:S(2)}) collective-permute-start(bf16[384,128]{1,0:T(8,128)(2,1)} %get-tuple-element.20), channel_id=1, source_target_pairs={{0,8},{1,24},{2,10},{3,26},{4,12},{5,28},{6,14},{7,30},{8,0},{9,16... | collective-permute-start | bytes 294920 | tf_op jit(solution)/shard_map/ppermute | solution.py:419
  148.2 1.0 collective-permute-start.17
  149.2 1.8 %collective-permute-done.16 = bf16[384,128]{1,0:T(8,128)(2,1)S(1)} collective-permute-done((bf16[384,128]{1,0:T(8,128)(2,1)}, bf16[384,128]{1,0:T(8,128)(2,1)S(1)}, u32[]{:S(2)}, u32[]{:S(2)}) %collective-permute-start.16) | collective-permute-done | bytes 98336 | tf_op jit(solution)/shard_map/ppermute | solution.py:419
  151.0 3.5 %collective-permute-done.17 = bf16[384,128]{1,0:T(8,128)(2,1)S(1)} collective-permute-done((bf16[384,128]{1,0:T(8,128)(2,1)}, bf16[384,128]{1,0:T(8,128)(2,1)S(1)}, u32[]{:S(2)}, u32[]{:S(2)}) %collective-permute-start.17) | collective-permute-done | bytes 98336 | tf_op jit(solution)/shard_map/ppermute | solution.py:419
  154.7 0.7 fusion.5
  155.3 7.3 %collective-permute-start.20 = (bf16[96,512]{1,0:T(8,128)(2,1)S(1)}, bf16[96,512]{1,0:T(8,128)(2,1)S(1)}, u32[]{:S(2)}, u32[]{:S(2)}) collective-permute-start(bf16[96,512]{1,0:T(8,128)(2,1)S(1)} %get-tuple-element.23), channel_id=1, source_target_pairs={{0,3},{1,2},{2,1},{3,0},{4,7},{5,6},{6,5},{7,4},{8,11},{9,10},{10,... | collective-permute-start | bytes 294920 | tf_op jit(solution)/shard_map/ppermute | solution.py:419
  162.6 0.5 collective-permute-start.18
  163.1 2.6 %collective-permute-done.20.refs_3_ = bf16[96,512]{1,0:T(8,128)(2,1)S(1)} collective-permute-done((bf16[96,512]{1,0:T(8,128)(2,1)S(1)}, bf16[96,512]{1,0:T(8,128)(2,1)S(1)}, u32[]{:S(2)}, u32[]{:S(2)}) %collective-permute-start.20) | collective-permute-done | bytes 98336 | tf_op jit(solution)/shard_map/ppermute | solution.py:419
  165.7 2.3 %collective-permute-done.18.refs_1_ = bf16[96,512]{1,0:T(8,128)(2,1)S(1)} collective-permute-done((bf16[96,512]{1,0:T(8,128)(2,1)S(1)}, bf16[96,512]{1,0:T(8,128)(2,1)S(1)}, u32[]{:S(2)}, u32[]{:S(2)}) %collective-permute-start.18) | collective-permute-done | bytes 98336 | tf_op jit(solution)/shard_map/ppermute | solution.py:419
  168.1 0.6 copy-done.8
  168.7 5.9 %output.1 = bf16[96,2048]{1,0:T(8,128)(2,1)} custom-call(bf16[96,512]{1,0:T(8,128)(2,1)} %get-tuple-element.26.refs_0_, bf16[96,512]{1,0:T(8,128)(2,1)} %copy-done.8, bf16[96,512]{1,0:T(8,128)(2,1)} %copy-done.7, bf16[96,512]{1,0:T(8,128)(2,1)} %copy-done.6, bf16[512,2048]{1,0:T(8,128)(2,1)} %refs_4_.3, bf16[512,2048]{1,0:T(8,128)(2,1)} %collective-permute-done.21.refs_5_, ...), custom_call_target="tpu_custom_call" | custom-call | flops 805306368 | bytes 8000000 | tf_op jit(solution)/shard_map/output/pallas_call | solution.py:517
  (55 shorter events, 0.5 us)
Async XLA Ops:
  0.0 22.0 %copy-start = (bf16[512,2048]{1,0:T(8,128)(2,1)S(1)}, bf16[512,2048]{1,0:T(8,128)(2,1)}, u32[]{:S(2)}) copy-start(bf16[512,2048]{1,0:T(8,128)(2,1)} %refs_4_.3) | copy-start | bytes 6291460
  0.0 23.8 %copy-start.1 = (bf16[96,2048]{1,0:T(8,128)(2,1)S(1)}, bf16[96,2048]{1,0:T(8,128)(2,1)}, u32[]{:S(2)}) copy-start(bf16[96,2048]{1,0:T(8,128)(2,1)} %refs_8_.3) | copy-start | bytes 1179652
  2.1 4.9 %collective-permute-start.3 = (f32[8,512]{1,0:T(8,128)}, f32[8,512]{1,0:T(8,128)S(1)}, u32[]{:S(2)}, u32[]{:S(2)}) collective-permute-start(f32[8,512]{1,0:T(8,128)} %modulation.1), channel_id=1, source_target_pairs={{0,4},{1,5},{2,6},{3,7},{4,0},{5,1},{6,2},{7,3},{8,12},{9,13},{10,... | collective-permute-start | bytes 49160 | tf_op jit(solution)/shard_map/ppermute | solution.py:419
  7.8 3.8 %collective-permute-start.4 = (f32[8,512]{1,0:T(8,128)S(1)}, f32[8,512]{1,0:T(8,128)S(1)}, u32[]{:S(2)}, u32[]{:S(2)}) collective-permute-start(f32[8,512]{1,0:T(8,128)S(1)} %add.109), channel_id=1, source_target_pairs={{0,8},{1,9},{2,10},{3,11},{4,12},{5,13},{6,14},{7,15},{8,0},{9,1},... | collective-permute-start | bytes 49160 | tf_op jit(solution)/shard_map/ppermute | solution.py:419
  11.6 4.8 %collective-permute-start.5 = (f32[8,512]{1,0:T(8,128)S(1)}, f32[8,512]{1,0:T(8,128)S(1)}, u32[]{:S(2)}, u32[]{:S(2)}) collective-permute-start(f32[8,512]{1,0:T(8,128)S(1)} %add.110), channel_id=1, source_target_pairs={{0,16},{1,17},{2,18},{3,19},{4,20},{5,21},{6,22},{7,23},{8,24},{9,... | collective-permute-start | bytes 49160 | tf_op jit(solution)/shard_map/ppermute | solution.py:419
  22.0 97.1 %collective-permute-start.21 = (bf16[512,2048]{1,0:T(8,128)(2,1)S(1)}, bf16[512,2048]{1,0:T(8,128)(2,1)}, u32[]{:S(2)}, u32[]{:S(2)}) collective-permute-start(bf16[512,2048]{1,0:T(8,128)(2,1)S(1)} %copy-done), channel_id=1, source_target_pairs={{0,2},{1,3},{2,0},{3,1},{4,6},{5,7},{6,4},{7,5},{8,10},{9,11},{10,... | collective-permute-start | bytes 6291464 | tf_op jit(solution)/shard_map/ppermute | solution.py:419
  23.8 57.0 %collective-permute-start.1 = (bf16[96,2048]{1,0:T(8,128)(2,1)S(1)}, bf16[96,2048]{1,0:T(8,128)(2,1)S(1)}, u32[]{:S(2)}, u32[]{:S(2)}) collective-permute-start(bf16[96,2048]{1,0:T(8,128)(2,1)S(1)} %copy-done.1), channel_id=1, source_target_pairs={{0,1},{1,0},{2,3},{3,2},{4,5},{5,4},{6,7},{7,6},{8,9},{9,8},{10,11... | collective-permute-start | bytes 1179656 | tf_op jit(solution)/shard_map/ppermute | solution.py:419
  23.9 54.6 %collective-permute-start = (bf16[96,2048]{1,0:T(8,128)(2,1)S(1)}, bf16[96,2048]{1,0:T(8,128)(2,1)}, u32[]{:S(2)}, u32[]{:S(2)}) collective-permute-start(bf16[96,2048]{1,0:T(8,128)(2,1)S(1)} %copy-done.1), channel_id=1, source_target_pairs={{0,2},{1,3},{2,0},{3,1},{4,6},{5,7},{6,4},{7,5},{8,10},{9,11},{10,... | collective-permute-start | bytes 1179656 | tf_op jit(solution)/shard_map/ppermute | solution.py:419
  78.5 2.4 %collective-permute-start.2 = (bf16[96,2048]{1,0:T(8,128)(2,1)}, bf16[96,2048]{1,0:T(8,128)(2,1)}, u32[]{:S(2)}, u32[]{:S(2)}) collective-permute-start(bf16[96,2048]{1,0:T(8,128)(2,1)} %collective-permute-done.refs_1_), channel_id=1, source_target_pairs={{0,1},{1,0},{2,3},{3,2},{4,5},{5,4},{6,7},{7,6},{8,9},{9,8},{10,11... | collective-permute-start | bytes 1179656 | tf_op jit(solution)/shard_map/ppermute | solution.py:419
  80.9 0.7 copy-start.9
  89.5 5.1 %collective-permute-start.6 = (bf16[1280,128]{1,0:T(8,128)(2,1)}, bf16[1280,128]{1,0:T(8,128)(2,1)S(1)}, u32[]{:S(2)}, u32[]{:S(2)}) collective-permute-start(bf16[1280,128]{1,0:T(8,128)(2,1)} %get-tuple-element.14), channel_id=1, source_target_pairs={{0,0},{1,16},{2,2},{3,18},{4,4},{5,20},{6,6},{7,22},{8,8},{9,24},{... | collective-permute-start | bytes 983048 | tf_op jit(solution)/shard_map/ppermute | solution.py:419
  91.1 11.2 %collective-permute-start.7 = (bf16[1280,128]{1,0:T(8,128)(2,1)}, bf16[1280,128]{1,0:T(8,128)(2,1)S(1)}, u32[]{:S(2)}, u32[]{:S(2)}) collective-permute-start(bf16[1280,128]{1,0:T(8,128)(2,1)} %get-tuple-element.15), channel_id=1, source_target_pairs={{0,4},{1,20},{2,6},{3,22},{4,0},{5,16},{6,2},{7,18},{8,12},{9,28},... | collective-permute-start | bytes 983048 | tf_op jit(solution)/shard_map/ppermute | solution.py:419
  92.9 17.5 %collective-permute-start.8 = (bf16[1280,128]{1,0:T(8,128)(2,1)}, bf16[1280,128]{1,0:T(8,128)(2,1)S(1)}, u32[]{:S(2)}, u32[]{:S(2)}) collective-permute-start(bf16[1280,128]{1,0:T(8,128)(2,1)} %get-tuple-element.16), channel_id=1, source_target_pairs={{0,8},{1,24},{2,10},{3,26},{4,12},{5,28},{6,14},{7,30},{8,0},{9,16... | collective-permute-start | bytes 983048 | tf_op jit(solution)/shard_map/ppermute | solution.py:419
  94.4 20.4 %collective-permute-start.9 = (bf16[1280,128]{1,0:T(8,128)(2,1)}, bf16[1280,128]{1,0:T(8,128)(2,1)S(1)}, u32[]{:S(2)}, u32[]{:S(2)}) collective-permute-start(bf16[1280,128]{1,0:T(8,128)(2,1)} %get-tuple-element.17), channel_id=1, source_target_pairs={{0,12},{1,28},{2,14},{3,30},{4,8},{5,24},{6,10},{7,26},{8,4},{9,20... | collective-permute-start | bytes 983048 | tf_op jit(solution)/shard_map/ppermute | solution.py:419
  94.6 25.5 %copy-start.2 = (bf16[1280,128]{1,0:T(8,128)(2,1)}, bf16[1280,128]{1,0:T(8,128)(2,1)S(1)}, u32[]{:S(2)}) copy-start(bf16[1280,128]{1,0:T(8,128)(2,1)S(1)} %collective-permute-done.6.refs_0_) | copy-start | bytes 983044
  94.6 24.3 %collective-permute-start.10 = (bf16[896,128]{1,0:T(8,128)(2,1)S(1)}, bf16[896,128]{1,0:T(8,128)(2,1)S(1)}, u32[]{:S(2)}, u32[]{:S(2)}) collective-permute-start(bf16[896,128]{1,0:T(8,128)(2,1)S(1)} %slice.32), channel_id=1, source_target_pairs={{0,1},{1,0},{2,3},{3,2},{4,5},{5,4},{6,7},{7,6},{8,9},{9,8},{10,11... | collective-permute-start | bytes 688136 | tf_op jit(solution)/shard_map/ppermute | solution.py:419
  102.3 17.7 %copy-start.3 = (bf16[1280,128]{1,0:T(8,128)(2,1)}, bf16[1280,128]{1,0:T(8,128)(2,1)S(1)}, u32[]{:S(2)}) copy-start(bf16[1280,128]{1,0:T(8,128)(2,1)S(1)} %collective-permute-done.7.refs_1_) | copy-start | bytes 983044
  102.4 17.1 %collective-permute-start.11 = (bf16[896,128]{1,0:T(8,128)(2,1)S(1)}, bf16[896,128]{1,0:T(8,128)(2,1)S(1)}, u32[]{:S(2)}, u32[]{:S(2)}) collective-permute-start(bf16[896,128]{1,0:T(8,128)(2,1)S(1)} %slice.33), channel_id=1, source_target_pairs={{0,1},{1,0},{2,3},{3,2},{4,5},{5,4},{6,7},{7,6},{8,9},{9,8},{10,11... | collective-permute-start | bytes 688136 | tf_op jit(solution)/shard_map/ppermute | solution.py:419
  110.4 9.7 %copy-start.4 = (bf16[1280,128]{1,0:T(8,128)(2,1)}, bf16[1280,128]{1,0:T(8,128)(2,1)S(1)}, u32[]{:S(2)}) copy-start(bf16[1280,128]{1,0:T(8,128)(2,1)S(1)} %collective-permute-done.8.refs_2_) | copy-start | bytes 983044
  110.4 9.1 %collective-permute-start.12 = (bf16[896,128]{1,0:T(8,128)(2,1)S(1)}, bf16[896,128]{1,0:T(8,128)(2,1)S(1)}, u32[]{:S(2)}, u32[]{:S(2)}) collective-permute-start(bf16[896,128]{1,0:T(8,128)(2,1)S(1)} %slice.34), channel_id=1, source_target_pairs={{0,1},{1,0},{2,3},{3,2},{4,5},{5,4},{6,7},{7,6},{8,9},{9,8},{10,11... | collective-permute-start | bytes 688136 | tf_op jit(solution)/shard_map/ppermute | solution.py:419
  114.9 5.2 %copy-start.5 = (bf16[1280,128]{1,0:T(8,128)(2,1)}, bf16[1280,128]{1,0:T(8,128)(2,1)S(1)}, u32[]{:S(2)}) copy-start(bf16[1280,128]{1,0:T(8,128)(2,1)S(1)} %collective-permute-done.9.refs_3_) | copy-start | bytes 983044
  114.9 5.2 %collective-permute-start.13 = (bf16[896,128]{1,0:T(8,128)(2,1)S(1)}, bf16[896,128]{1,0:T(8,128)(2,1)S(1)}, u32[]{:S(2)}, u32[]{:S(2)}) collective-permute-start(bf16[896,128]{1,0:T(8,128)(2,1)S(1)} %slice.35), channel_id=1, source_target_pairs={{0,1},{1,0},{2,3},{3,2},{4,5},{5,4},{6,7},{7,6},{8,9},{9,8},{10,11... | collective-permute-start | bytes 688136 | tf_op jit(solution)/shard_map/ppermute | solution.py:419
  118.9 1.1 copy-start.10
  118.9 49.1 %collective-permute-start.22 = (bf16[512,2048]{1,0:T(8,128)(2,1)S(1)}, bf16[512,2048]{1,0:T(8,128)(2,1)}, u32[]{:S(2)}, u32[]{:S(2)}) collective-permute-start(bf16[512,2048]{1,0:T(8,128)(2,1)S(1)} %copy-done), channel_id=1, source_target_pairs={{0,1},{1,0},{2,3},{3,2},{4,5},{5,4},{6,7},{7,6},{8,9},{9,8},{10,11... | collective-permute-start | bytes 6291464 | tf_op jit(solution)/shard_map/ppermute | solution.py:419
  119.0 49.0 %collective-permute-start.23 = (bf16[512,2048]{1,0:T(8,128)(2,1)}, bf16[512,2048]{1,0:T(8,128)(2,1)}, u32[]{:S(2)}, u32[]{:S(2)}) collective-permute-start(bf16[512,2048]{1,0:T(8,128)(2,1)} %collective-permute-done.21.refs_5_), channel_id=1, source_target_pairs={{0,1},{1,0},{2,3},{3,2},{4,5},{5,4},{6,7},{7,6},{8,9},{9,8},{10,11... | collective-permute-start | bytes 6291464 | tf_op jit(solution)/shard_map/ppermute | solution.py:419
  119.5 0.7 copy-start.11
  119.5 0.8 copy-start.12
  120.3 0.7 copy-start.13
  139.2 9.0 %collective-permute-start.14 = (bf16[384,128]{1,0:T(8,128)(2,1)}, bf16[384,128]{1,0:T(8,128)(2,1)S(1)}, u32[]{:S(2)}, u32[]{:S(2)}) collective-permute-start(bf16[384,128]{1,0:T(8,128)(2,1)} %get-tuple-element.18), channel_id=1, source_target_pairs={{0,0},{1,16},{2,2},{3,18},{4,4},{5,20},{6,6},{7,22},{8,8},{9,24},{... | collective-permute-start | bytes 294920 | tf_op jit(solution)/shard_map/ppermute | solution.py:419
  140.8 8.5 %collective-permute-start.15 = (bf16[384,128]{1,0:T(8,128)(2,1)}, bf16[384,128]{1,0:T(8,128)(2,1)S(1)}, u32[]{:S(2)}, u32[]{:S(2)}) collective-permute-start(bf16[384,128]{1,0:T(8,128)(2,1)} %get-tuple-element.19), channel_id=1, source_target_pairs={{0,4},{1,20},{2,6},{3,22},{4,0},{5,16},{6,2},{7,18},{8,12},{9,28},... | collective-permute-start | bytes 294920 | tf_op jit(solution)/shard_map/ppermute | solution.py:419
  141.6 9.3 %collective-permute-start.16 = (bf16[384,128]{1,0:T(8,128)(2,1)}, bf16[384,128]{1,0:T(8,128)(2,1)S(1)}, u32[]{:S(2)}, u32[]{:S(2)}) collective-permute-start(bf16[384,128]{1,0:T(8,128)(2,1)} %get-tuple-element.20), channel_id=1, source_target_pairs={{0,8},{1,24},{2,10},{3,26},{4,12},{5,28},{6,14},{7,30},{8,0},{9,16... | collective-permute-start | bytes 294920 | tf_op jit(solution)/shard_map/ppermute | solution.py:419
  148.2 6.3 %collective-permute-start.17 = (bf16[384,128]{1,0:T(8,128)(2,1)}, bf16[384,128]{1,0:T(8,128)(2,1)S(1)}, u32[]{:S(2)}, u32[]{:S(2)}) collective-permute-start(bf16[384,128]{1,0:T(8,128)(2,1)} %get-tuple-element.21), channel_id=1, source_target_pairs={{0,12},{1,28},{2,14},{3,30},{4,8},{5,24},{6,10},{7,26},{8,4},{9,20... | collective-permute-start | bytes 294920 | tf_op jit(solution)/shard_map/ppermute | solution.py:419
  155.3 10.4 %collective-permute-start.20 = (bf16[96,512]{1,0:T(8,128)(2,1)S(1)}, bf16[96,512]{1,0:T(8,128)(2,1)S(1)}, u32[]{:S(2)}, u32[]{:S(2)}) collective-permute-start(bf16[96,512]{1,0:T(8,128)(2,1)S(1)} %get-tuple-element.23), channel_id=1, source_target_pairs={{0,3},{1,2},{2,1},{3,0},{4,7},{5,6},{6,5},{7,4},{8,11},{9,10},{10,... | collective-permute-start | bytes 294920 | tf_op jit(solution)/shard_map/ppermute | solution.py:419
  162.6 3.1 %collective-permute-start.19 = (bf16[96,512]{1,0:T(8,128)(2,1)S(1)}, bf16[96,512]{1,0:T(8,128)(2,1)S(1)}, u32[]{:S(2)}, u32[]{:S(2)}) collective-permute-start(bf16[96,512]{1,0:T(8,128)(2,1)S(1)} %get-tuple-element.24), channel_id=1, source_target_pairs={{0,1},{1,0},{2,3},{3,2},{4,5},{5,4},{6,7},{7,6},{8,9},{9,8},{10,11... | collective-permute-start | bytes 294920 | tf_op jit(solution)/shard_map/ppermute | solution.py:419
  162.6 5.5 %collective-permute-start.18 = (bf16[96,512]{1,0:T(8,128)(2,1)S(1)}, bf16[96,512]{1,0:T(8,128)(2,1)S(1)}, u32[]{:S(2)}, u32[]{:S(2)}) collective-permute-start(bf16[96,512]{1,0:T(8,128)(2,1)S(1)} %get-tuple-element.25), channel_id=1, source_target_pairs={{0,2},{1,3},{2,0},{3,1},{4,6},{5,7},{6,4},{7,5},{8,10},{9,11},{10,... | collective-permute-start | bytes 294920 | tf_op jit(solution)/shard_map/ppermute | solution.py:419
  165.7 2.3 %copy-start.6 = (bf16[96,512]{1,0:T(8,128)(2,1)}, bf16[96,512]{1,0:T(8,128)(2,1)S(1)}, u32[]{:S(2)}) copy-start(bf16[96,512]{1,0:T(8,128)(2,1)S(1)} %collective-permute-done.20.refs_3_) | copy-start | bytes 294916
  165.7 2.3 %copy-start.7 = (bf16[96,512]{1,0:T(8,128)(2,1)}, bf16[96,512]{1,0:T(8,128)(2,1)S(1)}, u32[]{:S(2)}) copy-start(bf16[96,512]{1,0:T(8,128)(2,1)S(1)} %collective-permute-done.19.refs_2_) | copy-start | bytes 294916
  168.0 0.6 copy-start.8

commit v2 on v1

--- a/solution.py
+++ b/solution.py
@@ -17,7 +17,7 @@
 norm_eps = 1e-06
 rope_theta = 10000.0
 block_limit = 1024
-query_block = 256
+query_block = 128
 
 
 def rms_scale(matrix):
@@ -203,8 +203,8 @@
     return (latent.astype(jnp.float32) + whole_mod[4] * summed).astype(jnp.bfloat16)
 
 
-def query_slots_of(heads):
-    return (tuple(range(heads)),)
+def slot_head(sp, e, j):
+    return (sp // 4 ^ e) * 2 + (sp % 2 ^ j)
 
 
 def vmem(count):
@@ -212,14 +212,16 @@
 
 
 SMEM = pl.BlockSpec(memory_space=pltpu.SMEM)
+HBM = pl.BlockSpec(memory_space=pltpu.HBM)
+SLOTS = ((1, 0), (1, 1), (0, 0), (0, 1))
 
 
 def cost(flops, moved):
     return pl.CostEstimate(flops=flops, bytes_accessed=moved, transcendentals=0)
 
 
-def params():
-    return pltpu.CompilerParams(vmem_limit_bytes=56 * 1024 * 1024)
+def params(mebibytes):
+    return pltpu.CompilerParams(vmem_limit_bytes=mebibytes * 1024 * 1024)
 
 
 def modulation_kernel(lam, cond_latent, cond_context, shift_w, scale_w, gate_w, gain, out):
@@ -246,8 +248,16 @@
 def project_kernel(head_count, *refs):
     slots = refs[0:4]
     context, mods, cos_t, sin_t, query_w, key_w, value_w = refs[4:11]
-    outs = refs[11 : 11 + head_count]
-    hidden, ready = refs[11 + head_count :]
+    far_queries, far_pairs, near = refs[11:13], refs[13:15], refs[15:17]
+    hidden, ready, query_v, key_v, value_v, sems = refs[17:]
+    loads = [
+        pltpu.make_async_copy(source, held, sems.at[index])
+        for index, (source, held) in enumerate(
+            ((query_w, query_v), (key_w, key_v), (value_w, value_v))
+        )
+    ]
+    for load in loads:
+        load.start()
     own_rows = slots[0].shape[0]
     tok = 4 * own_rows
     ctx = context.shape[0]
@@ -280,7 +290,11 @@
         return jnp.where(lane < HEAD_DIM, first, pltpu.roll(second, HEAD_DIM, 1))
 
     per_tile = LANES // HEAD_DIM
-    for weight, base, count in ((query_w, 0, tok), (key_w, tok, tok + ctx)):
+    for load, weight, base, count in (
+        (loads[0], query_v, 0, tok),
+        (loads[1], key_v, tok, tok + ctx),
+    ):
+        load.wait()
         first = dot(hidden[:count, :], weight[0])
         second = dot(hidden[:count, :], weight[1])
         for head in range(head_count):
@@ -291,49 +305,60 @@
                 ready[head, base + tok : base + count, :] = whole[tok:].astype(jnp.bfloat16)
     base = 2 * tok + ctx
     wide = 2 * VALUE_DIM
+    loads[2].wait()
     for pair in range(head_count // 2):
-        both = dot(hidden[...], value_w[:, pair * wide : (pair + 1) * wide]).astype(jnp.bfloat16)
+        both = dot(hidden[...], value_v[:, pair * wide : (pair + 1) * wide]).astype(jnp.bfloat16)
         ready[2 * pair, base:, :] = both[:, :VALUE_DIM]
         ready[2 * pair + 1, base:, :] = both[:, VALUE_DIM:]
-    low = lax.axis_index("sp") % head_count
-    for k in range(head_count):
-        outs[k][...] = ready[low ^ k]
-
-
-def attention_kernel(head_count, tok, ctx, query_slots, *refs):
-    whole = refs[0:head_count]
-    swapped = refs[head_count : 2 * head_count]
-    mods = refs[2 * head_count]
-    outs = refs[2 * head_count + 1 : 2 * head_count + 1 + len(query_slots)]
-    queries, keys, values, results, scores_a, scores_b, top_a, top_b, weights = refs[
-        2 * head_count + 1 + len(query_slots) :
-    ]
-    part = tok + ctx
-    for index, k in enumerate(query_slots):
-        queries[index * tok : (index + 1) * tok, :] = whole[k][:tok, :]
-    for k in range(head_count):
-        for place_of, ref, base in ((k, whole[k], tok), (head_count + k, swapped[k], 0)):
-            rows = slice(place_of * part, (place_of + 1) * part)
-            keys[rows, :] = ref[base : base + part, :]
-            values[rows, :LANES] = ref[base + part : base + 2 * part, :]
-    ones = lax.broadcasted_iota(jnp.int32, (keys.shape[0], LANES), 1) == 0
+    sp = lax.axis_index("sp")
+    for j in range(2):
+        near[j][...] = ready[slot_head(sp, 0, j)]
+        far_queries[j][...] = ready[slot_head(sp, 1, j), :tok, :]
+        far_pairs[j][...] = ready[slot_head(sp, 1, j), tok:, :]
+
+
+def attention_kernel(head_count, tok, part, first, last, query_count, *refs):
+    refs = list(refs)
+    query_refs = [refs.pop(0) for _ in range(query_count)]
+    pair_refs = [refs.pop(0) for _ in range(4)]
+    if not first:
+        sums_in, tops_in = refs.pop(0), refs.pop(0)
+    if last:
+        mods = refs.pop(0)
+        outs = [refs.pop(0) for _ in range(query_count)]
+    else:
+        states = [(refs.pop(0), refs.pop(0)) for _ in range(2)]
+    queries, keys, values, scores_a, scores_b, top_a, top_b, weights, shares = refs
+    span = 4 * part
+    for index, ref in enumerate(query_refs):
+        queries[index * tok : (index + 1) * tok, :] = ref[:tok, :]
+    for index, ref in enumerate(pair_refs):
+        rows = slice(index * part, (index + 1) * part)
+        offset = ref.shape[0] - 2 * part
+        keys[rows, :] = ref[offset : offset + part, :]
+        values[rows, :LANES] = ref[offset + part :, :]
+    ones = lax.broadcasted_iota(jnp.int32, (span, LANES), 1) == 0
     values[:, LANES:] = ones.astype(jnp.float32).astype(jnp.bfloat16)
-    sp, tp = lax.axis_index("sp"), lax.axis_index("tp")
-    head = sp % head_count
-    owner = tp - tp % 2 + sp // head_count
-    width = head_count * VALUE_DIM
-    gain = mods[5:6, pl.ds(pl.multiple_of((owner * head_count + head) * VALUE_DIM, LANES), VALUE_DIM)]
-    lam_row = mods[6:7, pl.ds(pl.multiple_of(owner * width, LANES), LANES)]
-    lane_row = lax.broadcasted_iota(jnp.int32, lam_row.shape, 1)
-    lam = jnp.sum(jnp.where(lane_row == head, lam_row, 0.0), axis=-1, keepdims=True)
     factor = HEAD_DIM ** (-0.5) * math.log2(math.e)
-    block = scores_a.shape[0] // 2
-    blocks = queries.shape[0] // block
+    block = query_block
+    blocks = query_count * tok // block
     lane = lax.broadcasted_iota(jnp.int32, (block, LANES), 1)
-    span = keys.shape[0]
+    if last:
+        sp, tp = lax.axis_index("sp"), lax.axis_index("tp")
+        head = sp // 4 * 2 + sp % 2
+        owner = tp - tp % 2 + sp // 2 % 2
+        width = head_count * VALUE_DIM
+        start = pl.multiple_of((owner * head_count + head) * VALUE_DIM, LANES)
+        gain = mods[5:6, pl.ds(start, VALUE_DIM)]
+        lam_row = mods[6:7, pl.ds(pl.multiple_of(owner * width, LANES), LANES)]
+        lane_row = lax.broadcasted_iota(jnp.int32, lam_row.shape, 1)
+        lam = jnp.sum(jnp.where(lane_row == head, lam_row, 0.0), axis=-1, keepdims=True)
+
+    def at(index, size):
+        return pl.ds(pl.multiple_of(index * size, size), size) if not isinstance(index, int) else pl.ds(index * size, size)
 
     def score(index, scores, top):
-        q = queries[pl.ds(pl.multiple_of(index * block, block), block), :]
+        q = queries[at(index, block), :]
         zero = jnp.zeros_like(q)
         both = jnp.concatenate(
             [jnp.where(lane < HEAD_DIM, q, zero), jnp.where(lane < HEAD_DIM, zero, q)], axis=0
@@ -347,37 +372,78 @@
             running = jnp.maximum(running, result[:, start : start + LANES])
         top[...] = jnp.broadcast_to(jnp.max(running, axis=-1, keepdims=True), top.shape)
 
-    def absorb_block(index, scores, top):
-        weights[...] = jnp.exp2((scores[...] - top[:, 0:1]) * factor).astype(jnp.bfloat16)
-        sums = jnp.dot(weights[...], values[...], preferred_element_type=jnp.float32)
-        share = sums[:, :LANES] / sums[:, LANES : LANES + 1]
-        mixed = share[:block] - lam * share[block:]
-        norm = lax.rsqrt(jnp.mean(mixed * mixed, axis=-1, keepdims=True) + norm_eps)
-        rows = pl.ds(pl.multiple_of(index * block, block), block)
-        results[rows, :] = (mixed * norm * gain).astype(jnp.bfloat16)
+    wide_lane = lax.broadcasted_iota(jnp.int32, (2 * block, LANES), 1)
+
+    def absorb_block(index, scores, top, state=None, origin=0):
+        highest = top[...]
+        if not first:
+            rows = at(index, 2 * block)
+            held = tops_in[rows, :]
+            before = jnp.broadcast_to(held[:, :1], held.shape)
+            highest = jnp.maximum(highest, before)
+            shrink = jnp.exp2((before - highest) * factor)
+        for start in range(0, span, LANES):
+            tile = (scores[:, start : start + LANES] - highest) * factor
+            weights[:, start : start + LANES] = jnp.exp2(tile).astype(jnp.bfloat16)
+        both = jnp.dot(weights[...], values[...], preferred_element_type=jnp.float32)
+        sums, total = both[:, :LANES], both[:, LANES : LANES + 1]
+        if not first:
+            sums = sums + sums_in[rows, :] * shrink
+            total = total + held[:, LANES - 1 :] * shrink[:, :1]
+        if not last:
+            sums_out, tops_out = state
+            rows = at(index - origin, 2 * block)
+            sums_out[rows, :] = sums
+            tops_out[rows, :] = jnp.where(wide_lane < LANES // 2, highest, total)
+            return
+        for which in range(2):
+            rows = at(index + which * blocks, block)
+            ends = slice(which * block, (which + 1) * block)
+            shares[rows, :] = sums[ends] / total[ends]
+
+    def sweep(begin, end, state=None):
+        def step(pair, carry):
+            index = begin + 2 * pair
+            score(index + 1, scores_b, top_b)
+            absorb_block(index, scores_a, top_a, state, begin)
+            score(jnp.minimum(index + 2, blocks - 1), scores_a, top_a)
+            absorb_block(index + 1, scores_b, top_b, state, begin)
+            return carry
+
+        lax.fori_loop(0, (end - begin) // 2, step, 0)
 
     score(0, scores_a, top_a)
-
-    def step(pair, carry):
-        index = 2 * pair
-        score(jnp.minimum(index + 1, blocks - 1), scores_b, top_b)
-        absorb_block(index, scores_a, top_a)
-        score(jnp.minimum(index + 2, blocks - 1), scores_a, top_a)
-        absorb_block(jnp.minimum(index + 1, blocks - 1), scores_b, top_b)
-        return carry
-
-    lax.fori_loop(0, pl.cdiv(blocks, 2), step, 0)
-    for index in range(len(query_slots)):
-        outs[index][...] = results[index * tok : (index + 1) * tok, :]
+    if last:
+        sweep(0, blocks)
+        for index, out in enumerate(outs):
+            first_map = shares[index * tok : (index + 1) * tok, :]
+            second_map = shares[(query_count + index) * tok : (query_count + index + 1) * tok, :]
+            mixed = first_map - lam * second_map
+            norm = lax.rsqrt(jnp.mean(mixed * mixed, axis=-1, keepdims=True) + norm_eps)
+            out[...] = (mixed * norm * gain).astype(jnp.bfloat16)
+    else:
+        sweep(0, blocks // 2, states[0])
+        sweep(blocks // 2, blocks, states[1])
 
 
 def output_kernel(*refs):
-    terms = refs[0:4]
-    weights = refs[4:8]
-    latent, mods, out = refs[8:11]
+    terms, weights = refs[0:4], refs[4:8]
+    latent, mods, out, ordered, held, sems = refs[8:]
+    loads = [
+        pltpu.make_async_copy(weight, held.at[index], sems.at[index])
+        for index, weight in enumerate(weights)
+    ]
+    for load in loads:
+        load.start()
+    sp = lax.axis_index("sp")
+    for index, term in enumerate(terms):
+        for slot, (e, j) in enumerate(SLOTS):
+            place = pl.multiple_of(slot_head(sp, e, j) * VALUE_DIM, VALUE_DIM)
+            ordered[index, :, pl.ds(place, VALUE_DIM)] = term[:, slot * VALUE_DIM : (slot + 1) * VALUE_DIM]
     total = None
-    for term, weight in zip(terms, weights):
-        group = jnp.dot(term[...], weight[...], preferred_element_type=jnp.float32)
+    for index, load in enumerate(loads):
+        load.wait()
+        group = jnp.dot(ordered[index], held[index], preferred_element_type=jnp.float32)
         group = group.astype(jnp.bfloat16).astype(jnp.float32)
         total = group if total is None else total + group
     out[...] = (latent[...].astype(jnp.float32) + mods[4:5, :] * total).astype(jnp.bfloat16)
@@ -408,7 +474,6 @@
     f32, bf16 = jnp.float32, jnp.bfloat16
     sp = lax.axis_index("sp")
     tp = lax.axis_index("tp")
-    low = sp % heads
 
     def hop(array, target):
         pairs = []
@@ -421,15 +486,20 @@
     def across(array, bit):
         return hop(array, lambda s, t: (s, t ^ bit))
 
-    def to_owner(k):
-        return lambda s, t: ((t % 2) * heads + ((s % heads) ^ k), t - t % 2 + s // heads)
+    def to_owner(e, j):
+        def target(s, t):
+            return (s // 4 ^ e) * 4 + t % 2 * 2 + (s % 2 ^ j), t - t % 2 + s // 2 % 2
+
+        return target
+
+    from_owner = to_owner
 
     mod_part = pl.pallas_call(
         modulation_kernel,
         out_shape=jax.ShapeDtypeStruct((8, shift_weight.shape[1]), f32),
         in_specs=[SMEM] + vmem(6),
         out_specs=vmem(1)[0],
-        compiler_params=params(),
+        compiler_params=params(60),
         cost_estimate=cost(10**9, 10**6),
         name="modulation",
     )(
@@ -445,7 +515,9 @@
     lat_x = across(latent, 2)
     lat_c = across(latent, 1)
     step = 1
+    mod_sums = []
     while step < sp_size:
+        mod_sums.append(mod_part)
         mod_part = mod_part + hop(mod_part, lambda s, t, step=step: (s ^ step, t))
         step *= 2
     mods = lax.all_gather(mod_part, "tp", axis=1, tiled=True)
@@ -453,61 +525,90 @@
     slots = (latent, lat_x, lat_c, lat_xc)
     slot_bits = (0, 2, 1, 3)
 
-    positions = jnp.concatenate(
-        [sp * tok + (tp ^ bit) * own_rows + jnp.arange(own_rows, dtype=jnp.int32) for bit in slot_bits]
-    )
-    cos_half, sin_half = rope_tables(positions, GRID_W, HEAD_DIM)
-    cos_t = jnp.concatenate([cos_half] * (2 * LANES // HEAD_DIM), axis=-1)
-    sin_t = jnp.concatenate([-sin_half, sin_half] * (LANES // HEAD_DIM), axis=-1)
+    shape = (tok, LANES)
+    row = lax.broadcasted_iota(jnp.int32, shape, 0)
+    lane = lax.broadcasted_iota(jnp.int32, shape, 1)
+    slot = row // own_rows
+    bits = slot // 2 + slot % 2 * 2
+    positions = sp * tok + (tp ^ bits) * own_rows + row % own_rows
+    quarter = HEAD_DIM // 4
+    inverse = rope_theta ** (-jnp.arange(quarter, dtype=f32) / quarter)
+    inverse = jnp.tile(inverse, LANES // quarter)[None, :]
+    coordinate = jnp.where(lane % (2 * quarter) < quarter, positions // GRID_W, positions % GRID_W)
+    angles = coordinate.astype(f32) * inverse
+    cos_t = jnp.cos(angles)
+    angles, _ = lax.optimization_barrier((angles, mod_sums[1]))
+    sin_t = jnp.sin(angles)
+    sin_t = jnp.where(lane % HEAD_DIM < HEAD_DIM // 2, -sin_t, sin_t)
 
     part = tok + ctx
-    message = jax.ShapeDtypeStruct((tok + 2 * part, LANES), bf16)
+
+    def block(rows):
+        return jax.ShapeDtypeStruct((rows, LANES), bf16)
+
     messages = pl.pallas_call(
         functools.partial(project_kernel, heads),
-        out_shape=[message] * heads,
-        in_specs=vmem(11),
-        out_specs=vmem(heads),
+        out_shape=[block(tok)] * 2 + [block(2 * part)] * 2 + [block(tok + 2 * part)] * 2,
+        in_specs=vmem(8) + [HBM] * 3,
+        out_specs=vmem(6),
         scratch_shapes=[
             pltpu.VMEM((part, width), bf16),
-            pltpu.VMEM((heads,) + message.shape, bf16),
+            pltpu.VMEM((heads, tok + 2 * part, LANES), bf16),
+            pltpu.VMEM(query_weight.shape, bf16),
+            pltpu.VMEM(key_weight.shape, bf16),
+            pltpu.VMEM(value_weight.shape, bf16),
+            pltpu.SemaphoreType.DMA((3,)),
         ],
-        compiler_params=params(),
+        compiler_params=params(56),
         cost_estimate=cost(2 * part * width * 6 * heads * HEAD_DIM, 8 * 10**6),
         name="project",
     )(*slots, context, mods, cos_t, sin_t, query_weight, key_weight, value_weight)
 
-    arrived = [hop(messages[k], to_owner(k)) for k in range(heads)]
-    swapped = [across(arrived[k][tok:], 1) for k in range(heads)]
-
-    results = []
-    for slots_of in query_slots_of(heads):
-        results += pl.pallas_call(
-            functools.partial(attention_kernel, heads, tok, ctx, slots_of),
-            out_shape=[jax.ShapeDtypeStruct((tok, LANES), bf16)] * len(slots_of),
-            in_specs=vmem(2 * heads + 1),
-            out_specs=vmem(len(slots_of)),
+    far_queries = [hop(messages[j], to_owner(1, j)) for j in range(2)]
+    near = [hop(messages[4 + j], to_owner(0, j)) for j in range(2)]
+    far = [hop(messages[2 + j], to_owner(1, j)) for j in range(2)]
+    near_swapped = [across(near[j], 1) for j in range(2)]
+    far_swapped = [across(far[j], 1) for j in range(2)]
+
+    def attend(query_refs, pairs, state, last):
+        count = len(query_refs)
+        shapes = [jax.ShapeDtypeStruct((heads * tok, LANES), f32)] * 4
+        if last:
+            shapes = [block(tok)] * count
+        inputs = list(query_refs) + list(pairs) + list(state)
+        if last:
+            inputs.append(mods)
+        return pl.pallas_call(
+            functools.partial(attention_kernel, heads, tok, part, not state, last, count),
+            out_shape=shapes,
+            in_specs=vmem(len(inputs)),
+            out_specs=vmem(len(shapes)),
             scratch_shapes=[
-                pltpu.VMEM((len(slots_of) * tok, LANES), bf16),
-                pltpu.VMEM((2 * heads * part, LANES), bf16),
-                pltpu.VMEM((2 * heads * part, 2 * LANES), bf16),
-                pltpu.VMEM((len(slots_of) * tok, LANES), bf16),
-                pltpu.VMEM((2 * query_block, 2 * heads * part), f32),
-                pltpu.VMEM((2 * query_block, 2 * heads * part), f32),
+                pltpu.VMEM((count * tok, LANES), bf16),
+                pltpu.VMEM((4 * part, LANES), bf16),
+                pltpu.VMEM((4 * part, 2 * LANES), bf16),
+                pltpu.VMEM((2 * query_block, 4 * part), f32),
+                pltpu.VMEM((2 * query_block, 4 * part), f32),
                 pltpu.VMEM((2 * query_block, LANES), f32),
                 pltpu.VMEM((2 * query_block, LANES), f32),
-                pltpu.VMEM((2 * query_block, 2 * heads * part), bf16),
+                pltpu.VMEM((2 * query_block, 4 * part), bf16),
+                pltpu.VMEM((2 * count * tok if last else 8, LANES), f32),
             ],
-            compiler_params=params(),
-            cost_estimate=cost(2 * 2 * len(slots_of) * tok * 2 * heads * part * 4 * LANES, 4 * 10**6),
+            compiler_params=params(24),
+            cost_estimate=cost(16 * count * tok * 4 * part * LANES, 10**6),
             name="attention",
-        )(*arrived, *swapped, mods)
-
-    back = [hop(results[k], to_owner(k)) for k in range(heads)]
-    stacked = jnp.stack(back)
-    ordered = jnp.concatenate(
-        [lax.dynamic_index_in_dim(stacked, low ^ m, 0, keepdims=False) for m in range(heads)], axis=1
-    )
-    pieces = [ordered[i * own_rows : (i + 1) * own_rows] for i in range(tp_size)]
+        )(*inputs)
+
+    state = attend(far_queries + near, near + near_swapped, (), False)
+    late = far + far_swapped
+    results = attend(far_queries, late, state[:2], True)
+    back = [hop(results[j], from_owner(1, j)) for j in range(2)]
+    results = attend(near, late, state[2:], True)
+    back += [hop(results[j], from_owner(0, j)) for j in range(2)]
+    pieces = [
+        jnp.concatenate([held[i * own_rows : (i + 1) * own_rows] for held in back], axis=1)
+        for i in range(tp_size)
+    ]
     terms = [pieces[0]] + [across(pieces[i], slot_bits[i]) for i in range(1, tp_size)]
 
     late_weight, _ = lax.optimization_barrier((out_weight, mods))
@@ -517,9 +618,14 @@
     return pl.pallas_call(
         output_kernel,
         out_shape=jax.ShapeDtypeStruct(latent.shape, bf16),
-        in_specs=vmem(10),
+        in_specs=vmem(4) + [HBM] * 4 + vmem(2),
         out_specs=vmem(1)[0],
-        compiler_params=params(),
+        scratch_shapes=[
+            pltpu.VMEM((4, own_rows, heads * VALUE_DIM), bf16),
+            pltpu.VMEM((4,) + out_weight.shape, bf16),
+            pltpu.SemaphoreType.DMA((4,)),
+        ],
+        compiler_params=params(24),
         cost_estimate=cost(2 * own_rows * width * width, 8 * 10**6),
         name="output",
     )(*terms, out_weight, weight_x, weight_c, weight_xc, latent, mods)
@@ -548,13 +654,12 @@
         own_rows = args[0].shape[0]
         owner_plan = (
             tp_size == 4
-            and sp_size == 2 * heads
-            and heads % 2 == 0
-            and heads & (heads - 1) == 0
+            and sp_size == 8
+            and heads == 4
             and 2 * HEAD_DIM == LANES
             and VALUE_DIM == LANES
             and own_rows % 32 == 0
-            and (heads * tp_size * own_rows) % query_block == 0
+            and (2 * tp_size * own_rows) % query_block == 0
             and args[1].shape[0] % 16 == 0
         )
         if owner_plan:

time: 175 us -> 121 us (0.69)
  waiting for transfers between devices: 70.3 us -> 32.1 us
  starting transfers between devices: 58 us -> 42.6 us
  local copies, waits for them, and re-layouts: 3.29 us -> 0.87 us
    ppermute x24 -> x26, waiting for transfers between devices: 70.3 us -> 32.1 us  [hop(): return lax.ppermute(array, axes, pairs)]
    ppermute x24 -> x26, starting transfers between devices: 58 us -> 42.6 us  [hop(): return lax.ppermute(array, axes, pairs)]
    pallas_call x2 -> x4, Pallas kernels: 26.1 us -> 28.5 us  [the longest x3 19.9 us: attend(): pl.pallas_call(functools.partial(attention_kernel, heads, tok, part, not...]
    mul x1, other arithmetic: 0.07 us -> 2.05 us  [local_owner(): angles = coordinate.astype(f32) * inverse]
    pallas_call x1, Pallas kernels: 5.89 us -> 3.98 us  [local_owner(): pl.pallas_call(output_kernel, out_shape=jax.ShapeDtypeStruct(latent.shape...]
    concatenate x3 -> x4, other arithmetic: 1.87 us -> 0.06 us  [local_owner(): jnp.concatenate([held[i * own_rows:(i + 1) * own_rows] for held in back],...]
  transfers between devices with their start and end apart: 24 -> 26, of which waited for: 9 -> 10; matrix products, arithmetic and copies ran while one was open for 2% -> 3% of each run, Pallas kernels for 15% -> 24%
where the time goes in v2:
time: 121 us; the launch traced here: 120 us
  starting transfers between devices  42.6 us (35%)
  Pallas kernels  34.6 us (29%)
  waiting for transfers between devices  32.1 us (27%)
  blocking collectives  5.67 us (5%)
  other arithmetic  4.23 us (3%)
    ppermute x26, starting transfers between devices, hop(): return lax.ppermute(array, axes, pairs)  42.6 us
    ppermute x26, waiting for transfers between devices, hop(): return lax.ppermute(array, axes, pairs)  32.1 us
    pallas_call x3, Pallas kernels, attend(): pl.pallas_call(functools.partial(attention_kernel, heads, tok, part, not...  19.9 us
    pallas_call x1, Pallas kernels, local_owner(): pl.pallas_call(functools.partial(project_kernel, heads), out_shape=[block...  8.61 us
    all_gather x1, blocking collectives, local_owner(): mods = lax.all_gather(mod_part, 'tp', axis=1, tiled=True)  5.67 us
    pallas_call x1, Pallas kernels, local_owner(): pl.pallas_call(output_kernel, out_shape=jax.ShapeDtypeStruct(latent.shape...  3.98 us
  transfers between devices with their start and end apart: 26, of which 10 were waited for; matrix products, arithmetic and copies ran while one was open for 3% of the time, Pallas kernels for 24%

profile of v2, /device:TPU:0, one launch (start us, length us, event | category | flops | bytes accessed | tf_op | source)
XLA Modules:
  0.0 120.4 jit_solution(2068650570388524908)
XLA Ops:
  0.0 2.1 %modulation.1 = f32[8,512]{1,0:T(8,128)} custom-call(f32[4]{0:T(128)} %lam.1, f32[1,2048]{1,0:T(1,128)} %bitcast.3, f32[1,2048]{1,0:T(1,128)} %bitcast.4, bf16[256,512]{1,0:T(8,128)(2,1)} %shift_w.1, bf16[256,512]{1,0:T(8,128)(2,1)} %scale_w.1, bf16[256,512]{1,0:T(8,128)(2,1)} %gate_w.1, f32[1,512]{1,0:T(1,128)} %bitcast.5), custom_call_target="tpu_custom_call" | custom-call | flops 1000000000 | bytes 1000000 | tf_op jit(solution)/shard_map/modulation/pallas_call | solution.py:497
  2.1 3.0 %collective-permute-start.3 = (f32[8,512]{1,0:T(8,128)}, f32[8,512]{1,0:T(8,128)S(1)}, u32[]{:S(2)}, u32[]{:S(2)}) collective-permute-start(f32[8,512]{1,0:T(8,128)} %modulation.1), channel_id=1, source_target_pairs={{0,4},{1,5},{2,6},{3,7},{4,0},{5,1},{6,2},{7,3},{8,12},{9,13},{10,... | collective-permute-start | bytes 49160 | tf_op jit(solution)/shard_map/ppermute | solution.py:484
  5.1 1.9 %collective-permute-done.3 = f32[8,512]{1,0:T(8,128)S(1)} collective-permute-done((f32[8,512]{1,0:T(8,128)}, f32[8,512]{1,0:T(8,128)S(1)}, u32[]{:S(2)}, u32[]{:S(2)}) %collective-permute-start.3) | collective-permute-done | bytes 16416 | tf_op jit(solution)/shard_map/ppermute | solution.py:484
  7.1 0.7 add.50
  7.8 2.1 %collective-permute-start.4 = (f32[8,512]{1,0:T(8,128)S(1)}, f32[8,512]{1,0:T(8,128)S(1)}, u32[]{:S(2)}, u32[]{:S(2)}) collective-permute-start(f32[8,512]{1,0:T(8,128)S(1)} %add.50), channel_id=1, source_target_pairs={{0,8},{1,9},{2,10},{3,11},{4,12},{5,13},{6,14},{7,15},{8,0},{9,1},... | collective-permute-start | bytes 49160 | tf_op jit(solution)/shard_map/ppermute | solution.py:484
  9.9 1.5 %collective-permute-start = (bf16[96,2048]{1,0:T(8,128)(2,1)S(1)}, bf16[96,2048]{1,0:T(8,128)(2,1)S(1)}, u32[]{:S(2)}, u32[]{:S(2)}) collective-permute-start(bf16[96,2048]{1,0:T(8,128)(2,1)S(1)} %copy-done.1), channel_id=1, source_target_pairs={{0,2},{1,3},{2,0},{3,1},{4,6},{5,7},{6,4},{7,5},{8,10},{9,11},{10,... | collective-permute-start | bytes 1179656 | tf_op jit(solution)/shard_map/ppermute | solution.py:484
  11.4 0.2 collective-permute-done.4
  11.6 3.0 %collective-permute-start.5 = (f32[8,512]{1,0:T(8,128)S(1)}, f32[8,512]{1,0:T(8,128)S(1)}, u32[]{:S(2)}, u32[]{:S(2)}) collective-permute-start(f32[8,512]{1,0:T(8,128)S(1)} %add.51), channel_id=1, source_target_pairs={{0,16},{1,17},{2,18},{3,19},{4,20},{5,21},{6,22},{7,23},{8,24},{9,... | collective-permute-start | bytes 49160 | tf_op jit(solution)/shard_map/ppermute | solution.py:484
  14.6 1.7 %collective-permute-done.5 = f32[8,512]{1,0:T(8,128)S(1)} collective-permute-done((f32[8,512]{1,0:T(8,128)S(1)}, f32[8,512]{1,0:T(8,128)S(1)}, u32[]{:S(2)}, u32[]{:S(2)}) %collective-permute-start.5) | collective-permute-done | bytes 16416 | tf_op jit(solution)/shard_map/ppermute | solution.py:484
  16.3 5.7 %all_gather.3.refs_5_.refs_8_.refs_9_ = f32[8,2048]{1,0:T(8,128)} all-gather(f32[8,512]{1,0:T(8,128)S(1)} %add.52), channel_id=1, replica_groups=mesh['sp'=8,'tp'=4] {'tp'}, dimensions={1}, use_global_device_ids=true | all-gather | bytes 81920 | tf_op jit(solution)/shard_map/all_gather | solution.py:523
  22.0 1.8 %collective-permute-start.23 = (bf16[512,2048]{1,0:T(8,128)(2,1)S(1)}, bf16[512,2048]{1,0:T(8,128)(2,1)}, u32[]{:S(2)}, u32[]{:S(2)}) collective-permute-start(bf16[512,2048]{1,0:T(8,128)(2,1)S(1)} %copy-done), channel_id=1, source_target_pairs={{0,2},{1,3},{2,0},{3,1},{4,6},{5,7},{6,4},{7,5},{8,10},{9,11},{10,... | collective-permute-start | bytes 6291464 | tf_op jit(solution)/shard_map/ppermute | solution.py:484
  23.9 0.1 mul.24
  24.0 2.0 %fusion.8 = (f32[384,128]{1,0:T(8,128)S(1)}, f32[384,128]{1,0:T(8,128)}) fusion(f32[128]{0:T(128)S(1)} %mul.24, s32[384]{0:T(512)S(1)} %get-tuple-element.56, s32[384]{0:T(512)S(1)} %get-tuple-element.57, s32[384]{0:T(512)S(1)} %get-tuple-element.55, s32[384]{0:T(512)S(1)} %get-tuple-element.58, s32[]{:T(128)S(6)} %axis_index.25, s32[]{:T(128)S(6)} %mul.21, ...), kind=kLoop, calls=%fused_computation.22 | loop fusion | flops 2506752 | bytes 401800 | tf_op jit(solution)/shard_map/mul | solution.py:538
  26.0 0.1 collective-permute-start.2
  26.1 1.3 %negate_select_fusion.refs_7_ = f32[384,128]{1,0:T(8,128)} fusion(f32[384,128]{1,0:T(8,128)S(1)} %get-tuple-element.21, s32[128]{0:T(128)S(1)} %get-tuple-element.63, s32[128]{0:T(128)S(1)} %get-tuple-element.64, pred[128]{0:T(512)(128)(4,1)S(1)} %compare_and_fusion), kind=kLoop, calls=%fused_computation.4 | loop fusion | flops 196608 | bytes 394368 | tf_op jit(solution)/shard_map/jit(_where)/select_n | solution.py:542
  27.5 0.3 collective-permute-done.2.refs_3_
  27.8 0.5 copy-done.5
  28.2 0.3 copy-done.6
  28.5 8.6 %project.1 = (bf16[384,128]{1,0:T(8,128)(2,1)}, bf16[384,128]{1,0:T(8,128)(2,1)}, bf16[896,128]{1,0:T(8,128)(2,1)}, bf16[896,128]{1,0:T(8,128)(2,1)}, bf16[1280,...) custom-call(bf16[96,2048]{1,0:T(8,128)(2,1)} %refs_8_.3, bf16[96,2048]{1,0:T(8,128)(2,1)} %copy-done.4, ...), custom_call_target="tpu_custom_call" | custom-call | flops 2818572288 | bytes 8000000 | tf_op jit(solution)/shard_map/project/pallas_call | solution.py:549
  37.1 1.6 %collective-permute-start.12 = (bf16[1280,128]{1,0:T(8,128)(2,1)}, bf16[1280,128]{1,0:T(8,128)(2,1)S(1)}, u32[]{:S(2)}, u32[]{:S(2)}) collective-permute-start(bf16[1280,128]{1,0:T(8,128)(2,1)} %get-tuple-element.26), channel_id=1, source_target_pairs={{0,0},{1,8},{2,2},{3,10},{4,4},{5,12},{6,6},{7,14},{8,1},{9,9},{10... | collective-permute-start | bytes 983048 | tf_op jit(solution)/shard_map/ppermute | solution.py:484
  38.7 1.5 %collective-permute-start.13 = (bf16[1280,128]{1,0:T(8,128)(2,1)}, bf16[1280,128]{1,0:T(8,128)(2,1)S(1)}, u32[]{:S(2)}, u32[]{:S(2)}) collective-permute-start(bf16[1280,128]{1,0:T(8,128)(2,1)} %get-tuple-element.27), channel_id=1, source_target_pairs={{0,4},{1,12},{2,6},{3,14},{4,0},{5,8},{6,2},{7,10},{8,5},{9,13},{1... | collective-permute-start | bytes 983048 | tf_op jit(solution)/shard_map/ppermute | solution.py:484
  40.3 2.6 %collective-permute-start.6 = (bf16[384,128]{1,0:T(8,128)(2,1)}, bf16[384,128]{1,0:T(8,128)(2,1)S(1)}, u32[]{:S(2)}, u32[]{:S(2)}) collective-permute-start(bf16[384,128]{1,0:T(8,128)(2,1)} %get-tuple-element.22), channel_id=1, source_target_pairs={{0,16},{1,24},{2,18},{3,26},{4,20},{5,28},{6,22},{7,30},{8,17},{9,... | collective-permute-start | bytes 294920 | tf_op jit(solution)/shard_map/ppermute | solution.py:484
  42.9 0.3 collective-permute-start.7
  43.1 0.0 collective-permute-done.12.refs_2_.refs_4_.refs_0_
  43.1 4.1 %collective-permute-start.14 = (bf16[1280,128]{1,0:T(8,128)(2,1)S(1)}, bf16[1280,128]{1,0:T(8,128)(2,1)S(1)}, u32[]{:S(2)}, u32[]{:S(2)}) collective-permute-start(bf16[1280,128]{1,0:T(8,128)(2,1)S(1)} %collective-permute-done.12.refs_2_.refs_4_.refs_0_), channel_id=1, source_target_pairs={{0,1},{1,0},{2,3},{3,2},{4,5},{5,4},{6,7},{7,6},{8,9},{9,8},{10,11... | collective-permute-start | bytes 983048 | tf_op jit(solution)/shard_map/ppermute | solution.py:484
  47.3 0.0 collective-permute-done.13.refs_3_.refs_5_.refs_1_
  47.3 5.3 %collective-permute-start.15 = (bf16[1280,128]{1,0:T(8,128)(2,1)S(1)}, bf16[1280,128]{1,0:T(8,128)(2,1)S(1)}, u32[]{:S(2)}, u32[]{:S(2)}) collective-permute-start(bf16[1280,128]{1,0:T(8,128)(2,1)S(1)} %collective-permute-done.13.refs_3_.refs_5_.refs_1_), channel_id=1, source_target_pairs={{0,1},{1,0},{2,3},{3,2},{4,5},{5,4},{6,7},{7,6},{8,9},{9,8},{10,11... | collective-permute-start | bytes 983048 | tf_op jit(solution)/shard_map/ppermute | solution.py:484
  52.6 3.2 %collective-permute-start.8 = (bf16[896,128]{1,0:T(8,128)(2,1)}, bf16[896,128]{1,0:T(8,128)(2,1)S(1)}, u32[]{:S(2)}, u32[]{:S(2)}) collective-permute-start(bf16[896,128]{1,0:T(8,128)(2,1)} %get-tuple-element.24), channel_id=1, source_target_pairs={{0,16},{1,24},{2,18},{3,26},{4,20},{5,28},{6,22},{7,30},{8,17},{9,... | collective-permute-start | bytes 688136 | tf_op jit(solution)/shard_map/ppermute | solution.py:484
  55.8 0.9 collective-permute-start.9
  56.7 15.6 %collective-permute-done.8.refs_2_ = bf16[896,128]{1,0:T(8,128)(2,1)S(1)} collective-permute-done((bf16[896,128]{1,0:T(8,128)(2,1)}, bf16[896,128]{1,0:T(8,128)(2,1)S(1)}, u32[]{:S(2)}, u32[]{:S(2)}) %collective-permute-start.8) | collective-permute-done | bytes 229408 | tf_op jit(solution)/shard_map/ppermute | solution.py:484
  72.3 5.0 %collective-permute-done.9.refs_3_ = bf16[896,128]{1,0:T(8,128)(2,1)S(1)} collective-permute-done((bf16[896,128]{1,0:T(8,128)(2,1)}, bf16[896,128]{1,0:T(8,128)(2,1)S(1)}, u32[]{:S(2)}, u32[]{:S(2)}) %collective-permute-start.9) | collective-permute-done | bytes 229408 | tf_op jit(solution)/shard_map/ppermute | solution.py:484
  77.3 0.5 collective-permute-start.11
  77.8 0.1 collective-permute-start.25
  77.9 9.3 %attention.3 = (f32[1536,128]{1,0:T(8,128)S(1)}, f32[1536,128]{1,0:T(8,128)S(1)}, f32[1536,128]{1,0:T(8,128)S(1)}, f32[1536,128]{1,0:T(8,128)S(1)}) custom-call(bf16[384,128]{1,0:T(8,128)(2,1)S(1)} %collective-permute-done.6.refs_0_, bf16[384,128]{1,0:T(8,128)(2,1)S(1)} %collective-permute-done.7.refs_1_, ...), custom_call_target="tpu_custom_call" | custom-call | flops 5637144576 | bytes 1000000 | tf_op jit(solution)/shard_map/attention/pallas_call | solution.py:581
  87.3 5.3 %attention.4 = (bf16[384,128]{1,0:T(8,128)(2,1)S(1)}, bf16[384,128]{1,0:T(8,128)(2,1)S(1)}) custom-call(bf16[384,128]{1,0:T(8,128)(2,1)S(1)} %collective-permute-done.6.refs_0_, bf16[384,128]{1,0:T(8,128)(2,1)S(1)} %collective-permute-done.7.refs_1_, bf16[896,128]{1,0:T(8,128)(2,1)S(1)} %collective-permute-done.8.refs_2_, ...), custom_call_target="tpu_custom_call" | custom-call | flops 2818572288 | bytes 1000000 | tf_op jit(solution)/shard_map/attention/pallas_call | solution.py:581
  92.6 1.4 %collective-permute-start.16 = (bf16[384,128]{1,0:T(8,128)(2,1)S(1)}, bf16[384,128]{1,0:T(8,128)(2,1)S(1)}, u32[]{:S(2)}, u32[]{:S(2)}) collective-permute-start(bf16[384,128]{1,0:T(8,128)(2,1)S(1)} %get-tuple-element.30), channel_id=1, source_target_pairs={{0,16},{1,24},{2,18},{3,26},{4,20},{5,28},{6,22},{7,30},{8,17},{9,... | collective-permute-start | bytes 294920 | tf_op jit(solution)/shard_map/ppermute | solution.py:484
  94.0 2.3 %collective-permute-start.17 = (bf16[384,128]{1,0:T(8,128)(2,1)S(1)}, bf16[384,128]{1,0:T(8,128)(2,1)S(1)}, u32[]{:S(2)}, u32[]{:S(2)}) collective-permute-start(bf16[384,128]{1,0:T(8,128)(2,1)S(1)} %get-tuple-element.31), channel_id=1, source_target_pairs={{0,20},{1,28},{2,22},{3,30},{4,16},{5,24},{6,18},{7,26},{8,21},{9,... | collective-permute-start | bytes 294920 | tf_op jit(solution)/shard_map/ppermute | solution.py:484
  96.3 5.3 %attention.5 = (bf16[384,128]{1,0:T(8,128)(2,1)S(1)}, bf16[384,128]{1,0:T(8,128)(2,1)S(1)}) custom-call(bf16[1280,128]{1,0:T(8,128)(2,1)S(1)} %collective-permute-done.12.refs_2_.refs_4_.refs_0_, bf16[1280,128]{1,0:T(8,128)(2,1)S(1)} %collective-permute-done.13.refs_3_.refs_5_.refs_1_, bf16[896,128]{1,0:T(8,128)(2,1)S(1)} %collective-permute-done.8.refs_2_, ...), custom_call_target="tpu_custom_call" | custom-call | flops 2818572288 | bytes 1000000 | tf_op jit(solution)/shard_map/attention/pallas_call | solution.py:581
  101.5 0.7 collective-permute-start.18
  102.2 1.9 %collective-permute-start.19 = (bf16[384,128]{1,0:T(8,128)(2,1)S(1)}, bf16[384,128]{1,0:T(8,128)(2,1)S(1)}, u32[]{:S(2)}, u32[]{:S(2)}) collective-permute-start(bf16[384,128]{1,0:T(8,128)(2,1)S(1)} %get-tuple-element.35), channel_id=1, source_target_pairs={{0,4},{1,12},{2,6},{3,14},{4,0},{5,8},{6,2},{7,10},{8,5},{9,13},{1... | collective-permute-start | bytes 294920 | tf_op jit(solution)/shard_map/ppermute | solution.py:484
  104.1 0.5 collective-permute-done.17
  104.7 2.2 %collective-permute-done.19 = bf16[384,128]{1,0:T(8,128)(2,1)S(1)} collective-permute-done((bf16[384,128]{1,0:T(8,128)(2,1)S(1)}, bf16[384,128]{1,0:T(8,128)(2,1)S(1)}, u32[]{:S(2)}, u32[]{:S(2)}) %collective-permute-start.19) | collective-permute-done | bytes 98336 | tf_op jit(solution)/shard_map/ppermute | solution.py:484
  106.9 3.1 %collective-permute-start.22 = (bf16[96,512]{1,0:T(8,128)(2,1)S(1)}, bf16[96,512]{1,0:T(8,128)(2,1)S(1)}, u32[]{:S(2)}, u32[]{:S(2)}) collective-permute-start(bf16[96,512]{1,0:T(8,128)(2,1)S(1)} %pad_maximum_fusion.3), channel_id=1, source_target_pairs={{0,3},{1,2},{2,1},{3,0},{4,7},{5,6},{6,5},{7,4},{8,11},{9,10},{10,... | collective-permute-start | bytes 294920 | tf_op jit(solution)/shard_map/ppermute | solution.py:484
  110.1 0.1 collective-permute-start.21
  110.2 1.5 %collective-permute-start.20 = (bf16[96,512]{1,0:T(8,128)(2,1)S(1)}, bf16[96,512]{1,0:T(8,128)(2,1)S(1)}, u32[]{:S(2)}, u32[]{:S(2)}) collective-permute-start(bf16[96,512]{1,0:T(8,128)(2,1)S(1)} %pad_maximum_fusion.1), channel_id=1, source_target_pairs={{0,2},{1,3},{2,0},{3,1},{4,6},{5,7},{6,4},{7,5},{8,10},{9,11},{10,... | collective-permute-start | bytes 294920 | tf_op jit(solution)/shard_map/ppermute | solution.py:484
  111.7 0.8 collective-permute-done.22.refs_3_
  112.5 3.7 %collective-permute-done.20.refs_1_ = bf16[96,512]{1,0:T(8,128)(2,1)S(1)} collective-permute-done((bf16[96,512]{1,0:T(8,128)(2,1)S(1)}, bf16[96,512]{1,0:T(8,128)(2,1)S(1)}, u32[]{:S(2)}, u32[]{:S(2)}) %collective-permute-start.20) | collective-permute-done | bytes 98336 | tf_op jit(solution)/shard_map/ppermute | solution.py:484
  116.3 4.0 %output.1 = bf16[96,2048]{1,0:T(8,128)(2,1)} custom-call(bf16[96,512]{1,0:T(8,128)(2,1)S(1)} %pad_maximum_fusion.refs_0_, bf16[96,512]{1,0:T(8,128)(2,1)S(1)} %collective-permute-done.20.refs_1_, bf16[96,512]{1,0:T(8,128)(2,1)S(1)} %collective-permute-done.21.refs_2_, bf16[96,512]{1,0:T(8,128)(2,1)S(1)} %collective-permute-done.22.refs_3_, ...), custom_call_target="tpu_custom_call" | custom-call | flops 805306368 | bytes 8000000 | tf_op jit(solution)/shard_map/output/pallas_call | solution.py:618
  (48 shorter events, 0.2 us)
Async XLA Ops:
  0.0 9.9 %copy-start.1 = (bf16[96,2048]{1,0:T(8,128)(2,1)S(1)}, bf16[96,2048]{1,0:T(8,128)(2,1)}, u32[]{:S(2)}) copy-start(bf16[96,2048]{1,0:T(8,128)(2,1)} %refs_8_.3) | copy-start | bytes 1179652
  0.0 22.0 %copy-start = (bf16[512,2048]{1,0:T(8,128)(2,1)S(1)}, bf16[512,2048]{1,0:T(8,128)(2,1)}, u32[]{:S(2)}) copy-start(bf16[512,2048]{1,0:T(8,128)(2,1)} %refs_4_.3) | copy-start | bytes 6291460
  2.1 4.9 %collective-permute-start.3 = (f32[8,512]{1,0:T(8,128)}, f32[8,512]{1,0:T(8,128)S(1)}, u32[]{:S(2)}, u32[]{:S(2)}) collective-permute-start(f32[8,512]{1,0:T(8,128)} %modulation.1), channel_id=1, source_target_pairs={{0,4},{1,5},{2,6},{3,7},{4,0},{5,1},{6,2},{7,3},{8,12},{9,13},{10,... | collective-permute-start | bytes 49160 | tf_op jit(solution)/shard_map/ppermute | solution.py:484
  7.8 3.8 %collective-permute-start.4 = (f32[8,512]{1,0:T(8,128)S(1)}, f32[8,512]{1,0:T(8,128)S(1)}, u32[]{:S(2)}, u32[]{:S(2)}) collective-permute-start(f32[8,512]{1,0:T(8,128)S(1)} %add.50), channel_id=1, source_target_pairs={{0,8},{1,9},{2,10},{3,11},{4,12},{5,13},{6,14},{7,15},{8,0},{9,1},... | collective-permute-start | bytes 49160 | tf_op jit(solution)/shard_map/ppermute | solution.py:484
  9.9 16.2 %collective-permute-start = (bf16[96,2048]{1,0:T(8,128)(2,1)S(1)}, bf16[96,2048]{1,0:T(8,128)(2,1)S(1)}, u32[]{:S(2)}, u32[]{:S(2)}) collective-permute-start(bf16[96,2048]{1,0:T(8,128)(2,1)S(1)} %copy-done.1), channel_id=1, source_target_pairs={{0,2},{1,3},{2,0},{3,1},{4,6},{5,7},{6,4},{7,5},{8,10},{9,11},{10,... | collective-permute-start | bytes 1179656 | tf_op jit(solution)/shard_map/ppermute | solution.py:484
  11.4 16.1 %collective-permute-start.1 = (bf16[96,2048]{1,0:T(8,128)(2,1)S(1)}, bf16[96,2048]{1,0:T(8,128)(2,1)S(1)}, u32[]{:S(2)}, u32[]{:S(2)}) collective-permute-start(bf16[96,2048]{1,0:T(8,128)(2,1)S(1)} %copy-done.1), channel_id=1, source_target_pairs={{0,1},{1,0},{2,3},{3,2},{4,5},{5,4},{6,7},{7,6},{8,9},{9,8},{10,11... | collective-permute-start | bytes 1179656 | tf_op jit(solution)/shard_map/ppermute | solution.py:484
  11.6 4.8 %collective-permute-start.5 = (f32[8,512]{1,0:T(8,128)S(1)}, f32[8,512]{1,0:T(8,128)S(1)}, u32[]{:S(2)}, u32[]{:S(2)}) collective-permute-start(f32[8,512]{1,0:T(8,128)S(1)} %add.51), channel_id=1, source_target_pairs={{0,16},{1,17},{2,18},{3,19},{4,20},{5,21},{6,22},{7,23},{8,24},{9,... | collective-permute-start | bytes 49160 | tf_op jit(solution)/shard_map/ppermute | solution.py:484
  22.0 55.8 %collective-permute-start.23 = (bf16[512,2048]{1,0:T(8,128)(2,1)S(1)}, bf16[512,2048]{1,0:T(8,128)(2,1)}, u32[]{:S(2)}, u32[]{:S(2)}) collective-permute-start(bf16[512,2048]{1,0:T(8,128)(2,1)S(1)} %copy-done), channel_id=1, source_target_pairs={{0,2},{1,3},{2,0},{3,1},{4,6},{5,7},{6,4},{7,5},{8,10},{9,11},{10,... | collective-permute-start | bytes 6291464 | tf_op jit(solution)/shard_map/ppermute | solution.py:484
  26.0 1.7 %copy-start.4 = (bf16[96,2048]{1,0:T(8,128)(2,1)}, bf16[96,2048]{1,0:T(8,128)(2,1)S(1)}, u32[]{:S(2)}) copy-start(bf16[96,2048]{1,0:T(8,128)(2,1)S(1)} %collective-permute-done.refs_1_) | copy-start | bytes 1179652
  26.0 1.7 %collective-permute-start.2 = (bf16[96,2048]{1,0:T(8,128)(2,1)S(1)}, bf16[96,2048]{1,0:T(8,128)(2,1)S(1)}, u32[]{:S(2)}, u32[]{:S(2)}) collective-permute-start(bf16[96,2048]{1,0:T(8,128)(2,1)S(1)} %collective-permute-done.refs_1_), channel_id=1, source_target_pairs={{0,1},{1,0},{2,3},{3,2},{4,5},{5,4},{6,7},{7,6},{8,9},{9,8},{10,11... | collective-permute-start | bytes 1179656 | tf_op jit(solution)/shard_map/ppermute | solution.py:484
  27.4 0.8 copy-start.5
  27.7 0.7 copy-start.6
  37.1 6.0 %collective-permute-start.12 = (bf16[1280,128]{1,0:T(8,128)(2,1)}, bf16[1280,128]{1,0:T(8,128)(2,1)S(1)}, u32[]{:S(2)}, u32[]{:S(2)}) collective-permute-start(bf16[1280,128]{1,0:T(8,128)(2,1)} %get-tuple-element.26), channel_id=1, source_target_pairs={{0,0},{1,8},{2,2},{3,10},{4,4},{5,12},{6,6},{7,14},{8,1},{9,9},{10... | collective-permute-start | bytes 983048 | tf_op jit(solution)/shard_map/ppermute | solution.py:484
  38.7 8.5 %collective-permute-start.13 = (bf16[1280,128]{1,0:T(8,128)(2,1)}, bf16[1280,128]{1,0:T(8,128)(2,1)S(1)}, u32[]{:S(2)}, u32[]{:S(2)}) collective-permute-start(bf16[1280,128]{1,0:T(8,128)(2,1)} %get-tuple-element.27), channel_id=1, source_target_pairs={{0,4},{1,12},{2,6},{3,14},{4,0},{5,8},{6,2},{7,10},{8,5},{9,13},{1... | collective-permute-start | bytes 983048 | tf_op jit(solution)/shard_map/ppermute | solution.py:484
  40.3 12.3 %collective-permute-start.6 = (bf16[384,128]{1,0:T(8,128)(2,1)}, bf16[384,128]{1,0:T(8,128)(2,1)S(1)}, u32[]{:S(2)}, u32[]{:S(2)}) collective-permute-start(bf16[384,128]{1,0:T(8,128)(2,1)} %get-tuple-element.22), channel_id=1, source_target_pairs={{0,16},{1,24},{2,18},{3,26},{4,20},{5,28},{6,22},{7,30},{8,17},{9,... | collective-permute-start | bytes 294920 | tf_op jit(solution)/shard_map/ppermute | solution.py:484
  42.9 12.9 %collective-permute-start.7 = (bf16[384,128]{1,0:T(8,128)(2,1)}, bf16[384,128]{1,0:T(8,128)(2,1)S(1)}, u32[]{:S(2)}, u32[]{:S(2)}) collective-permute-start(bf16[384,128]{1,0:T(8,128)(2,1)} %get-tuple-element.23), channel_id=1, source_target_pairs={{0,20},{1,28},{2,22},{3,30},{4,16},{5,24},{6,18},{7,26},{8,21},{9,... | collective-permute-start | bytes 294920 | tf_op jit(solution)/shard_map/ppermute | solution.py:484
  43.1 34.2 %collective-permute-start.14 = (bf16[1280,128]{1,0:T(8,128)(2,1)S(1)}, bf16[1280,128]{1,0:T(8,128)(2,1)S(1)}, u32[]{:S(2)}, u32[]{:S(2)}) collective-permute-start(bf16[1280,128]{1,0:T(8,128)(2,1)S(1)} %collective-permute-done.12.refs_2_.refs_4_.refs_0_), channel_id=1, source_target_pairs={{0,1},{1,0},{2,3},{3,2},{4,5},{5,4},{6,7},{7,6},{8,9},{9,8},{10,11... | collective-permute-start | bytes 983048 | tf_op jit(solution)/shard_map/ppermute | solution.py:484
  47.3 30.6 %collective-permute-start.15 = (bf16[1280,128]{1,0:T(8,128)(2,1)S(1)}, bf16[1280,128]{1,0:T(8,128)(2,1)S(1)}, u32[]{:S(2)}, u32[]{:S(2)}) collective-permute-start(bf16[1280,128]{1,0:T(8,128)(2,1)S(1)} %collective-permute-done.13.refs_3_.refs_5_.refs_1_), channel_id=1, source_target_pairs={{0,1},{1,0},{2,3},{3,2},{4,5},{5,4},{6,7},{7,6},{8,9},{9,8},{10,11... | collective-permute-start | bytes 983048 | tf_op jit(solution)/shard_map/ppermute | solution.py:484
  52.6 19.7 %collective-permute-start.8 = (bf16[896,128]{1,0:T(8,128)(2,1)}, bf16[896,128]{1,0:T(8,128)(2,1)S(1)}, u32[]{:S(2)}, u32[]{:S(2)}) collective-permute-start(bf16[896,128]{1,0:T(8,128)(2,1)} %get-tuple-element.24), channel_id=1, source_target_pairs={{0,16},{1,24},{2,18},{3,26},{4,20},{5,28},{6,22},{7,30},{8,17},{9,... | collective-permute-start | bytes 688136 | tf_op jit(solution)/shard_map/ppermute | solution.py:484
  55.8 31.5 %copy-start.3 = (f32[8,2048]{1,0:T(8,128)S(1)}, f32[8,2048]{1,0:T(8,128)}, u32[]{:S(2)}) copy-start(f32[8,2048]{1,0:T(8,128)} %all_gather.3.refs_5_.refs_8_.refs_9_) | copy-start | bytes 196612
  55.8 21.5 %collective-permute-start.9 = (bf16[896,128]{1,0:T(8,128)(2,1)}, bf16[896,128]{1,0:T(8,128)(2,1)S(1)}, u32[]{:S(2)}, u32[]{:S(2)}) collective-permute-start(bf16[896,128]{1,0:T(8,128)(2,1)} %get-tuple-element.25), channel_id=1, source_target_pairs={{0,20},{1,28},{2,22},{3,30},{4,16},{5,24},{6,18},{7,26},{8,21},{9,... | collective-permute-start | bytes 688136 | tf_op jit(solution)/shard_map/ppermute | solution.py:484
  72.3 44.0 %collective-permute-start.24 = (bf16[512,2048]{1,0:T(8,128)(2,1)S(1)}, bf16[512,2048]{1,0:T(8,128)(2,1)S(1)}, u32[]{:S(2)}, u32[]{:S(2)}) collective-permute-start(bf16[512,2048]{1,0:T(8,128)(2,1)S(1)} %copy-done), channel_id=1, source_target_pairs={{0,1},{1,0},{2,3},{3,2},{4,5},{5,4},{6,7},{7,6},{8,9},{9,8},{10,11... | collective-permute-start | bytes 6291464 | tf_op jit(solution)/shard_map/ppermute | solution.py:484
  77.3 10.0 %collective-permute-start.10 = (bf16[896,128]{1,0:T(8,128)(2,1)S(1)}, bf16[896,128]{1,0:T(8,128)(2,1)S(1)}, u32[]{:S(2)}, u32[]{:S(2)}) collective-permute-start(bf16[896,128]{1,0:T(8,128)(2,1)S(1)} %collective-permute-done.8.refs_2_), channel_id=1, source_target_pairs={{0,1},{1,0},{2,3},{3,2},{4,5},{5,4},{6,7},{7,6},{8,9},{9,8},{10,11... | collective-permute-start | bytes 688136 | tf_op jit(solution)/shard_map/ppermute | solution.py:484
  77.3 10.0 %collective-permute-start.11 = (bf16[896,128]{1,0:T(8,128)(2,1)S(1)}, bf16[896,128]{1,0:T(8,128)(2,1)S(1)}, u32[]{:S(2)}, u32[]{:S(2)}) collective-permute-start(bf16[896,128]{1,0:T(8,128)(2,1)S(1)} %collective-permute-done.9.refs_3_), channel_id=1, source_target_pairs={{0,1},{1,0},{2,3},{3,2},{4,5},{5,4},{6,7},{7,6},{8,9},{9,8},{10,11... | collective-permute-start | bytes 688136 | tf_op jit(solution)/shard_map/ppermute | solution.py:484
  77.8 38.4 %collective-permute-start.25 = (bf16[512,2048]{1,0:T(8,128)(2,1)}, bf16[512,2048]{1,0:T(8,128)(2,1)S(1)}, u32[]{:S(2)}, u32[]{:S(2)}) collective-permute-start(bf16[512,2048]{1,0:T(8,128)(2,1)} %collective-permute-done.23.refs_5_), channel_id=1, source_target_pairs={{0,1},{1,0},{2,3},{3,2},{4,5},{5,4},{6,7},{7,6},{8,9},{9,8},{10,11... | collective-permute-start | bytes 6291464 | tf_op jit(solution)/shard_map/ppermute | solution.py:484
  92.6 9.6 %collective-permute-start.16 = (bf16[384,128]{1,0:T(8,128)(2,1)S(1)}, bf16[384,128]{1,0:T(8,128)(2,1)S(1)}, u32[]{:S(2)}, u32[]{:S(2)}) collective-permute-start(bf16[384,128]{1,0:T(8,128)(2,1)S(1)} %get-tuple-element.30), channel_id=1, source_target_pairs={{0,16},{1,24},{2,18},{3,26},{4,20},{5,28},{6,22},{7,30},{8,17},{9,... | collective-permute-start | bytes 294920 | tf_op jit(solution)/shard_map/ppermute | solution.py:484
  94.0 10.7 %collective-permute-start.17 = (bf16[384,128]{1,0:T(8,128)(2,1)S(1)}, bf16[384,128]{1,0:T(8,128)(2,1)S(1)}, u32[]{:S(2)}, u32[]{:S(2)}) collective-permute-start(bf16[384,128]{1,0:T(8,128)(2,1)S(1)} %get-tuple-element.31), channel_id=1, source_target_pairs={{0,20},{1,28},{2,22},{3,30},{4,16},{5,24},{6,18},{7,26},{8,21},{9,... | collective-permute-start | bytes 294920 | tf_op jit(solution)/shard_map/ppermute | solution.py:484
  96.3 20.0 %copy-start.2 = (bf16[96,2048]{1,0:T(8,128)(2,1)S(1)}, bf16[96,2048]{1,0:T(8,128)(2,1)}, u32[]{:S(2)}) copy-start(bf16[96,2048]{1,0:T(8,128)(2,1)} %refs_8_.3) | copy-start | bytes 1179652
  101.5 3.1 %collective-permute-start.18 = (bf16[384,128]{1,0:T(8,128)(2,1)S(1)}, bf16[384,128]{1,0:T(8,128)(2,1)S(1)}, u32[]{:S(2)}, u32[]{:S(2)}) collective-permute-start(bf16[384,128]{1,0:T(8,128)(2,1)S(1)} %get-tuple-element.34), channel_id=1, source_target_pairs={{0,0},{1,8},{2,2},{3,10},{4,4},{5,12},{6,6},{7,14},{8,1},{9,9},{10... | collective-permute-start | bytes 294920 | tf_op jit(solution)/shard_map/ppermute | solution.py:484
  102.2 4.7 %collective-permute-start.19 = (bf16[384,128]{1,0:T(8,128)(2,1)S(1)}, bf16[384,128]{1,0:T(8,128)(2,1)S(1)}, u32[]{:S(2)}, u32[]{:S(2)}) collective-permute-start(bf16[384,128]{1,0:T(8,128)(2,1)S(1)} %get-tuple-element.35), channel_id=1, source_target_pairs={{0,4},{1,12},{2,6},{3,14},{4,0},{5,8},{6,2},{7,10},{8,5},{9,13},{1... | collective-permute-start | bytes 294920 | tf_op jit(solution)/shard_map/ppermute | solution.py:484
  106.9 5.6 %collective-permute-start.22 = (bf16[96,512]{1,0:T(8,128)(2,1)S(1)}, bf16[96,512]{1,0:T(8,128)(2,1)S(1)}, u32[]{:S(2)}, u32[]{:S(2)}) collective-permute-start(bf16[96,512]{1,0:T(8,128)(2,1)S(1)} %pad_maximum_fusion.3), channel_id=1, source_target_pairs={{0,3},{1,2},{2,1},{3,0},{4,7},{5,6},{6,5},{7,4},{8,11},{9,10},{10,... | collective-permute-start | bytes 294920 | tf_op jit(solution)/shard_map/ppermute | solution.py:484
  110.1 2.4 %collective-permute-start.21 = (bf16[96,512]{1,0:T(8,128)(2,1)S(1)}, bf16[96,512]{1,0:T(8,128)(2,1)S(1)}, u32[]{:S(2)}, u32[]{:S(2)}) collective-permute-start(bf16[96,512]{1,0:T(8,128)(2,1)S(1)} %pad_maximum_fusion.2), channel_id=1, source_target_pairs={{0,1},{1,0},{2,3},{3,2},{4,5},{5,4},{6,7},{7,6},{8,9},{9,8},{10,11... | collective-permute-start | bytes 294920 | tf_op jit(solution)/shard_map/ppermute | solution.py:484
  110.2 6.1 %collective-permute-start.20 = (bf16[96,512]{1,0:T(8,128)(2,1)S(1)}, bf16[96,512]{1,0:T(8,128)(2,1)S(1)}, u32[]{:S(2)}, u32[]{:S(2)}) collective-permute-start(bf16[96,512]{1,0:T(8,128)(2,1)S(1)} %pad_maximum_fusion.1), channel_id=1, source_target_pairs={{0,2},{1,3},{2,0},{3,1},{4,6},{5,7},{6,4},{7,5},{8,10},{9,11},{10,... | collective-permute-start | bytes 294920 | tf_op jit(solution)/shard_map/ppermute | solution.py:484

commit v3 on v2

--- a/solution.py
+++ b/solution.py
@@ -245,19 +245,36 @@
     out[7:8, :] = jnp.zeros_like(gain)
 
 
+def hold_kernel(count, *refs):
+    sources, outs, sems = refs[:count], refs[count : 2 * count], refs[2 * count]
+    loads = [
+        pltpu.make_async_copy(source, out, sems.at[index])
+        for index, (source, out) in enumerate(zip(sources, outs))
+    ]
+    for load in loads:
+        load.start()
+    for load in loads:
+        load.wait()
+
+
+def hold(arrays, mebibytes):
+    return pl.pallas_call(
+        functools.partial(hold_kernel, len(arrays)),
+        out_shape=[jax.ShapeDtypeStruct(a.shape, a.dtype) for a in arrays],
+        in_specs=[HBM] * len(arrays),
+        out_specs=vmem(len(arrays)),
+        scratch_shapes=[pltpu.SemaphoreType.DMA((len(arrays),))],
+        compiler_params=params(mebibytes),
+        cost_estimate=cost(10**8, 8 * 10**6),
+        name="hold",
+    )(*arrays)
+
+
 def project_kernel(head_count, *refs):
     slots = refs[0:4]
     context, mods, cos_t, sin_t, query_w, key_w, value_w = refs[4:11]
     far_queries, far_pairs, near = refs[11:13], refs[13:15], refs[15:17]
-    hidden, ready, query_v, key_v, value_v, sems = refs[17:]
-    loads = [
-        pltpu.make_async_copy(source, held, sems.at[index])
-        for index, (source, held) in enumerate(
-            ((query_w, query_v), (key_w, key_v), (value_w, value_v))
-        )
-    ]
-    for load in loads:
-        load.start()
+    hidden, ready = refs[17:]
     own_rows = slots[0].shape[0]
     tok = 4 * own_rows
     ctx = context.shape[0]
@@ -290,11 +307,7 @@
         return jnp.where(lane < HEAD_DIM, first, pltpu.roll(second, HEAD_DIM, 1))
 
     per_tile = LANES // HEAD_DIM
-    for load, weight, base, count in (
-        (loads[0], query_v, 0, tok),
-        (loads[1], key_v, tok, tok + ctx),
-    ):
-        load.wait()
+    for weight, base, count in ((query_w, 0, tok), (key_w, tok, tok + ctx)):
         first = dot(hidden[:count, :], weight[0])
         second = dot(hidden[:count, :], weight[1])
         for head in range(head_count):
@@ -305,9 +318,8 @@
                 ready[head, base + tok : base + count, :] = whole[tok:].astype(jnp.bfloat16)
     base = 2 * tok + ctx
     wide = 2 * VALUE_DIM
-    loads[2].wait()
     for pair in range(head_count // 2):
-        both = dot(hidden[...], value_v[:, pair * wide : (pair + 1) * wide]).astype(jnp.bfloat16)
+        both = dot(hidden[...], value_w[:, pair * wide : (pair + 1) * wide]).astype(jnp.bfloat16)
         ready[2 * pair, base:, :] = both[:, :VALUE_DIM]
         ready[2 * pair + 1, base:, :] = both[:, VALUE_DIM:]
     sp = lax.axis_index("sp")
@@ -428,22 +440,15 @@
 
 def output_kernel(*refs):
     terms, weights = refs[0:4], refs[4:8]
-    latent, mods, out, ordered, held, sems = refs[8:]
-    loads = [
-        pltpu.make_async_copy(weight, held.at[index], sems.at[index])
-        for index, weight in enumerate(weights)
-    ]
-    for load in loads:
-        load.start()
+    latent, mods, out, ordered = refs[8:]
     sp = lax.axis_index("sp")
     for index, term in enumerate(terms):
         for slot, (e, j) in enumerate(SLOTS):
             place = pl.multiple_of(slot_head(sp, e, j) * VALUE_DIM, VALUE_DIM)
             ordered[index, :, pl.ds(place, VALUE_DIM)] = term[:, slot * VALUE_DIM : (slot + 1) * VALUE_DIM]
     total = None
-    for index, load in enumerate(loads):
-        load.wait()
-        group = jnp.dot(ordered[index], held[index], preferred_element_type=jnp.float32)
+    for index, weight in enumerate(weights):
+        group = jnp.dot(ordered[index], weight[...], preferred_element_type=jnp.float32)
         group = group.astype(jnp.bfloat16).astype(jnp.float32)
         total = group if total is None else total + group
     out[...] = (latent[...].astype(jnp.float32) + mods[4:5, :] * total).astype(jnp.bfloat16)
@@ -494,6 +499,8 @@
 
     from_owner = to_owner
 
+    *held_weights, held_context = hold((query_weight, key_weight, value_weight, context), 47)
+
     mod_part = pl.pallas_call(
         modulation_kernel,
         out_shape=jax.ShapeDtypeStruct((8, shift_weight.shape[1]), f32),
@@ -549,20 +556,16 @@
     messages = pl.pallas_call(
         functools.partial(project_kernel, heads),
         out_shape=[block(tok)] * 2 + [block(2 * part)] * 2 + [block(tok + 2 * part)] * 2,
-        in_specs=vmem(8) + [HBM] * 3,
+        in_specs=vmem(11),
         out_specs=vmem(6),
         scratch_shapes=[
             pltpu.VMEM((part, width), bf16),
             pltpu.VMEM((heads, tok + 2 * part, LANES), bf16),
-            pltpu.VMEM(query_weight.shape, bf16),
-            pltpu.VMEM(key_weight.shape, bf16),
-            pltpu.VMEM(value_weight.shape, bf16),
-            pltpu.SemaphoreType.DMA((3,)),
         ],
-        compiler_params=params(56),
+        compiler_params=params(28),
         cost_estimate=cost(2 * part * width * 6 * heads * HEAD_DIM, 8 * 10**6),
         name="project",
-    )(*slots, context, mods, cos_t, sin_t, query_weight, key_weight, value_weight)
+    )(*slots, held_context, mods, cos_t, sin_t, *held_weights)
 
     far_queries = [hop(messages[j], to_owner(1, j)) for j in range(2)]
     near = [hop(messages[4 + j], to_owner(0, j)) for j in range(2)]
@@ -618,12 +621,10 @@
     return pl.pallas_call(
         output_kernel,
         out_shape=jax.ShapeDtypeStruct(latent.shape, bf16),
-        in_specs=vmem(4) + [HBM] * 4 + vmem(2),
+        in_specs=vmem(10),
         out_specs=vmem(1)[0],
         scratch_shapes=[
             pltpu.VMEM((4, own_rows, heads * VALUE_DIM), bf16),
-            pltpu.VMEM((4,) + out_weight.shape, bf16),
-            pltpu.SemaphoreType.DMA((4,)),
         ],
         compiler_params=params(24),
         cost_estimate=cost(2 * own_rows * width * width, 8 * 10**6),

time: 121 us -> 116 us (0.959)
  Pallas kernels: 34.6 us -> 33.1 us
    pallas_call x1, Pallas kernels: 8.61 us -> 4.29 us  [local_owner(): pl.pallas_call(functools.partial(project_kernel, heads), out_shape=[block...]
    pallas_call x0 -> x1, Pallas kernels: none -> 2.89 us  [hold(): pl.pallas_call(functools.partial(hold_kernel, len(arrays)), out_shape=[ja...]
  transfers between devices with their start and end apart: 26 -> 26, of which waited for: 10 -> 9; matrix products, arithmetic and copies ran while one was open for 3% -> 2% of each run, Pallas kernels for 24% -> 23%
where the time goes in v3:
time: 116 us
  starting transfers between devices  42 us (36%)
  Pallas kernels  33.1 us (29%)
  waiting for transfers between devices  31.6 us (27%)
  blocking collectives  5.22 us (4%)
  other arithmetic  3.25 us (3%)
    ppermute x26, starting transfers between devices, hop(): return lax.ppermute(array, axes, pairs)  42 us
    ppermute x26, waiting for transfers between devices, hop(): return lax.ppermute(array, axes, pairs)  31.6 us
    pallas_call x3, Pallas kernels, attend(): pl.pallas_call(functools.partial(attention_kernel, heads, tok, part, not...  19.9 us
    all_gather x1, blocking collectives, local_owner(): mods = lax.all_gather(mod_part, 'tp', axis=1, tiled=True)  5.22 us
    pallas_call x1, Pallas kernels, local_owner(): pl.pallas_call(functools.partial(project_kernel, heads), out_shape=[block...  4.29 us
    pallas_call x1, Pallas kernels, local_owner(): pl.pallas_call(output_kernel, out_shape=jax.ShapeDtypeStruct(latent.shape...  3.92 us
    pallas_call x1, Pallas kernels, hold(): pl.pallas_call(functools.partial(hold_kernel, len(arrays)), out_shape=[ja...  2.89 us
  transfers between devices with their start and end apart: 26, of which 9 were waited for; matrix products, arithmetic and copies ran while one was open for 2% of the time, Pallas kernels for 23%

profile of v3, /device:TPU:0, one launch (start us, length us, event | category | flops | bytes accessed | tf_op | source)
XLA Modules:
  0.0 115.6 jit_solution(10242477294099355320)
XLA Ops:
  0.0 2.1 %modulation.1 = f32[8,512]{1,0:T(8,128)} custom-call(f32[4]{0:T(128)} %lam.1, f32[1,2048]{1,0:T(1,128)} %bitcast.3, f32[1,2048]{1,0:T(1,128)} %bitcast.4, bf16[256,512]{1,0:T(8,128)(2,1)} %shift_w.1, bf16[256,512]{1,0:T(8,128)(2,1)} %scale_w.1, bf16[256,512]{1,0:T(8,128)(2,1)} %gate_w.1, f32[1,512]{1,0:T(1,128)} %bitcast.5), custom_call_target="tpu_custom_call" | custom-call | flops 1000000000 | bytes 1000000 | tf_op jit(solution)/shard_map/modulation/pallas_call | solution.py:504
  2.1 3.0 %collective-permute-start.3 = (f32[8,512]{1,0:T(8,128)}, f32[8,512]{1,0:T(8,128)S(1)}, u32[]{:S(2)}, u32[]{:S(2)}) collective-permute-start(f32[8,512]{1,0:T(8,128)} %modulation.1), channel_id=1, source_target_pairs={{0,4},{1,5},{2,6},{3,7},{4,0},{5,1},{6,2},{7,3},{8,12},{9,13},{10,... | collective-permute-start | bytes 49160 | tf_op jit(solution)/shard_map/ppermute | solution.py:489
  5.1 1.9 %collective-permute-done.3 = f32[8,512]{1,0:T(8,128)S(1)} collective-permute-done((f32[8,512]{1,0:T(8,128)}, f32[8,512]{1,0:T(8,128)S(1)}, u32[]{:S(2)}, u32[]{:S(2)}) %collective-permute-start.3) | collective-permute-done | bytes 16416 | tf_op jit(solution)/shard_map/ppermute | solution.py:489
  7.1 0.7 add.50
  7.8 2.1 %collective-permute-start.4 = (f32[8,512]{1,0:T(8,128)S(1)}, f32[8,512]{1,0:T(8,128)S(1)}, u32[]{:S(2)}, u32[]{:S(2)}) collective-permute-start(f32[8,512]{1,0:T(8,128)S(1)} %add.50), channel_id=1, source_target_pairs={{0,8},{1,9},{2,10},{3,11},{4,12},{5,13},{6,14},{7,15},{8,0},{9,1},... | collective-permute-start | bytes 49160 | tf_op jit(solution)/shard_map/ppermute | solution.py:489
  9.9 1.5 %collective-permute-start = (bf16[96,2048]{1,0:T(8,128)(2,1)S(1)}, bf16[96,2048]{1,0:T(8,128)(2,1)S(1)}, u32[]{:S(2)}, u32[]{:S(2)}) collective-permute-start(bf16[96,2048]{1,0:T(8,128)(2,1)S(1)} %copy-done.1), channel_id=1, source_target_pairs={{0,2},{1,3},{2,0},{3,1},{4,6},{5,7},{6,4},{7,5},{8,10},{9,11},{10,... | collective-permute-start | bytes 1179656 | tf_op jit(solution)/shard_map/ppermute | solution.py:489
  11.4 0.2 collective-permute-done.4
  11.6 3.0 %collective-permute-start.5 = (f32[8,512]{1,0:T(8,128)S(1)}, f32[8,512]{1,0:T(8,128)S(1)}, u32[]{:S(2)}, u32[]{:S(2)}) collective-permute-start(f32[8,512]{1,0:T(8,128)S(1)} %add.51), channel_id=1, source_target_pairs={{0,16},{1,17},{2,18},{3,19},{4,20},{5,21},{6,22},{7,23},{8,24},{9,... | collective-permute-start | bytes 49160 | tf_op jit(solution)/shard_map/ppermute | solution.py:489
  14.6 1.7 %collective-permute-done.5 = f32[8,512]{1,0:T(8,128)S(1)} collective-permute-done((f32[8,512]{1,0:T(8,128)S(1)}, f32[8,512]{1,0:T(8,128)S(1)}, u32[]{:S(2)}, u32[]{:S(2)}) %collective-permute-start.5) | collective-permute-done | bytes 16416 | tf_op jit(solution)/shard_map/ppermute | solution.py:489
  16.3 5.2 %all_gather.3.refs_5_.refs_8_.refs_9_ = f32[8,2048]{1,0:T(8,128)S(1)} all-gather(f32[8,512]{1,0:T(8,128)S(1)} %add.52), channel_id=1, replica_groups=mesh['sp'=8,'tp'=4] {'tp'}, dimensions={1}, use_global_device_ids=true | all-gather | bytes 81920 | tf_op jit(solution)/shard_map/all_gather | solution.py:530
  21.6 1.8 %collective-permute-start.23 = (bf16[512,2048]{1,0:T(8,128)(2,1)S(1)}, bf16[512,2048]{1,0:T(8,128)(2,1)}, u32[]{:S(2)}, u32[]{:S(2)}) collective-permute-start(bf16[512,2048]{1,0:T(8,128)(2,1)S(1)} %copy-done), channel_id=1, source_target_pairs={{0,2},{1,3},{2,0},{3,1},{4,6},{5,7},{6,4},{7,5},{8,10},{9,11},{10,... | collective-permute-start | bytes 6291464 | tf_op jit(solution)/shard_map/ppermute | solution.py:489
  23.4 0.1 mul.24
  23.5 1.8 %fusion.8 = (f32[384,128]{1,0:T(8,128)S(1)}, f32[384,128]{1,0:T(8,128)S(1)}) fusion(f32[128]{0:T(128)S(1)} %mul.24, s32[384]{0:T(512)S(1)} %get-tuple-element.64, s32[384]{0:T(512)S(1)} %get-tuple-element.65, s32[384]{0:T(512)S(1)} %get-tuple-element.63, s32[384]{0:T(512)S(1)} %get-tuple-element.66, s32[]{:T(128)S(6)} %axis_index.25, s32[]{:T(128)S(6)} %mul.21, ...), kind=kLoop, calls=%fused_computation.22 | loop fusion | flops 2506752 | bytes 401800 | tf_op jit(solution)/shard_map/mul | solution.py:545
  25.3 0.0 collective-permute-done.refs_1_
  25.3 0.1 collective-permute-start.2
  25.4 2.9 %hold.1 = (bf16[2,2048,256]{2,1,0:T(8,128)(2,1)S(1)}, bf16[2,2048,256]{2,1,0:T(8,128)(2,1)S(1)}, bf16[2048,512]{1,0:T(8,128)(2,1)S(1)}, bf16[64,2048]{1,0:T(8,128)(2,1)S(1)}) custom-call(bf16[2,2048,256]{2,1,0:T(8,128)(2,1)} %refs_0_.2, bf16[2,2048,256]{2,1,0:T(8,128)(2,1)} %refs_1_.1, bf16[2048,512]{1,0:T(8,128)(2,1)} %refs_2_.1, bf16[64,2048]{1,0:T(8,128)(2,1)S(1)} %copy-done.2), custom_call_target="tpu_custom_call" | custom-call | flops 100000000 | bytes 8000000 | tf_op jit(solution)/shard_map/hold/pallas_call | solution.py:261
  28.4 0.7 negate_select_fusion.refs_7_
  29.0 0.0 collective-permute-done.1.refs_2_
  29.0 0.0 collective-permute-done.2.refs_3_
  29.0 4.3 %project.1 = (bf16[384,128]{1,0:T(8,128)(2,1)S(1)}, bf16[384,128]{1,0:T(8,128)(2,1)S(1)}, bf16[896,128]{1,0:T(8,128)(2,1)S(1)}, bf16[896,128]{1,0:T(8,128)(2,1)S...) custom-call(bf16[96,2048]{1,0:T(8,128)(2,1)S(1)} %copy-done.1, ...), custom_call_target="tpu_custom_call" | custom-call | flops 2818572288 | bytes 8000000 | tf_op jit(solution)/shard_map/project/pallas_call | solution.py:556
  33.3 0.9 collective-permute-start.12
  34.2 1.6 %collective-permute-start.13 = (bf16[1280,128]{1,0:T(8,128)(2,1)S(1)}, bf16[1280,128]{1,0:T(8,128)(2,1)S(1)}, u32[]{:S(2)}, u32[]{:S(2)}) collective-permute-start(bf16[1280,128]{1,0:T(8,128)(2,1)S(1)} %get-tuple-element.35), channel_id=1, source_target_pairs={{0,4},{1,12},{2,6},{3,14},{4,0},{5,8},{6,2},{7,10},{8,5},{9,13},{1... | collective-permute-start | bytes 983048 | tf_op jit(solution)/shard_map/ppermute | solution.py:489
  35.8 2.6 %collective-permute-start.6 = (bf16[384,128]{1,0:T(8,128)(2,1)S(1)}, bf16[384,128]{1,0:T(8,128)(2,1)S(1)}, u32[]{:S(2)}, u32[]{:S(2)}) collective-permute-start(bf16[384,128]{1,0:T(8,128)(2,1)S(1)} %get-tuple-element.30), channel_id=1, source_target_pairs={{0,16},{1,24},{2,18},{3,26},{4,20},{5,28},{6,22},{7,30},{8,17},{9,... | collective-permute-start | bytes 294920 | tf_op jit(solution)/shard_map/ppermute | solution.py:489
  38.4 0.3 collective-permute-start.7
  38.7 5.2 %collective-permute-start.14 = (bf16[1280,128]{1,0:T(8,128)(2,1)S(1)}, bf16[1280,128]{1,0:T(8,128)(2,1)S(1)}, u32[]{:S(2)}, u32[]{:S(2)}) collective-permute-start(bf16[1280,128]{1,0:T(8,128)(2,1)S(1)} %collective-permute-done.12.refs_2_.refs_4_.refs_0_), channel_id=1, source_target_pairs={{0,1},{1,0},{2,3},{3,2},{4,5},{5,4},{6,7},{7,6},{8,9},{9,8},{10,11... | collective-permute-start | bytes 983048 | tf_op jit(solution)/shard_map/ppermute | solution.py:489
  43.8 0.0 collective-permute-done.13.refs_3_.refs_5_.refs_1_
  43.8 4.9 %collective-permute-start.15 = (bf16[1280,128]{1,0:T(8,128)(2,1)S(1)}, bf16[1280,128]{1,0:T(8,128)(2,1)S(1)}, u32[]{:S(2)}, u32[]{:S(2)}) collective-permute-start(bf16[1280,128]{1,0:T(8,128)(2,1)S(1)} %collective-permute-done.13.refs_3_.refs_5_.refs_1_), channel_id=1, source_target_pairs={{0,1},{1,0},{2,3},{3,2},{4,5},{5,4},{6,7},{7,6},{8,9},{9,8},{10,11... | collective-permute-start | bytes 983048 | tf_op jit(solution)/shard_map/ppermute | solution.py:489
  48.7 2.6 %collective-permute-start.8 = (bf16[896,128]{1,0:T(8,128)(2,1)S(1)}, bf16[896,128]{1,0:T(8,128)(2,1)S(1)}, u32[]{:S(2)}, u32[]{:S(2)}) collective-permute-start(bf16[896,128]{1,0:T(8,128)(2,1)S(1)} %get-tuple-element.32), channel_id=1, source_target_pairs={{0,16},{1,24},{2,18},{3,26},{4,20},{5,28},{6,22},{7,30},{8,17},{9,... | collective-permute-start | bytes 688136 | tf_op jit(solution)/shard_map/ppermute | solution.py:489
  51.4 0.8 collective-permute-start.9
  52.2 15.7 %collective-permute-done.8.refs_2_ = bf16[896,128]{1,0:T(8,128)(2,1)S(1)} collective-permute-done((bf16[896,128]{1,0:T(8,128)(2,1)S(1)}, bf16[896,128]{1,0:T(8,128)(2,1)S(1)}, u32[]{:S(2)}, u32[]{:S(2)}) %collective-permute-start.8) | collective-permute-done | bytes 229408 | tf_op jit(solution)/shard_map/ppermute | solution.py:489
  68.0 4.8 %collective-permute-done.9.refs_3_ = bf16[896,128]{1,0:T(8,128)(2,1)S(1)} collective-permute-done((bf16[896,128]{1,0:T(8,128)(2,1)S(1)}, bf16[896,128]{1,0:T(8,128)(2,1)S(1)}, u32[]{:S(2)}, u32[]{:S(2)}) %collective-permute-start.9) | collective-permute-done | bytes 229408 | tf_op jit(solution)/shard_map/ppermute | solution.py:489
  72.7 0.5 collective-permute-start.11
  73.2 0.1 collective-permute-start.25
  73.3 9.4 %attention.3 = (f32[1536,128]{1,0:T(8,128)S(1)}, f32[1536,128]{1,0:T(8,128)S(1)}, f32[1536,128]{1,0:T(8,128)S(1)}, f32[1536,128]{1,0:T(8,128)S(1)}) custom-call(bf16[384,128]{1,0:T(8,128)(2,1)S(1)} %collective-permute-done.6.refs_0_, bf16[384,128]{1,0:T(8,128)(2,1)S(1)} %collective-permute-done.7.refs_1_, ...), custom_call_target="tpu_custom_call" | custom-call | flops 5637144576 | bytes 1000000 | tf_op jit(solution)/shard_map/attention/pallas_call | solution.py:584
  82.7 5.3 %attention.4 = (bf16[384,128]{1,0:T(8,128)(2,1)S(1)}, bf16[384,128]{1,0:T(8,128)(2,1)S(1)}) custom-call(bf16[384,128]{1,0:T(8,128)(2,1)S(1)} %collective-permute-done.6.refs_0_, bf16[384,128]{1,0:T(8,128)(2,1)S(1)} %collective-permute-done.7.refs_1_, bf16[896,128]{1,0:T(8,128)(2,1)S(1)} %collective-permute-done.8.refs_2_, ...), custom_call_target="tpu_custom_call" | custom-call | flops 2818572288 | bytes 1000000 | tf_op jit(solution)/shard_map/attention/pallas_call | solution.py:584
  88.0 1.8 %collective-permute-start.16 = (bf16[384,128]{1,0:T(8,128)(2,1)S(1)}, bf16[384,128]{1,0:T(8,128)(2,1)S(1)}, u32[]{:S(2)}, u32[]{:S(2)}) collective-permute-start(bf16[384,128]{1,0:T(8,128)(2,1)S(1)} %get-tuple-element.38), channel_id=1, source_target_pairs={{0,16},{1,24},{2,18},{3,26},{4,20},{5,28},{6,22},{7,30},{8,17},{9,... | collective-permute-start | bytes 294920 | tf_op jit(solution)/shard_map/ppermute | solution.py:489
  89.8 2.1 %collective-permute-start.17 = (bf16[384,128]{1,0:T(8,128)(2,1)S(1)}, bf16[384,128]{1,0:T(8,128)(2,1)S(1)}, u32[]{:S(2)}, u32[]{:S(2)}) collective-permute-start(bf16[384,128]{1,0:T(8,128)(2,1)S(1)} %get-tuple-element.39), channel_id=1, source_target_pairs={{0,20},{1,28},{2,22},{3,30},{4,16},{5,24},{6,18},{7,26},{8,21},{9,... | collective-permute-start | bytes 294920 | tf_op jit(solution)/shard_map/ppermute | solution.py:489
  91.9 5.3 %attention.5 = (bf16[384,128]{1,0:T(8,128)(2,1)S(1)}, bf16[384,128]{1,0:T(8,128)(2,1)S(1)}) custom-call(bf16[1280,128]{1,0:T(8,128)(2,1)S(1)} %collective-permute-done.12.refs_2_.refs_4_.refs_0_, bf16[1280,128]{1,0:T(8,128)(2,1)S(1)} %collective-permute-done.13.refs_3_.refs_5_.refs_1_, bf16[896,128]{1,0:T(8,128)(2,1)S(1)} %collective-permute-done.8.refs_2_, ...), custom_call_target="tpu_custom_call" | custom-call | flops 2818572288 | bytes 1000000 | tf_op jit(solution)/shard_map/attention/pallas_call | solution.py:584
  97.2 0.7 collective-permute-start.18
  97.9 1.9 %collective-permute-start.19 = (bf16[384,128]{1,0:T(8,128)(2,1)S(1)}, bf16[384,128]{1,0:T(8,128)(2,1)S(1)}, u32[]{:S(2)}, u32[]{:S(2)}) collective-permute-start(bf16[384,128]{1,0:T(8,128)(2,1)S(1)} %get-tuple-element.43), channel_id=1, source_target_pairs={{0,4},{1,12},{2,6},{3,14},{4,0},{5,8},{6,2},{7,10},{8,5},{9,13},{1... | collective-permute-start | bytes 294920 | tf_op jit(solution)/shard_map/ppermute | solution.py:489
  99.8 0.5 collective-permute-done.17
  100.3 2.2 %collective-permute-done.19 = bf16[384,128]{1,0:T(8,128)(2,1)S(1)} collective-permute-done((bf16[384,128]{1,0:T(8,128)(2,1)S(1)}, bf16[384,128]{1,0:T(8,128)(2,1)S(1)}, u32[]{:S(2)}, u32[]{:S(2)}) %collective-permute-start.19) | collective-permute-done | bytes 98336 | tf_op jit(solution)/shard_map/ppermute | solution.py:489
  102.6 2.8 %collective-permute-start.22 = (bf16[96,512]{1,0:T(8,128)(2,1)S(1)}, bf16[96,512]{1,0:T(8,128)(2,1)S(1)}, u32[]{:S(2)}, u32[]{:S(2)}) collective-permute-start(bf16[96,512]{1,0:T(8,128)(2,1)S(1)} %pad_maximum_fusion.3), channel_id=1, source_target_pairs={{0,3},{1,2},{2,1},{3,0},{4,7},{5,6},{6,5},{7,4},{8,11},{9,10},{10,... | collective-permute-start | bytes 294920 | tf_op jit(solution)/shard_map/ppermute | solution.py:489
  105.4 0.1 collective-permute-start.21
  105.5 1.6 %collective-permute-start.20 = (bf16[96,512]{1,0:T(8,128)(2,1)S(1)}, bf16[96,512]{1,0:T(8,128)(2,1)S(1)}, u32[]{:S(2)}, u32[]{:S(2)}) collective-permute-start(bf16[96,512]{1,0:T(8,128)(2,1)S(1)} %pad_maximum_fusion.1), channel_id=1, source_target_pairs={{0,2},{1,3},{2,0},{3,1},{4,6},{5,7},{6,4},{7,5},{8,10},{9,11},{10,... | collective-permute-start | bytes 294920 | tf_op jit(solution)/shard_map/ppermute | solution.py:489
  107.1 0.8 collective-permute-done.22.refs_3_
  107.9 3.7 %collective-permute-done.20.refs_1_ = bf16[96,512]{1,0:T(8,128)(2,1)S(1)} collective-permute-done((bf16[96,512]{1,0:T(8,128)(2,1)S(1)}, bf16[96,512]{1,0:T(8,128)(2,1)S(1)}, u32[]{:S(2)}, u32[]{:S(2)}) %collective-permute-start.20) | collective-permute-done | bytes 98336 | tf_op jit(solution)/shard_map/ppermute | solution.py:489
  111.6 3.9 %output.1 = bf16[96,2048]{1,0:T(8,128)(2,1)} custom-call(bf16[96,512]{1,0:T(8,128)(2,1)S(1)} %pad_maximum_fusion.refs_0_, bf16[96,512]{1,0:T(8,128)(2,1)S(1)} %collective-permute-done.20.refs_1_, bf16[96,512]{1,0:T(8,128)(2,1)S(1)} %collective-permute-done.21.refs_2_, bf16[96,512]{1,0:T(8,128)(2,1)S(1)} %collective-permute-done.22.refs_3_, ...), custom_call_target="tpu_custom_call" | custom-call | flops 805306368 | bytes 8000000 | tf_op jit(solution)/shard_map/output/pallas_call | solution.py:621
  (41 shorter events, 0.2 us)
Async XLA Ops:
  0.0 9.9 %copy-start.1 = (bf16[96,2048]{1,0:T(8,128)(2,1)S(1)}, bf16[96,2048]{1,0:T(8,128)(2,1)}, u32[]{:S(2)}) copy-start(bf16[96,2048]{1,0:T(8,128)(2,1)} %refs_8_.1) | copy-start | bytes 1179652
  0.0 21.6 %copy-start = (bf16[512,2048]{1,0:T(8,128)(2,1)S(1)}, bf16[512,2048]{1,0:T(8,128)(2,1)}, u32[]{:S(2)}) copy-start(bf16[512,2048]{1,0:T(8,128)(2,1)} %refs_4_.1) | copy-start | bytes 6291460
  0.0 25.4 %copy-start.2 = (bf16[64,2048]{1,0:T(8,128)(2,1)S(1)}, bf16[64,2048]{1,0:T(8,128)(2,1)}, u32[]{:S(2)}) copy-start(bf16[64,2048]{1,0:T(8,128)(2,1)} %refs_3_.1) | copy-start | bytes 786436
  2.1 4.9 %collective-permute-start.3 = (f32[8,512]{1,0:T(8,128)}, f32[8,512]{1,0:T(8,128)S(1)}, u32[]{:S(2)}, u32[]{:S(2)}) collective-permute-start(f32[8,512]{1,0:T(8,128)} %modulation.1), channel_id=1, source_target_pairs={{0,4},{1,5},{2,6},{3,7},{4,0},{5,1},{6,2},{7,3},{8,12},{9,13},{10,... | collective-permute-start | bytes 49160 | tf_op jit(solution)/shard_map/ppermute | solution.py:489
  7.8 3.8 %collective-permute-start.4 = (f32[8,512]{1,0:T(8,128)S(1)}, f32[8,512]{1,0:T(8,128)S(1)}, u32[]{:S(2)}, u32[]{:S(2)}) collective-permute-start(f32[8,512]{1,0:T(8,128)S(1)} %add.50), channel_id=1, source_target_pairs={{0,8},{1,9},{2,10},{3,11},{4,12},{5,13},{6,14},{7,15},{8,0},{9,1},... | collective-permute-start | bytes 49160 | tf_op jit(solution)/shard_map/ppermute | solution.py:489
  9.9 15.4 %collective-permute-start = (bf16[96,2048]{1,0:T(8,128)(2,1)S(1)}, bf16[96,2048]{1,0:T(8,128)(2,1)S(1)}, u32[]{:S(2)}, u32[]{:S(2)}) collective-permute-start(bf16[96,2048]{1,0:T(8,128)(2,1)S(1)} %copy-done.1), channel_id=1, source_target_pairs={{0,2},{1,3},{2,0},{3,1},{4,6},{5,7},{6,4},{7,5},{8,10},{9,11},{10,... | collective-permute-start | bytes 1179656 | tf_op jit(solution)/shard_map/ppermute | solution.py:489
  11.4 17.7 %collective-permute-start.1 = (bf16[96,2048]{1,0:T(8,128)(2,1)S(1)}, bf16[96,2048]{1,0:T(8,128)(2,1)}, u32[]{:S(2)}, u32[]{:S(2)}) collective-permute-start(bf16[96,2048]{1,0:T(8,128)(2,1)S(1)} %copy-done.1), channel_id=1, source_target_pairs={{0,1},{1,0},{2,3},{3,2},{4,5},{5,4},{6,7},{7,6},{8,9},{9,8},{10,11... | collective-permute-start | bytes 1179656 | tf_op jit(solution)/shard_map/ppermute | solution.py:489
  11.6 4.8 %collective-permute-start.5 = (f32[8,512]{1,0:T(8,128)S(1)}, f32[8,512]{1,0:T(8,128)S(1)}, u32[]{:S(2)}, u32[]{:S(2)}) collective-permute-start(f32[8,512]{1,0:T(8,128)S(1)} %add.51), channel_id=1, source_target_pairs={{0,16},{1,17},{2,18},{3,19},{4,20},{5,21},{6,22},{7,23},{8,24},{9,... | collective-permute-start | bytes 49160 | tf_op jit(solution)/shard_map/ppermute | solution.py:489
  21.6 51.7 %collective-permute-start.23 = (bf16[512,2048]{1,0:T(8,128)(2,1)S(1)}, bf16[512,2048]{1,0:T(8,128)(2,1)}, u32[]{:S(2)}, u32[]{:S(2)}) collective-permute-start(bf16[512,2048]{1,0:T(8,128)(2,1)S(1)} %copy-done), channel_id=1, source_target_pairs={{0,2},{1,3},{2,0},{3,1},{4,6},{5,7},{6,4},{7,5},{8,10},{9,11},{10,... | collective-permute-start | bytes 6291464 | tf_op jit(solution)/shard_map/ppermute | solution.py:489
  25.3 3.7 %collective-permute-start.2 = (bf16[96,2048]{1,0:T(8,128)(2,1)S(1)}, bf16[96,2048]{1,0:T(8,128)(2,1)S(1)}, u32[]{:S(2)}, u32[]{:S(2)}) collective-permute-start(bf16[96,2048]{1,0:T(8,128)(2,1)S(1)} %collective-permute-done.refs_1_), channel_id=1, source_target_pairs={{0,1},{1,0},{2,3},{3,2},{4,5},{5,4},{6,7},{7,6},{8,9},{9,8},{10,11... | collective-permute-start | bytes 1179656 | tf_op jit(solution)/shard_map/ppermute | solution.py:489
  33.3 5.3 %collective-permute-start.12 = (bf16[1280,128]{1,0:T(8,128)(2,1)S(1)}, bf16[1280,128]{1,0:T(8,128)(2,1)S(1)}, u32[]{:S(2)}, u32[]{:S(2)}) collective-permute-start(bf16[1280,128]{1,0:T(8,128)(2,1)S(1)} %get-tuple-element.34), channel_id=1, source_target_pairs={{0,0},{1,8},{2,2},{3,10},{4,4},{5,12},{6,6},{7,14},{8,1},{9,9},{10... | collective-permute-start | bytes 983048 | tf_op jit(solution)/shard_map/ppermute | solution.py:489
  34.2 9.6 %collective-permute-start.13 = (bf16[1280,128]{1,0:T(8,128)(2,1)S(1)}, bf16[1280,128]{1,0:T(8,128)(2,1)S(1)}, u32[]{:S(2)}, u32[]{:S(2)}) collective-permute-start(bf16[1280,128]{1,0:T(8,128)(2,1)S(1)} %get-tuple-element.35), channel_id=1, source_target_pairs={{0,4},{1,12},{2,6},{3,14},{4,0},{5,8},{6,2},{7,10},{8,5},{9,13},{1... | collective-permute-start | bytes 983048 | tf_op jit(solution)/shard_map/ppermute | solution.py:489
  35.8 13.0 %collective-permute-start.6 = (bf16[384,128]{1,0:T(8,128)(2,1)S(1)}, bf16[384,128]{1,0:T(8,128)(2,1)S(1)}, u32[]{:S(2)}, u32[]{:S(2)}) collective-permute-start(bf16[384,128]{1,0:T(8,128)(2,1)S(1)} %get-tuple-element.30), channel_id=1, source_target_pairs={{0,16},{1,24},{2,18},{3,26},{4,20},{5,28},{6,22},{7,30},{8,17},{9,... | collective-permute-start | bytes 294920 | tf_op jit(solution)/shard_map/ppermute | solution.py:489
  38.4 13.0 %collective-permute-start.7 = (bf16[384,128]{1,0:T(8,128)(2,1)S(1)}, bf16[384,128]{1,0:T(8,128)(2,1)S(1)}, u32[]{:S(2)}, u32[]{:S(2)}) collective-permute-start(bf16[384,128]{1,0:T(8,128)(2,1)S(1)} %get-tuple-element.31), channel_id=1, source_target_pairs={{0,20},{1,28},{2,22},{3,30},{4,16},{5,24},{6,18},{7,26},{8,21},{9,... | collective-permute-start | bytes 294920 | tf_op jit(solution)/shard_map/ppermute | solution.py:489
  38.7 34.1 %collective-permute-start.14 = (bf16[1280,128]{1,0:T(8,128)(2,1)S(1)}, bf16[1280,128]{1,0:T(8,128)(2,1)S(1)}, u32[]{:S(2)}, u32[]{:S(2)}) collective-permute-start(bf16[1280,128]{1,0:T(8,128)(2,1)S(1)} %collective-permute-done.12.refs_2_.refs_4_.refs_0_), channel_id=1, source_target_pairs={{0,1},{1,0},{2,3},{3,2},{4,5},{5,4},{6,7},{7,6},{8,9},{9,8},{10,11... | collective-permute-start | bytes 983048 | tf_op jit(solution)/shard_map/ppermute | solution.py:489
  43.8 29.5 %collective-permute-start.15 = (bf16[1280,128]{1,0:T(8,128)(2,1)S(1)}, bf16[1280,128]{1,0:T(8,128)(2,1)S(1)}, u32[]{:S(2)}, u32[]{:S(2)}) collective-permute-start(bf16[1280,128]{1,0:T(8,128)(2,1)S(1)} %collective-permute-done.13.refs_3_.refs_5_.refs_1_), channel_id=1, source_target_pairs={{0,1},{1,0},{2,3},{3,2},{4,5},{5,4},{6,7},{7,6},{8,9},{9,8},{10,11... | collective-permute-start | bytes 983048 | tf_op jit(solution)/shard_map/ppermute | solution.py:489
  48.7 19.2 %collective-permute-start.8 = (bf16[896,128]{1,0:T(8,128)(2,1)S(1)}, bf16[896,128]{1,0:T(8,128)(2,1)S(1)}, u32[]{:S(2)}, u32[]{:S(2)}) collective-permute-start(bf16[896,128]{1,0:T(8,128)(2,1)S(1)} %get-tuple-element.32), channel_id=1, source_target_pairs={{0,16},{1,24},{2,18},{3,26},{4,20},{5,28},{6,22},{7,30},{8,17},{9,... | collective-permute-start | bytes 688136 | tf_op jit(solution)/shard_map/ppermute | solution.py:489
  51.4 21.3 %collective-permute-start.9 = (bf16[896,128]{1,0:T(8,128)(2,1)S(1)}, bf16[896,128]{1,0:T(8,128)(2,1)S(1)}, u32[]{:S(2)}, u32[]{:S(2)}) collective-permute-start(bf16[896,128]{1,0:T(8,128)(2,1)S(1)} %get-tuple-element.33), channel_id=1, source_target_pairs={{0,20},{1,28},{2,22},{3,30},{4,16},{5,24},{6,18},{7,26},{8,21},{9,... | collective-permute-start | bytes 688136 | tf_op jit(solution)/shard_map/ppermute | solution.py:489
  68.0 43.7 %collective-permute-start.24 = (bf16[512,2048]{1,0:T(8,128)(2,1)S(1)}, bf16[512,2048]{1,0:T(8,128)(2,1)S(1)}, u32[]{:S(2)}, u32[]{:S(2)}) collective-permute-start(bf16[512,2048]{1,0:T(8,128)(2,1)S(1)} %copy-done), channel_id=1, source_target_pairs={{0,1},{1,0},{2,3},{3,2},{4,5},{5,4},{6,7},{7,6},{8,9},{9,8},{10,11... | collective-permute-start | bytes 6291464 | tf_op jit(solution)/shard_map/ppermute | solution.py:489
  72.7 10.0 %collective-permute-start.10 = (bf16[896,128]{1,0:T(8,128)(2,1)S(1)}, bf16[896,128]{1,0:T(8,128)(2,1)S(1)}, u32[]{:S(2)}, u32[]{:S(2)}) collective-permute-start(bf16[896,128]{1,0:T(8,128)(2,1)S(1)} %collective-permute-done.8.refs_2_), channel_id=1, source_target_pairs={{0,1},{1,0},{2,3},{3,2},{4,5},{5,4},{6,7},{7,6},{8,9},{9,8},{10,11... | collective-permute-start | bytes 688136 | tf_op jit(solution)/shard_map/ppermute | solution.py:489
  72.7 10.0 %collective-permute-start.11 = (bf16[896,128]{1,0:T(8,128)(2,1)S(1)}, bf16[896,128]{1,0:T(8,128)(2,1)S(1)}, u32[]{:S(2)}, u32[]{:S(2)}) collective-permute-start(bf16[896,128]{1,0:T(8,128)(2,1)S(1)} %collective-permute-done.9.refs_3_), channel_id=1, source_target_pairs={{0,1},{1,0},{2,3},{3,2},{4,5},{5,4},{6,7},{7,6},{8,9},{9,8},{10,11... | collective-permute-start | bytes 688136 | tf_op jit(solution)/shard_map/ppermute | solution.py:489
  73.2 38.4 %collective-permute-start.25 = (bf16[512,2048]{1,0:T(8,128)(2,1)}, bf16[512,2048]{1,0:T(8,128)(2,1)S(1)}, u32[]{:S(2)}, u32[]{:S(2)}) collective-permute-start(bf16[512,2048]{1,0:T(8,128)(2,1)} %collective-permute-done.23.refs_5_), channel_id=1, source_target_pairs={{0,1},{1,0},{2,3},{3,2},{4,5},{5,4},{6,7},{7,6},{8,9},{9,8},{10,11... | collective-permute-start | bytes 6291464 | tf_op jit(solution)/shard_map/ppermute | solution.py:489
  88.0 9.9 %collective-permute-start.16 = (bf16[384,128]{1,0:T(8,128)(2,1)S(1)}, bf16[384,128]{1,0:T(8,128)(2,1)S(1)}, u32[]{:S(2)}, u32[]{:S(2)}) collective-permute-start(bf16[384,128]{1,0:T(8,128)(2,1)S(1)} %get-tuple-element.38), channel_id=1, source_target_pairs={{0,16},{1,24},{2,18},{3,26},{4,20},{5,28},{6,22},{7,30},{8,17},{9,... | collective-permute-start | bytes 294920 | tf_op jit(solution)/shard_map/ppermute | solution.py:489
  89.8 10.5 %collective-permute-start.17 = (bf16[384,128]{1,0:T(8,128)(2,1)S(1)}, bf16[384,128]{1,0:T(8,128)(2,1)S(1)}, u32[]{:S(2)}, u32[]{:S(2)}) collective-permute-start(bf16[384,128]{1,0:T(8,128)(2,1)S(1)} %get-tuple-element.39), channel_id=1, source_target_pairs={{0,20},{1,28},{2,22},{3,30},{4,16},{5,24},{6,18},{7,26},{8,21},{9,... | collective-permute-start | bytes 294920 | tf_op jit(solution)/shard_map/ppermute | solution.py:489
  97.2 3.1 %collective-permute-start.18 = (bf16[384,128]{1,0:T(8,128)(2,1)S(1)}, bf16[384,128]{1,0:T(8,128)(2,1)S(1)}, u32[]{:S(2)}, u32[]{:S(2)}) collective-permute-start(bf16[384,128]{1,0:T(8,128)(2,1)S(1)} %get-tuple-element.42), channel_id=1, source_target_pairs={{0,0},{1,8},{2,2},{3,10},{4,4},{5,12},{6,6},{7,14},{8,1},{9,9},{10... | collective-permute-start | bytes 294920 | tf_op jit(solution)/shard_map/ppermute | solution.py:489
  97.9 4.7 %collective-permute-start.19 = (bf16[384,128]{1,0:T(8,128)(2,1)S(1)}, bf16[384,128]{1,0:T(8,128)(2,1)S(1)}, u32[]{:S(2)}, u32[]{:S(2)}) collective-permute-start(bf16[384,128]{1,0:T(8,128)(2,1)S(1)} %get-tuple-element.43), channel_id=1, source_target_pairs={{0,4},{1,12},{2,6},{3,14},{4,0},{5,8},{6,2},{7,10},{8,5},{9,13},{1... | collective-permute-start | bytes 294920 | tf_op jit(solution)/shard_map/ppermute | solution.py:489
  102.6 5.3 %collective-permute-start.22 = (bf16[96,512]{1,0:T(8,128)(2,1)S(1)}, bf16[96,512]{1,0:T(8,128)(2,1)S(1)}, u32[]{:S(2)}, u32[]{:S(2)}) collective-permute-start(bf16[96,512]{1,0:T(8,128)(2,1)S(1)} %pad_maximum_fusion.3), channel_id=1, source_target_pairs={{0,3},{1,2},{2,1},{3,0},{4,7},{5,6},{6,5},{7,4},{8,11},{9,10},{10,... | collective-permute-start | bytes 294920 | tf_op jit(solution)/shard_map/ppermute | solution.py:489
  105.4 2.5 %collective-permute-start.21 = (bf16[96,512]{1,0:T(8,128)(2,1)S(1)}, bf16[96,512]{1,0:T(8,128)(2,1)S(1)}, u32[]{:S(2)}, u32[]{:S(2)}) collective-permute-start(bf16[96,512]{1,0:T(8,128)(2,1)S(1)} %pad_maximum_fusion.2), channel_id=1, source_target_pairs={{0,1},{1,0},{2,3},{3,2},{4,5},{5,4},{6,7},{7,6},{8,9},{9,8},{10,11... | collective-permute-start | bytes 294920 | tf_op jit(solution)/shard_map/ppermute | solution.py:489
  105.5 6.1 %collective-permute-start.20 = (bf16[96,512]{1,0:T(8,128)(2,1)S(1)}, bf16[96,512]{1,0:T(8,128)(2,1)S(1)}, u32[]{:S(2)}, u32[]{:S(2)}) collective-permute-start(bf16[96,512]{1,0:T(8,128)(2,1)S(1)} %pad_maximum_fusion.1), channel_id=1, source_target_pairs={{0,2},{1,3},{2,0},{3,1},{4,6},{5,7},{6,4},{7,5},{8,10},{9,11},{10,... | collective-permute-start | bytes 294920 | tf_op jit(solution)/shard_map/ppermute | solution.py:489

commit v4 on v3

--- a/solution.py
+++ b/solution.py
@@ -17,7 +17,7 @@
 norm_eps = 1e-06
 rope_theta = 10000.0
 block_limit = 1024
-query_block = 128
+query_block = 192
 
 
 def rms_scale(matrix):
@@ -439,13 +439,14 @@
 
 
 def output_kernel(*refs):
-    terms, weights = refs[0:4], refs[4:8]
-    latent, mods, out, ordered = refs[8:]
+    terms, weights = (refs[0:4], refs[4:8]), refs[8:12]
+    latent, mods, out, ordered = refs[12:]
     sp = lax.axis_index("sp")
-    for index, term in enumerate(terms):
-        for slot, (e, j) in enumerate(SLOTS):
-            place = pl.multiple_of(slot_head(sp, e, j) * VALUE_DIM, VALUE_DIM)
-            ordered[index, :, pl.ds(place, VALUE_DIM)] = term[:, slot * VALUE_DIM : (slot + 1) * VALUE_DIM]
+    for slot, (e, j) in enumerate(SLOTS):
+        place = pl.ds(pl.multiple_of(slot_head(sp, e, j) * VALUE_DIM, VALUE_DIM), VALUE_DIM)
+        for index in range(4):
+            lanes = slice(slot % 2 * VALUE_DIM, (slot % 2 + 1) * VALUE_DIM)
+            ordered[index, :, place] = terms[slot // 2][index][:, lanes]
     total = None
     for index, weight in enumerate(weights):
         group = jnp.dot(ordered[index], weight[...], preferred_element_type=jnp.float32)
@@ -608,11 +609,13 @@
     back = [hop(results[j], from_owner(1, j)) for j in range(2)]
     results = attend(near, late, state[2:], True)
     back += [hop(results[j], from_owner(0, j)) for j in range(2)]
-    pieces = [
-        jnp.concatenate([held[i * own_rows : (i + 1) * own_rows] for held in back], axis=1)
-        for i in range(tp_size)
-    ]
-    terms = [pieces[0]] + [across(pieces[i], slot_bits[i]) for i in range(1, tp_size)]
+    terms = []
+    for held in (back[:2], back[2:]):
+        pieces = [
+            jnp.concatenate([part_of[i * own_rows : (i + 1) * own_rows] for part_of in held], axis=1)
+            for i in range(tp_size)
+        ]
+        terms.append([pieces[0]] + [across(pieces[i], slot_bits[i]) for i in range(1, tp_size)])
 
     late_weight, _ = lax.optimization_barrier((out_weight, mods))
     weight_x = across(late_weight, 2)
@@ -621,7 +624,7 @@
     return pl.pallas_call(
         output_kernel,
         out_shape=jax.ShapeDtypeStruct(latent.shape, bf16),
-        in_specs=vmem(10),
+        in_specs=vmem(14),
         out_specs=vmem(1)[0],
         scratch_shapes=[
             pltpu.VMEM((4, own_rows, heads * VALUE_DIM), bf16),
@@ -629,7 +632,7 @@
         compiler_params=params(24),
         cost_estimate=cost(2 * own_rows * width * width, 8 * 10**6),
         name="output",
-    )(*terms, out_weight, weight_x, weight_c, weight_xc, latent, mods)
+    )(*terms[0], *terms[1], out_weight, weight_x, weight_c, weight_xc, latent, mods)
 
 
 def solution(mesh):

time: 116 us -> 115 us (level)
  Pallas kernels: 33.1 us -> 29.2 us
  starting transfers between devices: 42 us -> 44.5 us
    ppermute x26 -> x29, starting transfers between devices: 42 us -> 44.5 us  [hop(): return lax.ppermute(array, axes, pairs)]
    pallas_call x1, Pallas kernels: 3.92 us -> 2.34 us  [local_owner(): pl.pallas_call(output_kernel, out_shape=jax.ShapeDtypeStruct(latent.shape...]
    pallas_call x3, Pallas kernels: 19.9 us -> 18.6 us  [attend(): pl.pallas_call(functools.partial(attention_kernel, heads, tok, part, not...]
    ppermute x26 -> x29, waiting for transfers between devices: 31.6 us -> 32.4 us  [hop(): return lax.ppermute(array, axes, pairs)]
  transfers between devices with their start and end apart: 26 -> 29, of which waited for: 9 -> 8; matrix products, arithmetic and copies ran while one was open for 2% -> 3% of each run, Pallas kernels for 23% -> 23%
where the time goes in v4:
time: 115 us
  starting transfers between devices  44.5 us (39%)
  waiting for transfers between devices  32.4 us (28%)
  Pallas kernels  29.2 us (25%)
  blocking collectives  5.22 us (5%)
  other arithmetic  3.25 us (3%)
    ppermute x29, starting transfers between devices, hop(): return lax.ppermute(array, axes, pairs)  44.5 us
    ppermute x29, waiting for transfers between devices, hop(): return lax.ppermute(array, axes, pairs)  32.4 us
    pallas_call x3, Pallas kernels, attend(): pl.pallas_call(functools.partial(attention_kernel, heads, tok, part, not...  18.6 us
    all_gather x1, blocking collectives, local_owner(): mods = lax.all_gather(mod_part, 'tp', axis=1, tiled=True)  5.22 us
    pallas_call x1, Pallas kernels, local_owner(): pl.pallas_call(functools.partial(project_kernel, heads), out_shape=[block...  3.29 us
    pallas_call x1, Pallas kernels, hold(): pl.pallas_call(functools.partial(hold_kernel, len(arrays)), out_shape=[ja...  2.94 us
    pallas_call x1, Pallas kernels, local_owner(): pl.pallas_call(output_kernel, out_shape=jax.ShapeDtypeStruct(latent.shape...  2.34 us
  transfers between devices with their start and end apart: 29, of which 8 were waited for; matrix products, arithmetic and copies ran while one was open for 3% of the time, Pallas kernels for 23%

profile of v4, /device:TPU:0, one launch (start us, length us, event | category | flops | bytes accessed | tf_op | source)
XLA Modules:
  0.0 115.0 jit_solution(5881737181008330805)
XLA Ops:
  0.0 3.0 %collective-permute-start = (bf16[96,2048]{1,0:T(8,128)(2,1)}, bf16[96,2048]{1,0:T(8,128)(2,1)S(1)}, u32[]{:S(2)}, u32[]{:S(2)}) collective-permute-start(bf16[96,2048]{1,0:T(8,128)(2,1)} %refs_12_.1), channel_id=1, source_target_pairs={{0,2},{1,3},{2,0},{3,1},{4,6},{5,7},{6,4},{7,5},{8,10},{9,11},{10,... | collective-permute-start | bytes 1179656 | tf_op jit(solution)/shard_map/ppermute | solution.py:490
  3.0 0.0 collective-permute-start.1
  3.0 2.0 %modulation.1 = f32[8,512]{1,0:T(8,128)} custom-call(f32[4]{0:T(128)} %lam.1, f32[1,2048]{1,0:T(1,128)} %bitcast.3, f32[1,2048]{1,0:T(1,128)} %bitcast.4, bf16[256,512]{1,0:T(8,128)(2,1)} %shift_w.1, bf16[256,512]{1,0:T(8,128)(2,1)} %scale_w.1, bf16[256,512]{1,0:T(8,128)(2,1)} %gate_w.1, f32[1,512]{1,0:T(1,128)} %bitcast.5), custom_call_target="tpu_custom_call" | custom-call | flops 1000000000 | bytes 1000000 | tf_op jit(solution)/shard_map/modulation/pallas_call | solution.py:505
  5.0 1.5 %collective-permute-start.3 = (f32[8,512]{1,0:T(8,128)}, f32[8,512]{1,0:T(8,128)S(1)}, u32[]{:S(2)}, u32[]{:S(2)}) collective-permute-start(f32[8,512]{1,0:T(8,128)} %modulation.1), channel_id=1, source_target_pairs={{0,4},{1,5},{2,6},{3,7},{4,0},{5,1},{6,2},{7,3},{8,12},{9,13},{10,... | collective-permute-start | bytes 49160 | tf_op jit(solution)/shard_map/ppermute | solution.py:490
  6.6 2.4 %collective-permute-done.3 = f32[8,512]{1,0:T(8,128)S(1)} collective-permute-done((f32[8,512]{1,0:T(8,128)}, f32[8,512]{1,0:T(8,128)S(1)}, u32[]{:S(2)}, u32[]{:S(2)}) %collective-permute-start.3) | collective-permute-done | bytes 16416 | tf_op jit(solution)/shard_map/ppermute | solution.py:490
  8.9 0.7 add.50
  9.7 1.6 %collective-permute-start.4 = (f32[8,512]{1,0:T(8,128)S(1)}, f32[8,512]{1,0:T(8,128)S(1)}, u32[]{:S(2)}, u32[]{:S(2)}) collective-permute-start(f32[8,512]{1,0:T(8,128)S(1)} %add.50), channel_id=1, source_target_pairs={{0,8},{1,9},{2,10},{3,11},{4,12},{5,13},{6,14},{7,15},{8,0},{9,1},... | collective-permute-start | bytes 49160 | tf_op jit(solution)/shard_map/ppermute | solution.py:490
  11.3 2.2 %collective-permute-done.4 = f32[8,512]{1,0:T(8,128)S(1)} collective-permute-done((f32[8,512]{1,0:T(8,128)S(1)}, f32[8,512]{1,0:T(8,128)S(1)}, u32[]{:S(2)}, u32[]{:S(2)}) %collective-permute-start.4) | collective-permute-done | bytes 16416 | tf_op jit(solution)/shard_map/ppermute | solution.py:490
  13.4 2.6 %collective-permute-start.5 = (f32[8,512]{1,0:T(8,128)S(1)}, f32[8,512]{1,0:T(8,128)S(1)}, u32[]{:S(2)}, u32[]{:S(2)}) collective-permute-start(f32[8,512]{1,0:T(8,128)S(1)} %add.51), channel_id=1, source_target_pairs={{0,16},{1,17},{2,18},{3,19},{4,20},{5,21},{6,22},{7,23},{8,24},{9,... | collective-permute-start | bytes 49160 | tf_op jit(solution)/shard_map/ppermute | solution.py:490
  16.0 0.1 mul.24
  16.1 2.0 %collective-permute-done.5 = f32[8,512]{1,0:T(8,128)S(1)} collective-permute-done((f32[8,512]{1,0:T(8,128)S(1)}, f32[8,512]{1,0:T(8,128)S(1)}, u32[]{:S(2)}, u32[]{:S(2)}) %collective-permute-start.5) | collective-permute-done | bytes 16416 | tf_op jit(solution)/shard_map/ppermute | solution.py:490
  18.1 5.2 %all_gather.3.refs_5_.refs_8_.refs_13_ = f32[8,2048]{1,0:T(8,128)S(1)} all-gather(f32[8,512]{1,0:T(8,128)S(1)} %add.52), channel_id=1, replica_groups=mesh['sp'=8,'tp'=4] {'tp'}, dimensions={1}, use_global_device_ids=true | all-gather | bytes 81920 | tf_op jit(solution)/shard_map/all_gather | solution.py:531
  23.3 0.3 collective-permute-start.26
  23.5 1.8 %fusion.8 = (f32[384,128]{1,0:T(8,128)S(1)}, f32[384,128]{1,0:T(8,128)S(1)}) fusion(f32[128]{0:T(128)S(1)} %mul.24, s32[384]{0:T(512)S(1)} %get-tuple-element.64, s32[384]{0:T(512)S(1)} %get-tuple-element.65, s32[384]{0:T(512)S(1)} %get-tuple-element.63, s32[384]{0:T(512)S(1)} %get-tuple-element.66, s32[]{:T(128)S(6)} %axis_index.25, s32[]{:T(128)S(6)} %mul.21, ...), kind=kLoop, calls=%fused_computation.22 | loop fusion | flops 2506752 | bytes 401800 | tf_op jit(solution)/shard_map/mul | solution.py:546
  25.3 0.2 collective-permute-start.2
  25.5 2.9 %hold.1 = (bf16[2,2048,256]{2,1,0:T(8,128)(2,1)S(1)}, bf16[2,2048,256]{2,1,0:T(8,128)(2,1)S(1)}, bf16[2048,512]{1,0:T(8,128)(2,1)S(1)}, bf16[64,2048]{1,0:T(8,128)(2,1)S(1)}) custom-call(bf16[2,2048,256]{2,1,0:T(8,128)(2,1)} %refs_0_.2, bf16[2,2048,256]{2,1,0:T(8,128)(2,1)} %refs_1_.1, bf16[2048,512]{1,0:T(8,128)(2,1)} %refs_2_.1, bf16[64,2048]{1,0:T(8,128)(2,1)S(1)} %copy-done.2), custom_call_target="tpu_custom_call" | custom-call | flops 100000000 | bytes 8000000 | tf_op jit(solution)/shard_map/hold/pallas_call | solution.py:261
  28.4 0.7 negate_select_fusion.refs_7_
  29.1 0.0 collective-permute-done.2.refs_3_
  29.1 3.3 %project.1 = (bf16[384,128]{1,0:T(8,128)(2,1)S(1)}, bf16[384,128]{1,0:T(8,128)(2,1)S(1)}, bf16[896,128]{1,0:T(8,128)(2,1)S(1)}, bf16[896,128]{1,0:T(8,128)(2,1)S...) custom-call(bf16[96,2048]{1,0:T(8,128)(2,1)S(1)} %copy-done.1, ...), custom_call_target="tpu_custom_call" | custom-call | flops 2818572288 | bytes 8000000 | tf_op jit(solution)/shard_map/project/pallas_call | solution.py:557
  32.4 0.9 collective-permute-start.12
  33.3 1.9 %collective-permute-start.13 = (bf16[1280,128]{1,0:T(8,128)(2,1)S(1)}, bf16[1280,128]{1,0:T(8,128)(2,1)S(1)}, u32[]{:S(2)}, u32[]{:S(2)}) collective-permute-start(bf16[1280,128]{1,0:T(8,128)(2,1)S(1)} %get-tuple-element.35), channel_id=1, source_target_pairs={{0,4},{1,12},{2,6},{3,14},{4,0},{5,8},{6,2},{7,10},{8,5},{9,13},{1... | collective-permute-start | bytes 983048 | tf_op jit(solution)/shard_map/ppermute | solution.py:490
  35.2 2.6 %collective-permute-start.6 = (bf16[384,128]{1,0:T(8,128)(2,1)S(1)}, bf16[384,128]{1,0:T(8,128)(2,1)S(1)}, u32[]{:S(2)}, u32[]{:S(2)}) collective-permute-start(bf16[384,128]{1,0:T(8,128)(2,1)S(1)} %get-tuple-element.30), channel_id=1, source_target_pairs={{0,16},{1,24},{2,18},{3,26},{4,20},{5,28},{6,22},{7,30},{8,17},{9,... | collective-permute-start | bytes 294920 | tf_op jit(solution)/shard_map/ppermute | solution.py:490
  37.8 0.0 collective-permute-start.7
  37.8 4.9 %collective-permute-start.14 = (bf16[1280,128]{1,0:T(8,128)(2,1)S(1)}, bf16[1280,128]{1,0:T(8,128)(2,1)S(1)}, u32[]{:S(2)}, u32[]{:S(2)}) collective-permute-start(bf16[1280,128]{1,0:T(8,128)(2,1)S(1)} %collective-permute-done.12.refs_2_.refs_4_.refs_0_), channel_id=1, source_target_pairs={{0,1},{1,0},{2,3},{3,2},{4,5},{5,4},{6,7},{7,6},{8,9},{9,8},{10,11... | collective-permute-start | bytes 983048 | tf_op jit(solution)/shard_map/ppermute | solution.py:490
  42.7 5.5 %collective-permute-start.15 = (bf16[1280,128]{1,0:T(8,128)(2,1)S(1)}, bf16[1280,128]{1,0:T(8,128)(2,1)S(1)}, u32[]{:S(2)}, u32[]{:S(2)}) collective-permute-start(bf16[1280,128]{1,0:T(8,128)(2,1)S(1)} %collective-permute-done.13.refs_3_.refs_5_.refs_1_), channel_id=1, source_target_pairs={{0,1},{1,0},{2,3},{3,2},{4,5},{5,4},{6,7},{7,6},{8,9},{9,8},{10,11... | collective-permute-start | bytes 983048 | tf_op jit(solution)/shard_map/ppermute | solution.py:490
  48.1 2.6 %collective-permute-start.8 = (bf16[896,128]{1,0:T(8,128)(2,1)S(1)}, bf16[896,128]{1,0:T(8,128)(2,1)S(1)}, u32[]{:S(2)}, u32[]{:S(2)}) collective-permute-start(bf16[896,128]{1,0:T(8,128)(2,1)S(1)} %get-tuple-element.32), channel_id=1, source_target_pairs={{0,16},{1,24},{2,18},{3,26},{4,20},{5,28},{6,22},{7,30},{8,17},{9,... | collective-permute-start | bytes 688136 | tf_op jit(solution)/shard_map/ppermute | solution.py:490
  50.8 0.8 collective-permute-start.9
  51.6 15.7 %collective-permute-done.8.refs_2_ = bf16[896,128]{1,0:T(8,128)(2,1)S(1)} collective-permute-done((bf16[896,128]{1,0:T(8,128)(2,1)S(1)}, bf16[896,128]{1,0:T(8,128)(2,1)S(1)}, u32[]{:S(2)}, u32[]{:S(2)}) %collective-permute-start.8) | collective-permute-done | bytes 229408 | tf_op jit(solution)/shard_map/ppermute | solution.py:490
  67.3 0.0 collective-permute-start.27
  67.4 4.7 %collective-permute-done.9.refs_3_ = bf16[896,128]{1,0:T(8,128)(2,1)S(1)} collective-permute-done((bf16[896,128]{1,0:T(8,128)(2,1)S(1)}, bf16[896,128]{1,0:T(8,128)(2,1)S(1)}, u32[]{:S(2)}, u32[]{:S(2)}) %collective-permute-start.9) | collective-permute-done | bytes 229408 | tf_op jit(solution)/shard_map/ppermute | solution.py:490
  72.1 0.5 collective-permute-start.11
  72.6 8.6 %attention.3 = (f32[1536,128]{1,0:T(8,128)S(1)}, f32[1536,128]{1,0:T(8,128)S(1)}, f32[1536,128]{1,0:T(8,128)S(1)}, f32[1536,128]{1,0:T(8,128)S(1)}) custom-call(bf16[384,128]{1,0:T(8,128)(2,1)S(1)} %collective-permute-done.6.refs_0_, bf16[384,128]{1,0:T(8,128)(2,1)S(1)} %collective-permute-done.7.refs_1_, ...), custom_call_target="tpu_custom_call" | custom-call | flops 5637144576 | bytes 1000000 | tf_op jit(solution)/shard_map/attention/pallas_call | solution.py:585
  81.2 0.1 collective-permute-start.28
  81.3 5.0 %attention.5 = (bf16[384,128]{1,0:T(8,128)(2,1)S(1)}, bf16[384,128]{1,0:T(8,128)(2,1)S(1)}) custom-call(bf16[1280,128]{1,0:T(8,128)(2,1)S(1)} %collective-permute-done.12.refs_2_.refs_4_.refs_0_, bf16[1280,128]{1,0:T(8,128)(2,1)S(1)} %collective-permute-done.13.refs_3_.refs_5_.refs_1_, bf16[896,128]{1,0:T(8,128)(2,1)S(1)} %collective-permute-done.8.refs_2_, ...), custom_call_target="tpu_custom_call" | custom-call | flops 2818572288 | bytes 1000000 | tf_op jit(solution)/shard_map/attention/pallas_call | solution.py:585
  86.4 0.9 collective-permute-start.21
  87.2 1.6 %collective-permute-start.22 = (bf16[384,128]{1,0:T(8,128)(2,1)S(1)}, bf16[384,128]{1,0:T(8,128)(2,1)S(1)}, u32[]{:S(2)}, u32[]{:S(2)}) collective-permute-start(bf16[384,128]{1,0:T(8,128)(2,1)S(1)} %get-tuple-element.43), channel_id=1, source_target_pairs={{0,4},{1,12},{2,6},{3,14},{4,0},{5,8},{6,2},{7,10},{8,5},{9,13},{1... | collective-permute-start | bytes 294920 | tf_op jit(solution)/shard_map/ppermute | solution.py:490
  88.8 5.0 %attention.4 = (bf16[384,128]{1,0:T(8,128)(2,1)S(1)}, bf16[384,128]{1,0:T(8,128)(2,1)S(1)}) custom-call(bf16[384,128]{1,0:T(8,128)(2,1)S(1)} %collective-permute-done.6.refs_0_, bf16[384,128]{1,0:T(8,128)(2,1)S(1)} %collective-permute-done.7.refs_1_, bf16[896,128]{1,0:T(8,128)(2,1)S(1)} %collective-permute-done.8.refs_2_, ...), custom_call_target="tpu_custom_call" | custom-call | flops 2818572288 | bytes 1000000 | tf_op jit(solution)/shard_map/attention/pallas_call | solution.py:585
  93.9 0.7 collective-permute-start.16
  94.6 2.2 %collective-permute-start.17 = (bf16[384,128]{1,0:T(8,128)(2,1)S(1)}, bf16[384,128]{1,0:T(8,128)(2,1)S(1)}, u32[]{:S(2)}, u32[]{:S(2)}) collective-permute-start(bf16[384,128]{1,0:T(8,128)(2,1)S(1)} %get-tuple-element.39), channel_id=1, source_target_pairs={{0,20},{1,28},{2,22},{3,30},{4,16},{5,24},{6,18},{7,26},{8,21},{9,... | collective-permute-start | bytes 294920 | tf_op jit(solution)/shard_map/ppermute | solution.py:490
  96.9 4.6 %collective-permute-start.25 = (bf16[96,256]{1,0:T(8,128)(2,1)S(1)}, bf16[96,256]{1,0:T(8,128)(2,1)S(1)}, u32[]{:S(2)}, u32[]{:S(2)}) collective-permute-start(bf16[96,256]{1,0:T(8,128)(2,1)S(1)} %pad_maximum_fusion.7), channel_id=1, source_target_pairs={{0,3},{1,2},{2,1},{3,0},{4,7},{5,6},{6,5},{7,4},{8,11},{9,10},{10,... | collective-permute-start | bytes 147464 | tf_op jit(solution)/shard_map/ppermute | solution.py:490
  101.5 1.5 %collective-permute-start.24 = (bf16[96,256]{1,0:T(8,128)(2,1)S(1)}, bf16[96,256]{1,0:T(8,128)(2,1)S(1)}, u32[]{:S(2)}, u32[]{:S(2)}) collective-permute-start(bf16[96,256]{1,0:T(8,128)(2,1)S(1)} %pad_maximum_fusion.6), channel_id=1, source_target_pairs={{0,1},{1,0},{2,3},{3,2},{4,5},{5,4},{6,7},{7,6},{8,9},{9,8},{10,11... | collective-permute-start | bytes 147464 | tf_op jit(solution)/shard_map/ppermute | solution.py:490
  103.0 1.1 collective-permute-done.17
  104.2 1.4 %collective-permute-start.23 = (bf16[96,256]{1,0:T(8,128)(2,1)S(1)}, bf16[96,256]{1,0:T(8,128)(2,1)S(1)}, u32[]{:S(2)}, u32[]{:S(2)}) collective-permute-start(bf16[96,256]{1,0:T(8,128)(2,1)S(1)} %pad_maximum_fusion.5), channel_id=1, source_target_pairs={{0,2},{1,3},{2,0},{3,1},{4,6},{5,7},{6,4},{7,5},{8,10},{9,11},{10,... | collective-permute-start | bytes 147464 | tf_op jit(solution)/shard_map/ppermute | solution.py:490
  105.7 1.2 %collective-permute-start.20 = (bf16[96,256]{1,0:T(8,128)(2,1)S(1)}, bf16[96,256]{1,0:T(8,128)(2,1)S(1)}, u32[]{:S(2)}, u32[]{:S(2)}) collective-permute-start(bf16[96,256]{1,0:T(8,128)(2,1)S(1)} %pad_maximum_fusion.3), channel_id=1, source_target_pairs={{0,3},{1,2},{2,1},{3,0},{4,7},{5,6},{6,5},{7,4},{8,11},{9,10},{10,... | collective-permute-start | bytes 147464 | tf_op jit(solution)/shard_map/ppermute | solution.py:490
  106.9 1.6 %collective-permute-done.23.refs_5_ = bf16[96,256]{1,0:T(8,128)(2,1)S(1)} collective-permute-done((bf16[96,256]{1,0:T(8,128)(2,1)S(1)}, bf16[96,256]{1,0:T(8,128)(2,1)S(1)}, u32[]{:S(2)}, u32[]{:S(2)}) %collective-permute-start.23) | collective-permute-done | bytes 49184 | tf_op jit(solution)/shard_map/ppermute | solution.py:490
  108.5 1.4 %collective-permute-start.18 = (bf16[96,256]{1,0:T(8,128)(2,1)S(1)}, bf16[96,256]{1,0:T(8,128)(2,1)S(1)}, u32[]{:S(2)}, u32[]{:S(2)}) collective-permute-start(bf16[96,256]{1,0:T(8,128)(2,1)S(1)} %pad_maximum_fusion.1), channel_id=1, source_target_pairs={{0,2},{1,3},{2,0},{3,1},{4,6},{5,7},{6,4},{7,5},{8,10},{9,11},{10,... | collective-permute-start | bytes 147464 | tf_op jit(solution)/shard_map/ppermute | solution.py:490
  110.0 2.6 %collective-permute-done.18.refs_1_ = bf16[96,256]{1,0:T(8,128)(2,1)S(1)} collective-permute-done((bf16[96,256]{1,0:T(8,128)(2,1)S(1)}, bf16[96,256]{1,0:T(8,128)(2,1)S(1)}, u32[]{:S(2)}, u32[]{:S(2)}) %collective-permute-start.18) | collective-permute-done | bytes 49184 | tf_op jit(solution)/shard_map/ppermute | solution.py:490
  112.6 2.3 %output.1 = bf16[96,2048]{1,0:T(8,128)(2,1)} custom-call(bf16[96,256]{1,0:T(8,128)(2,1)S(1)} %pad_maximum_fusion.refs_0_, bf16[96,256]{1,0:T(8,128)(2,1)S(1)} %collective-permute-done.18.refs_1_, bf16[96,256]{1,0:T(8,128)(2,1)S(1)} %collective-permute-done.19.refs_2_, bf16[96,256]{1,0:T(8,128)(2,1)S(1)} %collective-permute-done.20.refs_3_, ...), custom_call_target="tpu_custom_call" | custom-call | flops 805306368 | bytes 8000000 | tf_op jit(solution)/shard_map/output/pallas_call | solution.py:624
  (51 shorter events, 0.2 us)
Async XLA Ops:
  0.0 23.3 %copy-start = (bf16[512,2048]{1,0:T(8,128)(2,1)S(1)}, bf16[512,2048]{1,0:T(8,128)(2,1)}, u32[]{:S(2)}) copy-start(bf16[512,2048]{1,0:T(8,128)(2,1)} %refs_8_.1) | copy-start | bytes 6291460
  0.0 25.3 %collective-permute-start = (bf16[96,2048]{1,0:T(8,128)(2,1)}, bf16[96,2048]{1,0:T(8,128)(2,1)S(1)}, u32[]{:S(2)}, u32[]{:S(2)}) collective-permute-start(bf16[96,2048]{1,0:T(8,128)(2,1)} %refs_12_.1), channel_id=1, source_target_pairs={{0,2},{1,3},{2,0},{3,1},{4,6},{5,7},{6,4},{7,5},{8,10},{9,11},{10,... | collective-permute-start | bytes 1179656 | tf_op jit(solution)/shard_map/ppermute | solution.py:490
  3.0 26.1 %collective-permute-start.1 = (bf16[96,2048]{1,0:T(8,128)(2,1)}, bf16[96,2048]{1,0:T(8,128)(2,1)S(1)}, u32[]{:S(2)}, u32[]{:S(2)}) collective-permute-start(bf16[96,2048]{1,0:T(8,128)(2,1)} %refs_12_.1), channel_id=1, source_target_pairs={{0,1},{1,0},{2,3},{3,2},{4,5},{5,4},{6,7},{7,6},{8,9},{9,8},{10,11... | collective-permute-start | bytes 1179656 | tf_op jit(solution)/shard_map/ppermute | solution.py:490
  3.0 22.5 %copy-start.2 = (bf16[64,2048]{1,0:T(8,128)(2,1)S(1)}, bf16[64,2048]{1,0:T(8,128)(2,1)}, u32[]{:S(2)}) copy-start(bf16[64,2048]{1,0:T(8,128)(2,1)} %refs_3_.1) | copy-start | bytes 786436
  5.0 3.9 %collective-permute-start.3 = (f32[8,512]{1,0:T(8,128)}, f32[8,512]{1,0:T(8,128)S(1)}, u32[]{:S(2)}, u32[]{:S(2)}) collective-permute-start(f32[8,512]{1,0:T(8,128)} %modulation.1), channel_id=1, source_target_pairs={{0,4},{1,5},{2,6},{3,7},{4,0},{5,1},{6,2},{7,3},{8,12},{9,13},{10,... | collective-permute-start | bytes 49160 | tf_op jit(solution)/shard_map/ppermute | solution.py:490
  9.7 3.7 %collective-permute-start.4 = (f32[8,512]{1,0:T(8,128)S(1)}, f32[8,512]{1,0:T(8,128)S(1)}, u32[]{:S(2)}, u32[]{:S(2)}) collective-permute-start(f32[8,512]{1,0:T(8,128)S(1)} %add.50), channel_id=1, source_target_pairs={{0,8},{1,9},{2,10},{3,11},{4,12},{5,13},{6,14},{7,15},{8,0},{9,1},... | collective-permute-start | bytes 49160 | tf_op jit(solution)/shard_map/ppermute | solution.py:490
  13.4 4.6 %collective-permute-start.5 = (f32[8,512]{1,0:T(8,128)S(1)}, f32[8,512]{1,0:T(8,128)S(1)}, u32[]{:S(2)}, u32[]{:S(2)}) collective-permute-start(f32[8,512]{1,0:T(8,128)S(1)} %add.51), channel_id=1, source_target_pairs={{0,16},{1,17},{2,18},{3,19},{4,20},{5,21},{6,22},{7,23},{8,24},{9,... | collective-permute-start | bytes 49160 | tf_op jit(solution)/shard_map/ppermute | solution.py:490
  23.3 57.9 %collective-permute-start.26 = (bf16[512,2048]{1,0:T(8,128)(2,1)S(1)}, bf16[512,2048]{1,0:T(8,128)(2,1)S(1)}, u32[]{:S(2)}, u32[]{:S(2)}) collective-permute-start(bf16[512,2048]{1,0:T(8,128)(2,1)S(1)} %copy-done), channel_id=1, source_target_pairs={{0,2},{1,3},{2,0},{3,1},{4,6},{5,7},{6,4},{7,5},{8,10},{9,11},{10,... | collective-permute-start | bytes 6291464 | tf_op jit(solution)/shard_map/ppermute | solution.py:490
  25.3 3.8 %collective-permute-start.2 = (bf16[96,2048]{1,0:T(8,128)(2,1)S(1)}, bf16[96,2048]{1,0:T(8,128)(2,1)S(1)}, u32[]{:S(2)}, u32[]{:S(2)}) collective-permute-start(bf16[96,2048]{1,0:T(8,128)(2,1)S(1)} %collective-permute-done.refs_1_), channel_id=1, source_target_pairs={{0,1},{1,0},{2,3},{3,2},{4,5},{5,4},{6,7},{7,6},{8,9},{9,8},{10,11... | collective-permute-start | bytes 1179656 | tf_op jit(solution)/shard_map/ppermute | solution.py:490
  25.5 3.6 %copy-start.1 = (bf16[96,2048]{1,0:T(8,128)(2,1)S(1)}, bf16[96,2048]{1,0:T(8,128)(2,1)}, u32[]{:S(2)}) copy-start(bf16[96,2048]{1,0:T(8,128)(2,1)} %refs_12_.1) | copy-start | bytes 1179652
  32.4 5.4 %collective-permute-start.12 = (bf16[1280,128]{1,0:T(8,128)(2,1)S(1)}, bf16[1280,128]{1,0:T(8,128)(2,1)S(1)}, u32[]{:S(2)}, u32[]{:S(2)}) collective-permute-start(bf16[1280,128]{1,0:T(8,128)(2,1)S(1)} %get-tuple-element.34), channel_id=1, source_target_pairs={{0,0},{1,8},{2,2},{3,10},{4,4},{5,12},{6,6},{7,14},{8,1},{9,9},{10... | collective-permute-start | bytes 983048 | tf_op jit(solution)/shard_map/ppermute | solution.py:490
  33.3 9.4 %collective-permute-start.13 = (bf16[1280,128]{1,0:T(8,128)(2,1)S(1)}, bf16[1280,128]{1,0:T(8,128)(2,1)S(1)}, u32[]{:S(2)}, u32[]{:S(2)}) collective-permute-start(bf16[1280,128]{1,0:T(8,128)(2,1)S(1)} %get-tuple-element.35), channel_id=1, source_target_pairs={{0,4},{1,12},{2,6},{3,14},{4,0},{5,8},{6,2},{7,10},{8,5},{9,13},{1... | collective-permute-start | bytes 983048 | tf_op jit(solution)/shard_map/ppermute | solution.py:490
  35.2 13.0 %collective-permute-start.6 = (bf16[384,128]{1,0:T(8,128)(2,1)S(1)}, bf16[384,128]{1,0:T(8,128)(2,1)S(1)}, u32[]{:S(2)}, u32[]{:S(2)}) collective-permute-start(bf16[384,128]{1,0:T(8,128)(2,1)S(1)} %get-tuple-element.30), channel_id=1, source_target_pairs={{0,16},{1,24},{2,18},{3,26},{4,20},{5,28},{6,22},{7,30},{8,17},{9,... | collective-permute-start | bytes 294920 | tf_op jit(solution)/shard_map/ppermute | solution.py:490
  37.8 13.0 %collective-permute-start.7 = (bf16[384,128]{1,0:T(8,128)(2,1)S(1)}, bf16[384,128]{1,0:T(8,128)(2,1)S(1)}, u32[]{:S(2)}, u32[]{:S(2)}) collective-permute-start(bf16[384,128]{1,0:T(8,128)(2,1)S(1)} %get-tuple-element.31), channel_id=1, source_target_pairs={{0,20},{1,28},{2,22},{3,30},{4,16},{5,24},{6,18},{7,26},{8,21},{9,... | collective-permute-start | bytes 294920 | tf_op jit(solution)/shard_map/ppermute | solution.py:490
  37.8 34.3 %collective-permute-start.14 = (bf16[1280,128]{1,0:T(8,128)(2,1)S(1)}, bf16[1280,128]{1,0:T(8,128)(2,1)S(1)}, u32[]{:S(2)}, u32[]{:S(2)}) collective-permute-start(bf16[1280,128]{1,0:T(8,128)(2,1)S(1)} %collective-permute-done.12.refs_2_.refs_4_.refs_0_), channel_id=1, source_target_pairs={{0,1},{1,0},{2,3},{3,2},{4,5},{5,4},{6,7},{7,6},{8,9},{9,8},{10,11... | collective-permute-start | bytes 983048 | tf_op jit(solution)/shard_map/ppermute | solution.py:490
  42.7 29.9 %collective-permute-start.15 = (bf16[1280,128]{1,0:T(8,128)(2,1)S(1)}, bf16[1280,128]{1,0:T(8,128)(2,1)S(1)}, u32[]{:S(2)}, u32[]{:S(2)}) collective-permute-start(bf16[1280,128]{1,0:T(8,128)(2,1)S(1)} %collective-permute-done.13.refs_3_.refs_5_.refs_1_), channel_id=1, source_target_pairs={{0,1},{1,0},{2,3},{3,2},{4,5},{5,4},{6,7},{7,6},{8,9},{9,8},{10,11... | collective-permute-start | bytes 983048 | tf_op jit(solution)/shard_map/ppermute | solution.py:490
  48.1 19.2 %collective-permute-start.8 = (bf16[896,128]{1,0:T(8,128)(2,1)S(1)}, bf16[896,128]{1,0:T(8,128)(2,1)S(1)}, u32[]{:S(2)}, u32[]{:S(2)}) collective-permute-start(bf16[896,128]{1,0:T(8,128)(2,1)S(1)} %get-tuple-element.32), channel_id=1, source_target_pairs={{0,16},{1,24},{2,18},{3,26},{4,20},{5,28},{6,22},{7,30},{8,17},{9,... | collective-permute-start | bytes 688136 | tf_op jit(solution)/shard_map/ppermute | solution.py:490
  50.8 21.3 %collective-permute-start.9 = (bf16[896,128]{1,0:T(8,128)(2,1)S(1)}, bf16[896,128]{1,0:T(8,128)(2,1)S(1)}, u32[]{:S(2)}, u32[]{:S(2)}) collective-permute-start(bf16[896,128]{1,0:T(8,128)(2,1)S(1)} %get-tuple-element.33), channel_id=1, source_target_pairs={{0,20},{1,28},{2,22},{3,30},{4,16},{5,24},{6,18},{7,26},{8,21},{9,... | collective-permute-start | bytes 688136 | tf_op jit(solution)/shard_map/ppermute | solution.py:490
  67.3 45.3 %collective-permute-start.27 = (bf16[512,2048]{1,0:T(8,128)(2,1)S(1)}, bf16[512,2048]{1,0:T(8,128)(2,1)S(1)}, u32[]{:S(2)}, u32[]{:S(2)}) collective-permute-start(bf16[512,2048]{1,0:T(8,128)(2,1)S(1)} %copy-done), channel_id=1, source_target_pairs={{0,1},{1,0},{2,3},{3,2},{4,5},{5,4},{6,7},{7,6},{8,9},{9,8},{10,11... | collective-permute-start | bytes 6291464 | tf_op jit(solution)/shard_map/ppermute | solution.py:490
  72.1 9.2 %collective-permute-start.10 = (bf16[896,128]{1,0:T(8,128)(2,1)S(1)}, bf16[896,128]{1,0:T(8,128)(2,1)S(1)}, u32[]{:S(2)}, u32[]{:S(2)}) collective-permute-start(bf16[896,128]{1,0:T(8,128)(2,1)S(1)} %collective-permute-done.8.refs_2_), channel_id=1, source_target_pairs={{0,1},{1,0},{2,3},{3,2},{4,5},{5,4},{6,7},{7,6},{8,9},{9,8},{10,11... | collective-permute-start | bytes 688136 | tf_op jit(solution)/shard_map/ppermute | solution.py:490
  72.1 9.2 %collective-permute-start.11 = (bf16[896,128]{1,0:T(8,128)(2,1)S(1)}, bf16[896,128]{1,0:T(8,128)(2,1)S(1)}, u32[]{:S(2)}, u32[]{:S(2)}) collective-permute-start(bf16[896,128]{1,0:T(8,128)(2,1)S(1)} %collective-permute-done.9.refs_3_), channel_id=1, source_target_pairs={{0,1},{1,0},{2,3},{3,2},{4,5},{5,4},{6,7},{7,6},{8,9},{9,8},{10,11... | collective-permute-start | bytes 688136 | tf_op jit(solution)/shard_map/ppermute | solution.py:490
  81.2 31.4 %collective-permute-start.28 = (bf16[512,2048]{1,0:T(8,128)(2,1)S(1)}, bf16[512,2048]{1,0:T(8,128)(2,1)S(1)}, u32[]{:S(2)}, u32[]{:S(2)}) collective-permute-start(bf16[512,2048]{1,0:T(8,128)(2,1)S(1)} %collective-permute-done.26.refs_9_), channel_id=1, source_target_pairs={{0,1},{1,0},{2,3},{3,2},{4,5},{5,4},{6,7},{7,6},{8,9},{9,8},{10,11... | collective-permute-start | bytes 6291464 | tf_op jit(solution)/shard_map/ppermute | solution.py:490
  86.4 8.3 %collective-permute-start.21 = (bf16[384,128]{1,0:T(8,128)(2,1)S(1)}, bf16[384,128]{1,0:T(8,128)(2,1)S(1)}, u32[]{:S(2)}, u32[]{:S(2)}) collective-permute-start(bf16[384,128]{1,0:T(8,128)(2,1)S(1)} %get-tuple-element.42), channel_id=1, source_target_pairs={{0,0},{1,8},{2,2},{3,10},{4,4},{5,12},{6,6},{7,14},{8,1},{9,9},{10... | collective-permute-start | bytes 294920 | tf_op jit(solution)/shard_map/ppermute | solution.py:490
  87.2 9.6 %collective-permute-start.22 = (bf16[384,128]{1,0:T(8,128)(2,1)S(1)}, bf16[384,128]{1,0:T(8,128)(2,1)S(1)}, u32[]{:S(2)}, u32[]{:S(2)}) collective-permute-start(bf16[384,128]{1,0:T(8,128)(2,1)S(1)} %get-tuple-element.43), channel_id=1, source_target_pairs={{0,4},{1,12},{2,6},{3,14},{4,0},{5,8},{6,2},{7,10},{8,5},{9,13},{1... | collective-permute-start | bytes 294920 | tf_op jit(solution)/shard_map/ppermute | solution.py:490
  93.9 7.6 %collective-permute-start.16 = (bf16[384,128]{1,0:T(8,128)(2,1)S(1)}, bf16[384,128]{1,0:T(8,128)(2,1)S(1)}, u32[]{:S(2)}, u32[]{:S(2)}) collective-permute-start(bf16[384,128]{1,0:T(8,128)(2,1)S(1)} %get-tuple-element.38), channel_id=1, source_target_pairs={{0,16},{1,24},{2,18},{3,26},{4,20},{5,28},{6,22},{7,30},{8,17},{9,... | collective-permute-start | bytes 294920 | tf_op jit(solution)/shard_map/ppermute | solution.py:490
  94.6 9.6 %collective-permute-start.17 = (bf16[384,128]{1,0:T(8,128)(2,1)S(1)}, bf16[384,128]{1,0:T(8,128)(2,1)S(1)}, u32[]{:S(2)}, u32[]{:S(2)}) collective-permute-start(bf16[384,128]{1,0:T(8,128)(2,1)S(1)} %get-tuple-element.39), channel_id=1, source_target_pairs={{0,20},{1,28},{2,22},{3,30},{4,16},{5,24},{6,18},{7,26},{8,21},{9,... | collective-permute-start | bytes 294920 | tf_op jit(solution)/shard_map/ppermute | solution.py:490
  96.9 8.8 %collective-permute-start.25 = (bf16[96,256]{1,0:T(8,128)(2,1)S(1)}, bf16[96,256]{1,0:T(8,128)(2,1)S(1)}, u32[]{:S(2)}, u32[]{:S(2)}) collective-permute-start(bf16[96,256]{1,0:T(8,128)(2,1)S(1)} %pad_maximum_fusion.7), channel_id=1, source_target_pairs={{0,3},{1,2},{2,1},{3,0},{4,7},{5,6},{6,5},{7,4},{8,11},{9,10},{10,... | collective-permute-start | bytes 147464 | tf_op jit(solution)/shard_map/ppermute | solution.py:490
  101.5 5.4 %collective-permute-start.24 = (bf16[96,256]{1,0:T(8,128)(2,1)S(1)}, bf16[96,256]{1,0:T(8,128)(2,1)S(1)}, u32[]{:S(2)}, u32[]{:S(2)}) collective-permute-start(bf16[96,256]{1,0:T(8,128)(2,1)S(1)} %pad_maximum_fusion.6), channel_id=1, source_target_pairs={{0,1},{1,0},{2,3},{3,2},{4,5},{5,4},{6,7},{7,6},{8,9},{9,8},{10,11... | collective-permute-start | bytes 147464 | tf_op jit(solution)/shard_map/ppermute | solution.py:490
  104.2 4.3 %collective-permute-start.23 = (bf16[96,256]{1,0:T(8,128)(2,1)S(1)}, bf16[96,256]{1,0:T(8,128)(2,1)S(1)}, u32[]{:S(2)}, u32[]{:S(2)}) collective-permute-start(bf16[96,256]{1,0:T(8,128)(2,1)S(1)} %pad_maximum_fusion.5), channel_id=1, source_target_pairs={{0,2},{1,3},{2,0},{3,1},{4,6},{5,7},{6,4},{7,5},{8,10},{9,11},{10,... | collective-permute-start | bytes 147464 | tf_op jit(solution)/shard_map/ppermute | solution.py:490
  105.7 4.3 %collective-permute-start.20 = (bf16[96,256]{1,0:T(8,128)(2,1)S(1)}, bf16[96,256]{1,0:T(8,128)(2,1)S(1)}, u32[]{:S(2)}, u32[]{:S(2)}) collective-permute-start(bf16[96,256]{1,0:T(8,128)(2,1)S(1)} %pad_maximum_fusion.3), channel_id=1, source_target_pairs={{0,3},{1,2},{2,1},{3,0},{4,7},{5,6},{6,5},{7,4},{8,11},{9,10},{10,... | collective-permute-start | bytes 147464 | tf_op jit(solution)/shard_map/ppermute | solution.py:490
  106.9 3.0 %collective-permute-start.19 = (bf16[96,256]{1,0:T(8,128)(2,1)S(1)}, bf16[96,256]{1,0:T(8,128)(2,1)S(1)}, u32[]{:S(2)}, u32[]{:S(2)}) collective-permute-start(bf16[96,256]{1,0:T(8,128)(2,1)S(1)} %pad_maximum_fusion.2), channel_id=1, source_target_pairs={{0,1},{1,0},{2,3},{3,2},{4,5},{5,4},{6,7},{7,6},{8,9},{9,8},{10,11... | collective-permute-start | bytes 147464 | tf_op jit(solution)/shard_map/ppermute | solution.py:490
  108.5 4.1 %collective-permute-start.18 = (bf16[96,256]{1,0:T(8,128)(2,1)S(1)}, bf16[96,256]{1,0:T(8,128)(2,1)S(1)}, u32[]{:S(2)}, u32[]{:S(2)}) collective-permute-start(bf16[96,256]{1,0:T(8,128)(2,1)S(1)} %pad_maximum_fusion.1), channel_id=1, source_target_pairs={{0,2},{1,3},{2,0},{3,1},{4,6},{5,7},{6,4},{7,5},{8,10},{9,11},{10,... | collective-permute-start | bytes 147464 | tf_op jit(solution)/shard_map/ppermute | solution.py:490
